TPU v7x, 512 devices: a whole 4x8x8 slice. The times are simulated.
512 devices in a mesh: ep: 32 (over z, x), tp: 16 (over y, core).
Axes of the slice: x: 4, y: 8, z: 8, core: 2. Of those that a mesh axis runs over, the one named last changes fastest.
Arguments:
- tokens: bfloat16 [256, 4096], P('ep', 'tp'), may hold values from -6 to 6
- norm_gain: float32 [4096], replicated, may hold values from 0.1 to 1.9
- route_experts: int32 [256, 2], P('ep'), may hold values from 0 to 63, all different within a row; in each aligned block of 8 rows (0 to 7, 8 to 15, ...) at most 2 rows name the same one
- route_logits: float32 [256, 2], P('ep'), may hold values from -4 to 4
- expert_gate: bfloat16 [64, 4096, 1024], P('ep', None, 'tp'), may hold values from -0.09375 to 0.09375
- expert_up: bfloat16 [64, 4096, 1024], P('ep', None, 'tp'), may hold values from -0.09375 to 0.09375
- expert_down: bfloat16 [64, 1024, 4096], P('ep', 'tp'), may hold values from -0.1875 to 0.1875
- dense_gate: bfloat16 [4096, 1024], P(None, 'tp'), may hold values from -0.09375 to 0.09375
- dense_up: bfloat16 [4096, 1024], P(None, 'tp'), may hold values from -0.09375 to 0.09375
- dense_down: bfloat16 [1024, 4096], P('tp'), may hold values from -0.1875 to 0.1875
- mix_weight: float32 [4096], replicated, may hold values from -0.09375 to 0.09375
- out_gain: float32 [4096], P('tp'), may hold values from 0.1 to 1.9
Outputs:
- result: bfloat16 [256, 4096], P('ep', 'tp')
Inputs may be any that keep to these rules, and one draw needn't show every extreme that they name: `route_experts`: each row names 2 different experts; the 8 rows of one index of ep (aligned blocks) name any one expert at most 2 times, and some block names some expert exactly 2 times; every expert is named somewhere.
All inputs are finite; a program needn't handle non-finite values.
Results may differ from a plain program's by a relative error of at most 0.0025.
Values may be sent and summed in bfloat16 or wider, within the bound.
A program may use at most 64 MiB of HBM per device.

v0:
```python
import jax
import jax.numpy as jnp
from jax import lax
from jax.sharding import Mesh
from jax.sharding import PartitionSpec as P

CAP = 2
TP = ("tp_0", "tp_1")


norm_eps = 1e-06


def summed_rows(x, axes, dim):
    if not axes:
        return x
    nearer = lax.psum_scatter(x, axes[0], scatter_dimension=dim, tiled=True)
    return summed_rows(nearer, axes[1:], dim)


def local(
    tokens,
    norm_gain,
    route_experts,
    route_logits,
    expert_gate,
    expert_up,
    expert_down,
    dense_gate,
    dense_up,
    dense_down,
    mix_weight,
    out_gain,
):
    tok_rows, width_part = tokens.shape
    groups = lax.axis_size(TP)
    width = width_part * groups
    whole_rows = lax.all_gather(tokens, TP, axis=1, tiled=True).astype(jnp.float32)
    normed = (
        whole_rows
        * lax.rsqrt(jnp.mean(whole_rows * whole_rows, axis=1, keepdims=True) + norm_eps)
        * norm_gain
    ).astype(jnp.bfloat16)
    weights = jax.nn.softmax(route_logits, axis=-1)
    top_count = route_experts.shape[1]
    local_experts = expert_gate.shape[0]
    peer_count = lax.axis_size("ep")
    experts = local_experts * peer_count
    dense_hidden = (
        jax.nn.silu(jnp.dot(normed, dense_gate, preferred_element_type=jnp.float32))
        * jnp.dot(normed, dense_up, preferred_element_type=jnp.float32)
    ).astype(jnp.bfloat16)
    dense_out = summed_rows(
        jnp.dot(dense_hidden, dense_down, preferred_element_type=jnp.float32), TP, 1
    )
    mix_gate = jax.nn.sigmoid(
        jnp.dot(normed.astype(jnp.float32), mix_weight, precision=lax.Precision.HIGHEST)
    )
    flat_routes = route_experts.reshape(-1)
    expert_ids = jnp.arange(experts, dtype=jnp.int32)
    capacity = CAP
    slot_count = experts * capacity
    route_hits = (flat_routes[:, None] == expert_ids[None, :]).astype(jnp.int32)
    before = jnp.cumsum(route_hits, axis=0) - route_hits
    slot_rank = jnp.sum(before * route_hits, axis=1)
    position = flat_routes * capacity + slot_rank
    onehot_place = (position[:, None] == jnp.arange(slot_count, dtype=jnp.int32)[None, :]).astype(
        jnp.float32
    )
    placing = jnp.sum(onehot_place.reshape(tok_rows, top_count, slot_count), axis=1).T.astype(
        jnp.bfloat16
    )
    outgoing = jnp.dot(placing, normed, preferred_element_type=jnp.float32).astype(jnp.bfloat16)
    received = lax.all_to_all(outgoing, "ep", split_axis=0, concat_axis=0, tiled=True)
    arranged = (
        received.reshape(peer_count, local_experts, capacity, width)
        .transpose(1, 0, 2, 3)
        .reshape(local_experts, peer_count * capacity, width)
    )
    gate_act = jnp.einsum("erd,edf->erf", arranged, expert_gate, preferred_element_type=jnp.float32)
    up_act = jnp.einsum("erd,edf->erf", arranged, expert_up, preferred_element_type=jnp.float32)
    hidden = (jax.nn.silu(gate_act) * up_act).astype(jnp.bfloat16)
    partial_value = jnp.einsum(
        "erf,efd->erd", hidden, expert_down, preferred_element_type=jnp.float32
    )
    summed = lax.psum_scatter(partial_value, TP, scatter_dimension=2, tiled=True)
    back_send = (
        summed.reshape(local_experts, peer_count, capacity, width_part)
        .transpose(1, 0, 2, 3)
        .reshape(slot_count, width_part)
    )
    returned = lax.all_to_all(back_send, "ep", split_axis=0, concat_axis=0, tiled=True)
    combine_map = jnp.sum(
        (onehot_place * weights.reshape(-1)[:, None]).reshape(tok_rows, top_count, slot_count),
        axis=1,
    )
    expert_mix = jnp.dot(combine_map, returned, precision=lax.Precision.HIGHEST)
    combined = expert_mix + mix_gate[:, None] * dense_out
    squares_out = lax.psum(jnp.sum(combined * combined, axis=1), TP)
    result = combined * lax.rsqrt(squares_out[:, None] / width + norm_eps) * out_gain
    return result.astype(jnp.bfloat16)


def solution(mesh):
    split = Mesh(mesh.devices.reshape(mesh.shape["ep"], 8, 2), ("ep", "tp_0", "tp_1"))
    in_specs = (
        P("ep", TP),
        P(),
        P("ep", None),
        P("ep", None),
        P("ep", None, TP),
        P("ep", None, TP),
        P("ep", TP, None),
        P(None, TP),
        P(None, TP),
        P(TP, None),
        P(),
        P(TP),
    )
    out_specs = P("ep", TP)
    return jax.shard_map(local, mesh=split, in_specs=in_specs, out_specs=out_specs, check_vma=False)
```

profile of v0, /device:TPU:1, one launch (start us, length us, event | category | flops | bytes accessed | tf_op | source)
XLA Modules:
  0.0 228.6 jit_solution(5264460515615627035)
XLA Ops:
  6.5 0.8 reduce_max.9
  7.3 0.7 fusion.26
  8.0 0.7 fusion.25
  8.7 0.8 copy.34
  10.0 21.2 %all_gather.3 = bf16[8,4096]{1,0:T(8,128)(2,1)S(1)} all-gather(bf16[8,256]{1,0:T(8,128)(2,1)} %param.12), channel_id=1, replica_groups=mesh['ep'=32,'tp_0'=8,'tp_1'=2] {'tp_0','tp_1'}, dimensions={1}, use_global_device_ids=true | all-gather | bytes 69632 | tf_op jit(solution)/shard_map/all_gather | solution.py:38
  31.4 1.2 convolution_convert_fusion
  32.7 0.4 all_to_all.14
  33.1 37.3 %all_to_all.21 = bf16[32,4,4096]{2,1,0:T(4,128)(2,1)S(1)} all-to-all(bf16[32,4,4096]{2,1,0:T(4,128)(2,1)S(1)} %all_to_all.14), channel_id=1, replica_groups=mesh['ep'=32,'tp_0'=8,'tp_1'=2] {'ep'}, dimensions={0} | all-to-all | bytes 2097152 | tf_op jit(solution)/shard_map/all_to_all | solution.py:74
  70.4 0.5 reshape.67
  70.9 2.0 copy.41
  73.0 1.6 reshape.68
  74.5 0.4 fusion.35
  75.0 3.4 %fusion.1 = f32[2,64,4096]{2,1,0:T(8,128)} fusion(bf16[2,64,4096]{2,1,0:T(8,128)(2,1)S(1)} %copy-done, bf16[2,64,4096]{2,1,0:T(8,128)(2,1)S(1)} %reshape.68, bf16[2,4096,64]{1,2,0:T(8,128)(2,1)} %param.17, f32[2,64,64]{2,1,0:T(8,128)S(1)} %fusion.35), kind=kOutput, calls=%fused_computation.3 | convolution fusion | flops 134266880 | bytes 5275648 | tf_op jit(solution)/shard_map/erf,efd->erd/dot_general | solution.py:83
  78.5 0.9 copy-done.2
  79.7 1.3 fusion.3
  81.0 55.0 %reduce-scatter.4.cloned.1.call-done = f32[2,64,256]{2,1,0:T(8,128)} async-done(((f32[2,64,4096]{2,1,0:T(8,128)}), f32[2,64,256]{2,1,0:T(8,128)}) %reduce-scatter.4.cloned.1.call-update) | async-done | bytes 131088 | tf_op jit(solution)/shard_map/reduce_scatter | solution.py:86
  136.0 1.0 reshape.69
  137.0 0.7 copy.39
  137.7 8.9 %all-to-all-start.1 = ((f32[32,4,256]{2,1,0:T(4,128)}), f32[32,4,256]{2,1,0:T(4,128)S(1)}, u32[]{:S(2)}, u32[]{:S(2)}) async-start(f32[32,4,256]{2,1,0:T(4,128)} %copy.39), calls=%async_computation.2 | async-start | bytes 262144 | tf_op jit(solution)/shard_map/all_to_all | solution.py:92
  146.7 26.9 %reduce-scatter.6.cloned.1.call-done = f32[8,512]{1,0:T(8,128)} async-done(((f32[8,4096]{1,0:T(8,128)}), f32[8,512]{1,0:T(8,128)}) %reduce-scatter.6.cloned.1.call-update) | async-done | bytes 16400 | tf_op jit(solution)/shard_map/reduce_scatter | solution.py:17
  174.0 23.7 %reduce-scatter.8.cloned.1.call-done = f32[8,256]{1,0:T(8,128)} async-done(((f32[8,512]{1,0:T(8,128)}), f32[8,256]{1,0:T(8,128)}) %reduce-scatter.8.cloned.1.call-update) | async-done | bytes 8208 | tf_op jit(solution)/shard_map/reduce_scatter | solution.py:17
  197.7 1.0 multiply_reduce_fusion
  198.7 22.7 %psum.7 = f32[8]{0:T(128)S(1)} all-reduce(f32[8]{0:T(128)S(1)} %get-tuple-element.7), channel_id=1, replica_groups=mesh['ep'=32,'tp_0'=8,'tp_1'=2] {'tp_0','tp_1'}, use_global_device_ids=true, to_apply=%region_11.12 | all-reduce | flops 8 | bytes 64 | tf_op jit(solution)/shard_map/psum | solution.py:99
  221.4 0.7 multiply_convert_fusion
  (37 shorter events, 1.7 us)
Async XLA Ops:
  6.5 68.4 %copy-start = (bf16[2,64,4096]{2,1,0:T(8,128)(2,1)S(1)}, bf16[2,64,4096]{2,1,0:T(8,128)(2,1)}, u32[]{:S(2)}) copy-start(bf16[2,64,4096]{2,1,0:T(8,128)(2,1)} %param.18) | copy-start | bytes 3145732
  6.5 129.4 %reduce-scatter.4.cloned.1.call-start = ((), (), s32[]{:S(2)}) async-start(), calls=%async_computation.5 | async-start | bytes 2228224 | tf_op jit(solution)/shard_map/reduce_scatter | solution.py:86
  73.0 1.6 copy-start.1
  78.4 1.0 copy-start.2
  78.4 1.0 copy-start.5
  78.4 1.3 copy-start.3
  78.4 1.4 copy-start.4
  78.4 95.3 %copy-start.7 = (f32[4096]{0:T(1024)S(1)}, f32[4096]{0:T(1024)}, u32[]{:S(2)}) copy-start(f32[4096]{0:T(1024)} %param.22) | copy-start | bytes 49156
  78.4 143.0 %copy-start.6 = (f32[256]{0:T(256)S(1)}, f32[256]{0:T(256)}, u32[]{:S(2)}) copy-start(f32[256]{0:T(256)} %param.23) | copy-start | bytes 3076
  78.4 95.2 %reduce-scatter.6.cloned.1.call-start = ((), (), s32[]{:S(2)}) async-start(), calls=%async_computation.6 | async-start | bytes 147456 | tf_op jit(solution)/shard_map/reduce_scatter | solution.py:17
  137.7 36.3 %all-to-all-start.1 = ((f32[32,4,256]{2,1,0:T(4,128)}), f32[32,4,256]{2,1,0:T(4,128)S(1)}, u32[]{:S(2)}, u32[]{:S(2)}) async-start(f32[32,4,256]{2,1,0:T(4,128)} %copy.39), calls=%async_computation.2 | async-start | bytes 262144 | tf_op jit(solution)/shard_map/all_to_all | solution.py:92
  146.6 51.1 %reduce-scatter.8.cloned.1.call-start = ((), (), s32[]{:S(2)}) async-start(), calls=%async_computation.7 | async-start | bytes 24576 | tf_op jit(solution)/shard_map/reduce_scatter | solution.py:17
Sparse Core Ops, SparseCore 0:
  78.5 57.4 reduce-scatter.3
  138.8 34.8 reduce-scatter.5
  176.3 21.3 reduce-scatter.7
where the time goes:
time: 230 us; the launch traced here: 229 us
  waiting for transfers between devices  106 us (46%)
  blocking collectives  81.2 us (35%)
  between operations  13.2 us (6%)
  starting transfers between devices  9 us (4%)
  local copies, waits for them, and re-layouts  8.3 us (4%)
  matrix products  7.81 us (3%)
  other arithmetic  3.38 us (1%)
    reduce_scatter x1, waiting for transfers between devices, local(): lax.psum_scatter(partial_value, TP, scatter_dimension=2, tiled=True)  55 us
    reduce_scatter x2, waiting for transfers between devices, summed_rows(): nearer = lax.psum_scatter(x, axes[0], scatter_dimension=dim, tiled=True)  50.6 us
    all_to_all x1, blocking collectives, local(): lax.all_to_all(outgoing, 'ep', split_axis=0, concat_axis=0, tiled=True)  37.3 us
    psum x1, blocking collectives, local(): squares_out = lax.psum(jnp.sum(combined * combined, axis=1), TP)  22.7 us
    all_gather x1, blocking collectives, local(): lax.all_gather(tokens, TP, axis=1, tiled=True).astype(jnp.float32)  21.2 us
    all_to_all x1, starting transfers between devices, local(): lax.all_to_all(back_send, 'ep', split_axis=0, concat_axis=0, tiled=True)  8.91 us
  transfers between devices with their start and end apart: 4, of which 3 were waited for; matrix products, arithmetic and copies ran while one was open for 2% of the time, Pallas kernels for 0%

commit v1 on v0

v1 whole, which is shorter than its diff:
```python
import functools

import jax
import jax.numpy as jnp
from jax import lax
from jax.experimental import pallas as pl
from jax.experimental.pallas import tpu as pltpu
from jax.sharding import PartitionSpec as P

MESH = pl.DeviceIdType.MESH
F32 = jnp.float32
BF16 = jnp.bfloat16
EPS = 1e-06

NX, NZ, NY = 4, 8, 8
NEP = NX * NZ
NTP = 2 * NY
ROWS = 128
PART = 256
WIDTH = 4096


def rcopy(src, dst, send_sem, recv_sem, device):
    return pltpu.make_async_remote_copy(
        src_ref=src,
        dst_ref=dst,
        send_sem=send_sem,
        recv_sem=recv_sem,
        device_id=device,
        device_id_type=MESH,
    )


def nt_dot(a, b):
    return lax.dot_general(a, b, (((1,), (1,)), ((), ())), preferred_element_type=F32)


def silu(v):
    return v / (1.0 + jnp.exp(-v))


def kernel(
    tok,
    gain,
    routes,
    logits,
    wg,
    wu,
    wd,
    dg,
    du,
    dd,
    mixw,
    ogain,
    out,
    w_gu,
    wd_own,
    wd_par,
    w_dense,
    d_down,
    a2a_out,
    a2a_in,
    gathered,
    tok_all,
    dense_out,
    dense_in,
    comb,
    h_own,
    h_par,
    q_out,
    q_in,
    s_out,
    s_in,
    kept,
    ret_out,
    ret_in,
    sq_out,
    sq_in,
    ssq,
    gate_ref,
    w_sem,
    wp_ssem,
    wp_rsem,
    a2a_ssem,
    a2a_rsem,
    tok_ssem,
    tok_rsem,
    dense_ssem,
    dense_rsem,
    ag_ssem,
    ag_rsem,
    pf_ssem,
    pf_rsem,
    h_ssem,
    h_rsem,
    q_ssem,
    q_rsem,
    sc_ssem,
    sc_rsem,
    ret_ssem,
    ret_rsem,
    sq_ssem,
    sq_rsem,
):
    me_e = lax.axis_index("ep")
    me_t = lax.axis_index("tp")
    z, x = me_e // NX, me_e % NX
    y, core = me_t // 2, me_t % 2
    partner = (me_e, y * 2 + 1 - core)

    def ydev(step):
        return (me_e, ((y + step + NY) % NY) * 2 + core)

    def ysrc(step, c):
        return ((y + step + NY) % NY) * 2 + c

    def ep_peer(i):
        zi, xi = i // NX, i % NX
        dz, dx = (zi + 1) // 2, (xi + 1) // 2
        dz = 4 + dz * (1 - 2 * (zi % 2))
        dx = 2 + dx * (1 - 2 * (xi % 2))
        return ((z + dz) % NZ) * NX + (x + dx) % NX

    barrier = pltpu.get_barrier_semaphore()

    def greet_ep(k, carry):
        pl.semaphore_signal(barrier, inc=1, device_id=(ep_peer(k), me_t), device_id_type=MESH)
        return carry

    def greet_tp(k, carry):
        pl.semaphore_signal(
            barrier, inc=1, device_id=(me_e, (me_t + k) % NTP), device_id_type=MESH
        )
        return carry

    lax.fori_loop(0, NEP - 1, greet_ep, 0)
    lax.fori_loop(1, NTP, greet_tp, 0)

    loads = [
        pltpu.make_async_copy(dg, w_dense.at[pl.ds(0, 64)], w_sem.at[0]),
        pltpu.make_async_copy(du, w_dense.at[pl.ds(64, 64)], w_sem.at[1]),
        pltpu.make_async_copy(dd, d_down, w_sem.at[2]),
        pltpu.make_async_copy(wg, w_gu.at[pl.ds(0, 2)], w_sem.at[3]),
        pltpu.make_async_copy(wu, w_gu.at[pl.ds(2, 2)], w_sem.at[4]),
    ]
    for k in range(NY):
        columns = pl.ds(pl.multiple_of((2 * k + core) * PART, PART), PART)
        loads.append(pltpu.make_async_copy(wd.at[:, :, columns], wd_own.at[k], w_sem.at[5 + k]))
    for load in loads:
        load.start()

    lane = lax.broadcasted_iota(jnp.int32, (8, 256), 1)
    sub = lax.broadcasted_iota(jnp.int32, (8, 256), 0)
    expert = 2 * (lane // 8) + (lane // 2) % 2
    half = (lane // 4) % 2
    r0 = jnp.zeros((8, 256), jnp.int32)
    r1 = jnp.zeros((8, 256), jnp.int32)
    l0 = jnp.zeros((8, 256), F32)
    l1 = jnp.zeros((8, 256), F32)
    for t in range(8):
        r0 = jnp.where(sub == t, routes[0, t], r0)
        r1 = jnp.where(sub == t, routes[1, t], r1)
        l0 = jnp.where(sub == t, logits[0, t], l0)
        l1 = jnp.where(sub == t, logits[1, t], l1)
    top = jnp.maximum(l0, l1)
    e0, e1 = jnp.exp(l0 - top), jnp.exp(l1 - top)
    is0, is1 = (r0 == expert), (r1 == expert)
    hit = jnp.where(is0, 1.0, 0.0) + jnp.where(is1, 1.0, 0.0)
    before = jnp.zeros((8, 256), F32)
    for t in range(7):
        before = before + jnp.where(sub > t, hit[t : t + 1, :], 0.0)
    placed = jnp.where(before == (lane % 2).astype(F32), hit, 0.0)
    weight = (jnp.where(is0, e0, 0.0) + jnp.where(is1, e1, 0.0)) / (e0 + e1) * placed
    comb[0:8, :] = jnp.where(half == 0, weight, 0.0)
    comb[8:16, :] = jnp.where(half == 1, weight, 0.0)
    place = jnp.concatenate(
        [jnp.where(half == 0, placed, 0.0), jnp.where(half == 1, placed, 0.0)], axis=0
    ).astype(BF16)
    tok_value = tok[...]
    halves = jnp.concatenate(
        [tok_value[:, 0:128].astype(F32), tok_value[:, 128:256].astype(F32)], axis=0
    ).astype(BF16)
    a2a_out[...] = (
        lax.dot_general(place, halves, (((0,), (0,)), ((), ())), preferred_element_type=F32)
        .astype(BF16)
        .reshape(NEP, 8, 128)
    )

    pl.semaphore_wait(barrier, NEP - 1 + NTP - 1)

    def send_a2a(k, carry):
        peer = ep_peer(k)
        rcopy(a2a_out.at[peer], a2a_in.at[me_e], a2a_ssem, a2a_rsem, (peer, me_t)).start()
        return carry

    lax.fori_loop(0, NEP - 1, send_a2a, 0)

    def send_tok(k, carry):
        to = (me_t + k) % NTP
        rcopy(tok, tok_all.at[me_t], tok_ssem, tok_rsem, (me_e, to)).start()
        return carry

    lax.fori_loop(1, NTP, send_tok, 0)
    tok_all[me_t] = tok_value
    a2a_in[me_e] = a2a_out[me_e]

    wparts = []
    for k in range(NY):
        columns = pl.ds(pl.multiple_of((2 * k + 1 - core) * PART, PART), PART)
        copy = rcopy(wd.at[:, :, columns], wd_par.at[k], wp_ssem.at[k], wp_rsem.at[k], partner)
        copy.start()
        wparts.append(copy)

    rcopy(
        tok_all.at[pl.ds(0, NTP - 1)],
        tok_all.at[pl.ds(0, NTP - 1)],
        tok_ssem,
        tok_rsem,
        partner,
    ).wait_recv()
    squares = jnp.zeros((8, PART), F32)
    for j in range(NTP):
        v = tok_all[j].astype(F32)
        squares = squares + v * v
    scale = lax.rsqrt(jnp.sum(squares, axis=1, keepdims=True) / WIDTH + EPS)
    for load in loads[0:3]:
        load.wait()
    act = jnp.zeros((8, 128), F32)
    mix_acc = jnp.zeros((8, PART), F32)
    for j in range(NTP):
        cols = slice(j * PART, (j + 1) * PART)
        n = (tok_all[j].astype(F32) * scale * gain[:, cols]).astype(BF16)
        mix_acc = mix_acc + n.astype(F32) * mixw[:, cols]
        act = act + nt_dot(n, w_dense[:, cols])
    gate_ref[...] = jnp.broadcast_to(
        jax.nn.sigmoid(jnp.sum(mix_acc, axis=1, keepdims=True)), (8, 128)
    )
    dense_h = (silu(act[:, 0:64]) * act[:, 64:128]).astype(BF16)
    for j in range(NTP):
        cols = slice(j * PART, (j + 1) * PART)
        dense_out[j] = jnp.dot(dense_h, d_down[:, cols], preferred_element_type=F32)

    def send_dense(k, carry):
        to = (me_t + k) % NTP
        rcopy(
            dense_out.at[to], dense_in.at[me_t], dense_ssem, dense_rsem, (me_e, to)
        ).start()
        return carry

    lax.fori_loop(1, NTP, send_dense, 0)
    dense_in[me_t] = dense_out[me_t]

    rcopy(
        a2a_out.at[pl.ds(0, NEP - 1)],
        a2a_in.at[pl.ds(0, NEP - 1)],
        a2a_ssem,
        a2a_rsem,
        partner,
    ).wait_recv()
    pairs = a2a_in[...].astype(F32).reshape(16, 2, 8, 128)
    even, odd = pairs[:, 0], pairs[:, 1]
    sub3 = lax.broadcasted_iota(jnp.int32, (16, 8, 128), 1)
    left = jnp.where(sub3 < 4, even, pltpu.roll(odd, 4, 1)).reshape(ROWS, 128)
    right = jnp.where(sub3 < 4, pltpu.roll(even, 4, 1), odd).reshape(ROWS, 128)
    gathered[me_t, :, 0:128] = left.astype(BF16)
    gathered[me_t, :, 128:256] = right.astype(BF16)

    sends = []

    def ag_send(slot, rows, sem, device):
        ref = gathered.at[slot, rows]
        copy = rcopy(ref, ref, ag_ssem.at[len(sends)], ag_rsem.at[sem], device)
        copy.start()
        sends.append(copy)

    def ag_wait(slot, rows, sem):
        ref = gathered.at[slot, rows]
        rcopy(ref, ref, ag_ssem.at[0], ag_rsem.at[sem], partner).wait_recv()

    passes = []

    def pass_on(rel):
        ref = gathered.at[ysrc(rel, core)]
        copy = rcopy(ref, ref, pf_ssem.at[rel], pf_rsem.at[rel], partner)
        copy.start()
        passes.append(copy)

    whole, low, high = pl.ds(0, ROWS), pl.ds(0, ROWS // 2), pl.ds(ROWS // 2, ROWS // 2)
    ag_send(me_t, whole, 6, ydev(2))
    ag_send(me_t, whole, 2, ydev(-2))
    ag_send(me_t, whole, 7, ydev(1))
    ag_send(me_t, whole, 1, ydev(-1))
    pass_on(0)
    ssq[...] = left * left + right * right

    def add_squares(slot):
        v = gathered[slot].astype(F32)
        v = v * v
        ssq[...] += v[:, 0:128] + v[:, 128:256]

    s6, s2 = ysrc(6, core), ysrc(2, core)
    ag_wait(s6, whole, 6)
    ag_send(s6, low, 4, ydev(2))
    ag_send(s6, whole, 5, ydev(1))
    ag_wait(s2, whole, 2)
    ag_send(s2, high, 8, ydev(-2))
    ag_send(s2, whole, 3, ydev(-1))
    pass_on(6)
    pass_on(2)
    for rel in (7, 1):
        ag_wait(ysrc(rel, core), whole, rel)
        pass_on(rel)
    for rel in (6, 2, 7, 1):
        add_squares(ysrc(rel, core))
    for rel in (5, 3):
        ag_wait(ysrc(rel, core), whole, rel)
        pass_on(rel)
        add_squares(ysrc(rel, core))
    s4 = ysrc(4, core)
    ag_wait(s4, low, 4)
    ag_wait(s4, high, 8)
    pass_on(4)
    add_squares(s4)
    for rel in (0, 6, 2, 7, 1, 5, 3, 4):
        slot = ysrc(rel, 1 - core)
        ref = gathered.at[slot]
        rcopy(ref, ref, pf_ssem.at[rel], pf_rsem.at[rel], partner).wait_recv()
        add_squares(slot)

    row_scale = lax.rsqrt(jnp.sum(ssq[...], axis=1, keepdims=True) / WIDTH + EPS)
    loads[3].wait()
    loads[4].wait()
    acts = jnp.zeros((ROWS, 256), F32)
    for j in range(NTP):
        cols = slice(j * PART, (j + 1) * PART)
        n = (gathered[j].astype(F32) * row_scale * gain[:, cols]).astype(BF16)
        acts = acts + nt_dot(n, w_gu[:, :, cols].reshape(256, PART))
    hidden = silu(acts[:, 0:128]) * acts[:, 128:256]
    row = lax.broadcasted_iota(jnp.int32, (ROWS, 128), 0)
    col = lax.broadcasted_iota(jnp.int32, (ROWS, 128), 1)
    hidden = jnp.where((row // 2) % 2 == col // 64, hidden, 0.0).astype(BF16)
    h_own[...] = hidden
    h_copy = rcopy(h_own, h_par, h_ssem, h_rsem, partner)
    h_copy.start()
    for load in loads[5:]:
        load.wait()
    for copy in wparts:
        copy.wait_recv()
    h_copy.wait_recv()

    diagonal = row == col

    def partial(rel):
        k = (y + rel) % NY
        return jnp.dot(
            h_own[...], wd_own[k].reshape(128, PART), preferred_element_type=F32
        ) + jnp.dot(h_par[...], wd_par[k].reshape(128, PART), preferred_element_type=F32)

    def pack(value, slot):
        most = jnp.maximum(jnp.max(jnp.abs(value), axis=1, keepdims=True), 1e-30)
        q_out[slot] = jnp.round(value * (32767.0 / most)).astype(jnp.int16)
        s_out[slot] = jnp.sum(
            jnp.where(diagonal, most * (1.0 / 32767.0), 0.0), axis=0, keepdims=True
        )

    def unpack(slot, sslot):
        unit = jnp.sum(jnp.where(diagonal, s_in[sslot], 0.0), axis=1, keepdims=True)
        return q_in[slot].astype(F32) * unit

    qsends = []

    def q_send(slot, rows, sem, device):
        copy = rcopy(
            q_out.at[slot, rows], q_in.at[slot, rows], q_ssem.at[sem], q_rsem.at[sem], device
        )
        copy.start()
        qsends.append(copy)
        copy = rcopy(s_out.at[slot], s_in.at[sem], sc_ssem.at[sem], sc_rsem.at[sem], device)
        copy.start()
        qsends.append(copy)

    def q_wait(slot, rows, sem):
        rcopy(
            q_out.at[slot, rows], q_in.at[slot, rows], q_ssem.at[sem], q_rsem.at[sem], partner
        ).wait_recv()
        rcopy(s_out.at[slot], s_in.at[sem], sc_ssem.at[sem], sc_rsem.at[sem], partner).wait_recv()

    pack(partial(4), 2)
    q_send(2, low, 2, ydev(2))
    q_send(2, high, 7, ydev(-2))
    pack(partial(3), 0)
    q_send(0, whole, 0, ydev(1))
    pack(partial(5), 1)
    q_send(1, whole, 1, ydev(-1))
    pack(partial(1), 3)
    q_send(3, whole, 3, ydev(1))
    pack(partial(7), 4)
    q_send(4, whole, 4, ydev(-1))
    kept[0] = partial(2)
    kept[1] = partial(6)
    kept[2] = partial(0)
    q_wait(0, whole, 0)
    q_wait(2, low, 2)
    total = kept[0] + unpack(0, 0)
    far = jnp.where(lax.broadcasted_iota(jnp.int32, (ROWS, PART), 0) < ROWS // 2, 1.0, 0.0)
    q_wait(2, high, 7)
    q_wait(1, whole, 1)
    pack(total + unpack(2, 2) * far, 5)
    q_send(5, whole, 5, ydev(2))
    pack(kept[1] + unpack(1, 1) + unpack(2, 7) * (1.0 - far), 6)
    q_send(6, whole, 6, ydev(-2))
    q_wait(3, whole, 3)
    q_wait(4, whole, 4)
    kept[2] += unpack(3, 3) + unpack(4, 4)
    q_wait(5, whole, 5)
    q_wait(6, whole, 6)
    summed = kept[2] + unpack(5, 5) + unpack(6, 6)

    left = summed[:, 0:128].reshape(16, 8, 128)
    right = summed[:, 128:256].reshape(16, 8, 128)
    even = jnp.where(sub3 < 4, left, pltpu.roll(right, 4, 1))
    odd = jnp.where(sub3 < 4, pltpu.roll(left, 4, 1), right)
    ret_out[...] = jnp.stack([even, odd], axis=1).reshape(NEP, 8, 128)

    def send_ret(k, carry):
        peer = ep_peer(k)
        rcopy(ret_out.at[peer], ret_in.at[me_e], ret_ssem, ret_rsem, (peer, me_t)).start()
        return carry

    lax.fori_loop(0, NEP - 1, send_ret, 0)
    ret_in[me_e] = ret_out[me_e]

    rcopy(
        dense_out.at[pl.ds(0, NTP - 1)],
        dense_in.at[pl.ds(0, NTP - 1)],
        dense_ssem,
        dense_rsem,
        partner,
    ).wait_recv()
    dense = dense_in[0]
    for j in range(1, NTP):
        dense = dense + dense_in[j]
    gate = gate_ref[...]
    dense = jnp.concatenate([gate, gate], axis=1) * dense

    rcopy(
        ret_out.at[pl.ds(0, NEP - 1)],
        ret_in.at[pl.ds(0, NEP - 1)],
        ret_ssem,
        ret_rsem,
        partner,
    ).wait_recv()
    mixed = jnp.dot(
        comb[...],
        ret_in[...].reshape(256, 128),
        preferred_element_type=F32,
        precision=lax.Precision.HIGHEST,
    )
    combined = jnp.concatenate([mixed[0:8], mixed[8:16]], axis=1) + dense
    own = combined * combined
    own = own[:, 0:128] + own[:, 128:256]
    sq_out[...] = own

    def send_sq(k, carry):
        to = (me_t + k) % NTP
        rcopy(sq_out, sq_in.at[me_t], sq_ssem, sq_rsem, (me_e, to)).start()
        return carry

    lax.fori_loop(1, NTP, send_sq, 0)
    sq_in[me_t] = own
    rcopy(
        sq_in.at[pl.ds(0, NTP - 1)], sq_in.at[pl.ds(0, NTP - 1)], sq_ssem, sq_rsem, partner
    ).wait_recv()
    total_sq = sq_in[0]
    for j in range(1, NTP):
        total_sq = total_sq + sq_in[j]
    final = lax.rsqrt(jnp.sum(total_sq, axis=1, keepdims=True) / WIDTH + EPS)
    out[...] = (combined * final * ogain[...]).astype(BF16)

    for copy in wparts + sends + passes + [h_copy] + qsends:
        copy.wait_send()
    for ref, ssem, rsem, n in (
        (a2a_out, a2a_ssem, a2a_rsem, NEP - 1),
        (tok_all, tok_ssem, tok_rsem, NTP - 1),
        (dense_out, dense_ssem, dense_rsem, NTP - 1),
        (ret_out, ret_ssem, ret_rsem, NEP - 1),
        (sq_in, sq_ssem, sq_rsem, NTP - 1),
    ):
        part = ref.at[pl.ds(0, n)]
        rcopy(part, part, ssem, rsem, partner).wait_send()


def local(
    tokens,
    norm_gain,
    route_experts,
    route_logits,
    expert_gate,
    expert_up,
    expert_down,
    dense_gate,
    dense_up,
    dense_down,
    mix_weight,
    out_gain,
):
    vmem = pl.BlockSpec(memory_space=pltpu.VMEM)
    smem = pl.BlockSpec(memory_space=pltpu.SMEM)
    hbm = pl.BlockSpec(memory_space=pl.ANY)
    dma = pltpu.SemaphoreType.DMA
    return pl.pallas_call(
        kernel,
        out_shape=jax.ShapeDtypeStruct((8, PART), BF16),
        in_specs=[vmem, vmem, smem, smem, hbm, hbm, hbm, hbm, hbm, hbm, vmem, vmem],
        out_specs=vmem,
        scratch_shapes=[
            pltpu.VMEM((4, 64, WIDTH), BF16),
            pltpu.VMEM((NY, 2, 64, PART), BF16),
            pltpu.VMEM((NY, 2, 64, PART), BF16),
            pltpu.VMEM((128, WIDTH), BF16),
            pltpu.VMEM((64, WIDTH), BF16),
            pltpu.VMEM((NEP, 8, 128), BF16),
            pltpu.VMEM((NEP, 8, 128), BF16),
            pltpu.VMEM((NTP, ROWS, PART), BF16),
            pltpu.VMEM((NTP, 8, PART), BF16),
            pltpu.VMEM((NTP, 8, PART), F32),
            pltpu.VMEM((NTP, 8, PART), F32),
            pltpu.VMEM((16, 256), F32),
            pltpu.VMEM((ROWS, 128), BF16),
            pltpu.VMEM((ROWS, 128), BF16),
            pltpu.VMEM((7, ROWS, PART), jnp.int16),
            pltpu.VMEM((7, ROWS, PART), jnp.int16),
            pltpu.VMEM((7, 1, 128), F32),
            pltpu.VMEM((8, 1, 128), F32),
            pltpu.VMEM((3, ROWS, PART), F32),
            pltpu.VMEM((NEP, 8, 128), F32),
            pltpu.VMEM((NEP, 8, 128), F32),
            pltpu.VMEM((8, 128), F32),
            pltpu.VMEM((NTP, 8, 128), F32),
            pltpu.VMEM((ROWS, 128), F32),
            pltpu.VMEM((8, 128), F32),
            dma((13,)),
            dma((NY,)),
            dma((NY,)),
            dma,
            dma,
            dma,
            dma,
            dma,
            dma,
            dma((8,)),
            dma((9,)),
            dma((8,)),
            dma((8,)),
            dma,
            dma,
            dma((8,)),
            dma((8,)),
            dma((8,)),
            dma((8,)),
            dma,
            dma,
            dma,
            dma,
        ],
        compiler_params=pltpu.CompilerParams(collective_id=0, has_side_effects=True),
    )(
        tokens,
        norm_gain.reshape(1, WIDTH),
        route_experts.T,
        route_logits.T,
        jnp.swapaxes(expert_gate, 1, 2),
        jnp.swapaxes(expert_up, 1, 2),
        expert_down,
        dense_gate.T,
        dense_up.T,
        dense_down,
        mix_weight.reshape(1, WIDTH),
        out_gain.reshape(1, PART),
    )


def solution(mesh):
    tp = "tp"
    in_specs = (
        P("ep", tp),
        P(),
        P("ep", None),
        P("ep", None),
        P("ep", None, tp),
        P("ep", None, tp),
        P("ep", tp, None),
        P(None, tp),
        P(None, tp),
        P(tp, None),
        P(),
        P(tp),
    )
    return jax.shard_map(
        local, mesh=mesh, in_specs=in_specs, out_specs=P("ep", tp), check_vma=False
    )
```

time: 230 us -> 66.1 us (0.29)
  waiting for transfers between devices: 106 us -> 0 us
  blocking collectives: 81.2 us -> 0 us
  Pallas kernels: 0 us -> 64.6 us
  between operations: 13.2 us -> 0.01 us
  starting transfers between devices: 9 us -> 0 us
  matrix products: 7.81 us -> 0 us
  local copies, waits for them, and re-layouts: 8.3 us -> 1.28 us
  other arithmetic: 3.38 us -> 0 us
    reduce_scatter x3 -> x0, waiting for transfers between devices: 106 us -> none  [the longest x1 55 us: local(): lax.psum_scatter(partial_value, TP, scatter_dimension=2, tiled=True)]
    pallas_call x0 -> x1, Pallas kernels: none -> 64.6 us  [local(): pl.pallas_call(kernel, out_shape=jax.ShapeDtypeStruct((8, PART), BF16), i...]
    all_to_all x1 -> x0, blocking collectives: 37.3 us -> none  [local(): lax.all_to_all(outgoing, 'ep', split_axis=0, concat_axis=0, tiled=True)]
    psum x1 -> x0, blocking collectives: 22.7 us -> none  [local(): squares_out = lax.psum(jnp.sum(combined * combined, axis=1), TP)]
    all_gather x1 -> x0, blocking collectives: 21.2 us -> none  [local(): lax.all_gather(tokens, TP, axis=1, tiled=True).astype(jnp.float32)]
    all_to_all x1 -> x0, starting transfers between devices: 8.91 us -> none  [local(): lax.all_to_all(back_send, 'ep', split_axis=0, concat_axis=0, tiled=True)]
    dot_general x7 -> x0, matrix products: 7.81 us -> none  [the longest x1 3.39 us: local(): jnp.einsum('erf,efd->erd', hidden, expert_down, preferred_element_type=jn...]
    reshape x5 -> x0, local copies, waits for them, and re-layouts: 5.09 us -> none  [the longest x2 2.55 us: local(): received.reshape(peer_count, local_experts, capacity, width)]
  transfers between devices with their start and end apart: 4 -> 0, of which waited for: 3 -> 0; matrix products, arithmetic and copies ran while one was open for 2% -> 0% of each run, Pallas kernels for 0% -> 0%
where the time goes in v1:
time: 66.1 us; the launch traced here: 65.8 us
  Pallas kernels  64.6 us (98%)
  local copies, waits for them, and re-layouts  1.28 us (2%)
    pallas_call x1, Pallas kernels, local(): pl.pallas_call(kernel, out_shape=jax.ShapeDtypeStruct((8, PART), BF16), i...  64.6 us

profile of v1, /device:TPU:1, one launch (start us, length us, event | category | flops | bytes accessed | tf_op | source)
XLA Modules:
  0.0 65.8 jit_solution(16051970788691623372)
XLA Ops:
  0.0 64.6 %shard_map.118 = bf16[8,256]{1,0:T(8,128)(2,1)} custom-call(bf16[8,256]{1,0:T(8,128)(2,1)} %tok.1, f32[1,4096]{1,0:T(1,128)} %bitcast.13, s32[2,8]{1,0:T(2,128)} %bitcast.15, f32[2,8]{1,0:T(2,128)} %bitcast.16, bf16[2,64,4096]{2,1,0:T(8,128)(2,1)} %bitcast.9, bf16[2,64,4096]{2,1,0:T(8,128)(2,1)} %bitcast.10, bf16[2,64,4096]{2,1,0:T(8,128)(2,1)} %wd.1, ...), custom_call_target="tpu_custom_call" | custom-call | tf_op jit(solution)/shard_map/pallas_call | solution.py:511
  64.6 1.3 %copy.14 = bf16[8,256]{1,0:T(8,128)(2,1)} copy(bf16[8,256]{1,0:T(8,128)(2,1)} %shard_map.118) | data formatting | bytes 8192

commit v2 on v1

v2 whole, which is shorter than its diff:
```python
import functools

import jax
import jax.numpy as jnp
from jax import lax
from jax.experimental import pallas as pl
from jax.experimental.pallas import tpu as pltpu
from jax.sharding import PartitionSpec as P

MESH = pl.DeviceIdType.MESH
F32 = jnp.float32
BF16 = jnp.bfloat16
EPS = 1e-06

NX, NZ, NY = 4, 8, 8
NEP = NX * NZ
NTP = 2 * NY
ROWS = 128
PART = 256
WIDTH = 4096


def rcopy(src, dst, send_sem, recv_sem, device):
    return pltpu.make_async_remote_copy(
        src_ref=src,
        dst_ref=dst,
        send_sem=send_sem,
        recv_sem=recv_sem,
        device_id=device,
        device_id_type=MESH,
    )


def nt_dot(a, b):
    return lax.dot_general(a, b, (((1,), (1,)), ((), ())), preferred_element_type=F32)


def silu(v):
    return v / (1.0 + jnp.exp(-v))


def kernel(
    tok_hbm,
    gain_hbm,
    routes_hbm,
    logits_hbm,
    wg,
    wu,
    wd,
    dg,
    du,
    dd,
    mixw_hbm,
    ogain_hbm,
    out,
    tok,
    gain,
    routes,
    logits,
    mixw,
    ogain,
    w_gu,
    wd_own,
    wd_par,
    w_dense,
    dd_own,
    dd_par,
    a2a_out,
    a2a_in,
    gathered,
    tok_all,
    dense_out,
    dense_in,
    dh_own,
    dh_par,
    comb,
    h_own,
    h_par,
    q_out,
    q_in,
    s_out,
    s_in,
    kept,
    ret_out,
    ret_in,
    sq_out,
    sq_in,
    ssq,
    gate_ref,
    i_sem,
    w_sem,
    wp_ssem,
    wp_rsem,
    a2a_ssem,
    a2a_rsem,
    tok_ssem,
    tok_rsem,
    tp_ssem,
    tp_rsem,
    dh_ssem,
    dh_rsem,
    dense_ssem,
    dense_rsem,
    ag_ssem,
    ag_rsem,
    pf_ssem,
    pf_rsem,
    h_ssem,
    h_rsem,
    q_ssem,
    q_rsem,
    sc_ssem,
    sc_rsem,
    ret_ssem,
    ret_rsem,
    sq_ssem,
    sq_rsem,
):
    me_e = lax.axis_index("ep")
    me_t = lax.axis_index("tp")
    z, x = lax.div(me_e, NX), lax.rem(me_e, NX)
    y, core = lax.div(me_t, 2), lax.rem(me_t, 2)
    other = 1 - core
    partner = (me_e, y * 2 + other)
    zs = [lax.rem(z + k, NZ) * NX for k in range(NZ)]
    xs = [lax.rem(x + k, NX) for k in range(NX)]
    ys = [lax.rem(y + k, NY) for k in range(NY)]
    peers = [zs[dz] + xs[dx] for dz in (4, 3, 5, 2, 6, 1, 7, 0) for dx in (2, 1, 3, 0)][:-1]
    y_order = (4, 3, 5, 2, 6, 1, 7)

    def ydev(step):
        return (me_e, ys[step % NY] * 2 + core)

    barrier = pltpu.get_barrier_semaphore()
    for peer in peers:
        pl.semaphore_signal(barrier, inc=1, device_id=(peer, me_t), device_id_type=MESH)
    for step in y_order:
        for c in range(2):
            pl.semaphore_signal(
                barrier, inc=1, device_id=(me_e, ys[step] * 2 + c), device_id_type=MESH
            )
    pl.semaphore_signal(barrier, inc=1, device_id=partner, device_id_type=MESH)

    smalls = [
        pltpu.make_async_copy(routes_hbm, routes, i_sem.at[0]),
        pltpu.make_async_copy(logits_hbm, logits, i_sem.at[1]),
        pltpu.make_async_copy(tok_hbm, tok, i_sem.at[2]),
        pltpu.make_async_copy(gain_hbm, gain, i_sem.at[3]),
        pltpu.make_async_copy(mixw_hbm, mixw, i_sem.at[4]),
        pltpu.make_async_copy(ogain_hbm, ogain, i_sem.at[5]),
    ]
    loads = [
        pltpu.make_async_copy(dg, w_dense.at[pl.ds(0, 64)], w_sem.at[0]),
        pltpu.make_async_copy(du, w_dense.at[pl.ds(64, 64)], w_sem.at[1]),
        pltpu.make_async_copy(wg, w_gu.at[pl.ds(0, 2)], w_sem.at[2]),
        pltpu.make_async_copy(wu, w_gu.at[pl.ds(2, 2)], w_sem.at[3]),
    ]

    def columns(k, c):
        return pl.ds(pl.multiple_of((2 * k + c) * PART, PART), PART)

    for k in range(NY):
        loads.append(
            pltpu.make_async_copy(dd.at[:, columns(k, core)], dd_own.at[k], w_sem.at[4 + k])
        )
    for k in range(NY):
        loads.append(
            pltpu.make_async_copy(wd.at[:, :, columns(k, core)], wd_own.at[k], w_sem.at[12 + k])
        )
    for load in smalls + loads:
        load.start()

    for load in smalls[0:3]:
        load.wait()
    lane = lax.broadcasted_iota(jnp.int32, (8, 256), 1)
    sub = lax.broadcasted_iota(jnp.int32, (8, 256), 0)
    expert = 2 * (lane // 8) + (lane // 2) % 2
    half = (lane // 4) % 2
    r0 = jnp.zeros((8, 256), jnp.int32)
    r1 = jnp.zeros((8, 256), jnp.int32)
    l0 = jnp.zeros((8, 256), F32)
    l1 = jnp.zeros((8, 256), F32)
    for t in range(8):
        r0 = jnp.where(sub == t, routes[0, t], r0)
        r1 = jnp.where(sub == t, routes[1, t], r1)
        l0 = jnp.where(sub == t, logits[0, t], l0)
        l1 = jnp.where(sub == t, logits[1, t], l1)
    top = jnp.maximum(l0, l1)
    e0, e1 = jnp.exp(l0 - top), jnp.exp(l1 - top)
    is0, is1 = (r0 == expert), (r1 == expert)
    hit = jnp.where(is0, 1.0, 0.0) + jnp.where(is1, 1.0, 0.0)
    before = jnp.zeros((8, 256), F32)
    for t in range(7):
        before = before + jnp.where(sub > t, hit[t : t + 1, :], 0.0)
    placed = jnp.where(before == (lane % 2).astype(F32), hit, 0.0)
    weight = (jnp.where(is0, e0, 0.0) + jnp.where(is1, e1, 0.0)) / (e0 + e1) * placed
    comb[0:8, :] = jnp.where(half == 0, weight, 0.0)
    comb[8:16, :] = jnp.where(half == 1, weight, 0.0)
    place = jnp.concatenate(
        [jnp.where(half == 0, placed, 0.0), jnp.where(half == 1, placed, 0.0)], axis=0
    ).astype(BF16)
    tok_value = tok[...]
    halves = jnp.concatenate(
        [tok_value[:, 0:128].astype(F32), tok_value[:, 128:256].astype(F32)], axis=0
    ).astype(BF16)
    a2a_out[...] = (
        lax.dot_general(place, halves, (((0,), (0,)), ((), ())), preferred_element_type=F32)
        .astype(BF16)
        .reshape(NEP, 8, 128)
    )
    a2a_in[me_e] = a2a_out[me_e]
    tok_all[core, y] = tok_value

    pl.semaphore_wait(barrier, NEP - 1 + NTP - 1)

    for peer in peers:
        rcopy(a2a_out.at[peer], a2a_in.at[me_e], a2a_ssem, a2a_rsem, (peer, me_t)).start()

    for step in y_order:
        rcopy(tok, tok_all.at[core, y], tok_ssem, tok_rsem, ydev(step)).start()

    wparts = []
    for k in range(NY):
        copy = rcopy(
            dd.at[:, columns(k, other)], dd_par.at[k], wp_ssem.at[k], wp_rsem.at[k], partner
        )
        copy.start()
        wparts.append(copy)
    for k in range(NY):
        copy = rcopy(
            wd.at[:, :, columns(k, other)],
            wd_par.at[k],
            wp_ssem.at[NY + k],
            wp_rsem.at[NY + k],
            partner,
        )
        copy.start()
        wparts.append(copy)

    rcopy(
        a2a_out.at[pl.ds(0, NEP - 1)],
        a2a_in.at[pl.ds(0, NEP - 1)],
        a2a_ssem,
        a2a_rsem,
        partner,
    ).wait_recv()
    pairs = a2a_in[...].astype(F32).reshape(16, 2, 8, 128)
    even, odd = pairs[:, 0], pairs[:, 1]
    sub3 = lax.broadcasted_iota(jnp.int32, (16, 8, 128), 1)
    left = jnp.where(sub3 < 4, even, pltpu.roll(odd, 4, 1)).reshape(ROWS, 128)
    right = jnp.where(sub3 < 4, pltpu.roll(even, 4, 1), odd).reshape(ROWS, 128)
    gathered[core, y, :, 0:128] = left.astype(BF16)
    gathered[core, y, :, 128:256] = right.astype(BF16)

    sends = []
    whole, low, high = pl.ds(0, ROWS), pl.ds(0, ROWS // 2), pl.ds(ROWS // 2, ROWS // 2)

    def ag_send(rel, rows, sem, step):
        ref = gathered.at[core, ys[rel], rows]
        copy = rcopy(ref, ref, ag_ssem.at[len(sends)], ag_rsem.at[sem], ydev(step))
        copy.start()
        sends.append(copy)

    def ag_wait(rel, rows, sem):
        ref = gathered.at[core, ys[rel], rows]
        rcopy(ref, ref, ag_ssem.at[0], ag_rsem.at[sem], partner).wait_recv()

    passes = []

    def pass_on(rel):
        ref = gathered.at[core, ys[rel]]
        copy = rcopy(ref, ref, pf_ssem.at[rel], pf_rsem.at[rel], partner)
        copy.start()
        passes.append(copy)

    def pass_wait(rel):
        ref = gathered.at[other, ys[rel]]
        rcopy(ref, ref, pf_ssem.at[rel], pf_rsem.at[rel], partner).wait_recv()

    def add_squares(c, rel):
        v = gathered[c, ys[rel]].astype(F32)
        v = v * v
        ssq[...] += v[:, 0:128] + v[:, 128:256]

    ag_send(0, low, 12, 2)
    ag_send(0, low, 4, -2)
    ag_send(0, high, 13, 2)
    ag_send(0, high, 5, -2)
    ag_send(0, whole, 14, 1)
    ag_send(0, whole, 2, -1)
    pass_on(0)
    ssq[...] = left * left + right * right

    tok_step = rcopy(
        tok_all.at[0, pl.ds(0, NY - 1)], tok_all.at[0, pl.ds(0, NY - 1)], tok_ssem, tok_rsem, partner
    )
    tok_step.wait_recv()
    tok_pass = rcopy(tok_all.at[core], tok_all.at[core], tp_ssem, tp_rsem, partner)
    tok_pass.start()
    for load in smalls[3:6] + loads[0:2]:
        load.wait()
    rcopy(tok_all.at[other], tok_all.at[other], tp_ssem, tp_rsem, partner).wait_recv()

    squares = jnp.zeros((8, PART), F32)
    for j in range(NTP):
        v = tok_all[j % 2, j // 2].astype(F32)
        squares = squares + v * v
    scale = lax.rsqrt(jnp.sum(squares, axis=1, keepdims=True) / WIDTH + EPS)
    act = jnp.zeros((8, 128), F32)
    mix_acc = jnp.zeros((8, PART), F32)
    for j in range(NTP):
        cols = slice(j * PART, (j + 1) * PART)
        n = (tok_all[j % 2, j // 2].astype(F32) * scale * gain[:, cols]).astype(BF16)
        mix_acc = mix_acc + n.astype(F32) * mixw[:, cols]
        act = act + nt_dot(n, w_dense[:, cols])
    gate_ref[...] = jnp.broadcast_to(
        jax.nn.sigmoid(jnp.sum(mix_acc, axis=1, keepdims=True)), (8, 128)
    )
    dh_own[...] = (silu(act[:, 0:64]) * act[:, 64:128]).astype(BF16)
    dh_copy = rcopy(dh_own, dh_par, dh_ssem, dh_rsem, partner)
    dh_copy.start()

    ag_wait(6, low, 12)
    ag_send(6, low, 8, 2)
    ag_send(6, low, 10, 1)
    ag_wait(2, low, 4)
    ag_send(2, low, 6, -1)
    ag_wait(6, high, 13)
    ag_send(6, high, 11, 1)
    ag_wait(2, high, 5)
    ag_send(2, high, 9, -2)
    ag_send(2, high, 7, -1)
    pass_on(6)
    pass_on(2)
    for load in loads[4:12]:
        load.wait()
    for copy in wparts[0:NY]:
        copy.wait_recv()
    dh_copy.wait_recv()
    for k in range(NY):
        dense_out[k] = jnp.dot(
            dh_own[...], dd_own[k], preferred_element_type=F32
        ) + jnp.dot(dh_par[...], dd_par[k], preferred_element_type=F32)
    dense_in[y] = dense_out[y]
    add_squares(core, 6)
    add_squares(core, 2)
    for rel in (7, 1):
        ag_wait(rel, whole, 2 * rel)
        pass_on(rel)
    for rel in (7, 1):
        add_squares(core, rel)
    for step in y_order:
        rcopy(
            dense_out.at[ys[step]], dense_in.at[y], dense_ssem, dense_rsem, ydev(step)
        ).start()
    for rel in (5, 3):
        ag_wait(rel, low, 2 * rel)
        ag_wait(rel, high, 2 * rel + 1)
        pass_on(rel)
    for rel in (0, 6, 2, 7, 1):
        pass_wait(rel)
        add_squares(other, rel)
    for rel in (5, 3):
        add_squares(core, rel)
    ag_wait(4, low, 8)
    ag_wait(4, high, 9)
    pass_on(4)
    add_squares(core, 4)
    for rel in (5, 3, 4):
        pass_wait(rel)
        add_squares(other, rel)

    row_scale = lax.rsqrt(jnp.sum(ssq[...], axis=1, keepdims=True) / WIDTH + EPS)
    loads[2].wait()
    loads[3].wait()
    acts = jnp.zeros((ROWS, 256), F32)
    for j in range(NTP):
        cols = slice(j * PART, (j + 1) * PART)
        n = (gathered[j % 2, j // 2].astype(F32) * row_scale * gain[:, cols]).astype(BF16)
        acts = acts + nt_dot(n, w_gu[:, :, cols].reshape(256, PART))
    hidden = silu(acts[:, 0:128]) * acts[:, 128:256]
    row = lax.broadcasted_iota(jnp.int32, (ROWS, 128), 0)
    col = lax.broadcasted_iota(jnp.int32, (ROWS, 128), 1)
    hidden = jnp.where((row // 2) % 2 == col // 64, hidden, 0.0).astype(BF16)
    h_own[...] = hidden
    h_copy = rcopy(h_own, h_par, h_ssem, h_rsem, partner)
    h_copy.start()
    for load in loads[12:]:
        load.wait()
    for copy in wparts[NY:]:
        copy.wait_recv()
    h_copy.wait_recv()

    diagonal = row == col

    def partial(rel):
        k = ys[rel]
        return jnp.dot(
            h_own[...], wd_own[k].reshape(128, PART), preferred_element_type=F32
        ) + jnp.dot(h_par[...], wd_par[k].reshape(128, PART), preferred_element_type=F32)

    def pack(value, slot):
        most = jnp.maximum(jnp.max(jnp.abs(value), axis=1, keepdims=True), 1e-30)
        q_out[slot] = jnp.round(value * (32767.0 / most)).astype(jnp.int16)
        s_out[slot] = jnp.sum(
            jnp.where(diagonal, most * (1.0 / 32767.0), 0.0), axis=0, keepdims=True
        )

    def unpack(slot, sslot):
        unit = jnp.sum(jnp.where(diagonal, s_in[sslot], 0.0), axis=1, keepdims=True)
        return q_in[slot].astype(F32) * unit

    qsends = []

    def q_send(slot, rows, sem, step):
        device = ydev(step)
        copy = rcopy(
            q_out.at[slot, rows], q_in.at[slot, rows], q_ssem.at[sem], q_rsem.at[sem], device
        )
        copy.start()
        qsends.append(copy)
        copy = rcopy(s_out.at[slot], s_in.at[sem], sc_ssem.at[sem], sc_rsem.at[sem], device)
        copy.start()
        qsends.append(copy)

    def q_wait(slot, rows, sem):
        rcopy(
            q_out.at[slot, rows], q_in.at[slot, rows], q_ssem.at[sem], q_rsem.at[sem], partner
        ).wait_recv()
        rcopy(s_out.at[slot], s_in.at[sem], sc_ssem.at[sem], sc_rsem.at[sem], partner).wait_recv()

    pack(partial(4), 2)
    q_send(2, low, 2, 2)
    q_send(2, high, 7, -2)
    pack(partial(3), 0)
    q_send(0, whole, 0, 1)
    pack(partial(5), 1)
    q_send(1, whole, 1, -1)
    pack(partial(1), 3)
    q_send(3, whole, 3, 1)
    pack(partial(7), 4)
    q_send(4, whole, 4, -1)
    kept[0] = partial(2)
    kept[1] = partial(6)
    kept[2] = partial(0)
    dense_step = rcopy(
        dense_out.at[pl.ds(0, NY - 1)],
        dense_in.at[pl.ds(0, NY - 1)],
        dense_ssem,
        dense_rsem,
        partner,
    )
    dense_step.wait_recv()
    dense = dense_in[0]
    for k in range(1, NY):
        dense = dense + dense_in[k]
    gate = gate_ref[...]
    dense = jnp.concatenate([gate, gate], axis=1) * dense
    q_wait(0, whole, 0)
    q_wait(2, low, 2)
    total = kept[0] + unpack(0, 0)
    far = jnp.where(lax.broadcasted_iota(jnp.int32, (ROWS, PART), 0) < ROWS // 2, 1.0, 0.0)
    q_wait(2, high, 7)
    q_wait(1, whole, 1)
    pack(total + unpack(2, 2) * far, 5)
    q_send(5, whole, 5, 2)
    pack(kept[1] + unpack(1, 1) + unpack(2, 7) * (1.0 - far), 6)
    q_send(6, whole, 6, -2)
    q_wait(3, whole, 3)
    q_wait(4, whole, 4)
    kept[2] += unpack(3, 3) + unpack(4, 4)
    q_wait(5, whole, 5)
    q_wait(6, whole, 6)
    summed = kept[2] + unpack(5, 5) + unpack(6, 6)

    left = summed[:, 0:128].reshape(16, 8, 128)
    right = summed[:, 128:256].reshape(16, 8, 128)
    even = jnp.where(sub3 < 4, left, pltpu.roll(right, 4, 1))
    odd = jnp.where(sub3 < 4, pltpu.roll(left, 4, 1), right)
    ret_out[...] = jnp.stack([even, odd], axis=1).reshape(NEP, 8, 128)
    for peer in peers:
        rcopy(ret_out.at[peer], ret_in.at[me_e], ret_ssem, ret_rsem, (peer, me_t)).start()
    ret_in[me_e] = ret_out[me_e]
    rcopy(
        ret_out.at[pl.ds(0, NEP - 1)],
        ret_in.at[pl.ds(0, NEP - 1)],
        ret_ssem,
        ret_rsem,
        partner,
    ).wait_recv()
    mixed = jnp.dot(
        comb[...],
        ret_in[...].reshape(256, 128),
        preferred_element_type=F32,
        precision=lax.Precision.HIGHEST,
    )
    combined = jnp.concatenate([mixed[0:8], mixed[8:16]], axis=1) + dense
    token_diagonal = (
        lax.broadcasted_iota(jnp.int32, (8, 128), 0)
        == lax.broadcasted_iota(jnp.int32, (8, 128), 1)
    )
    own = jnp.sum(
        jnp.where(token_diagonal, jnp.sum(combined * combined, axis=1, keepdims=True), 0.0),
        axis=0,
        keepdims=True,
    )
    sq_out[...] = own
    for step in y_order:
        for c in range(2):
            rcopy(sq_out, sq_in.at[me_t], sq_ssem, sq_rsem, (me_e, ys[step] * 2 + c)).start()
    rcopy(sq_out, sq_in.at[me_t], sq_ssem, sq_rsem, partner).start()
    sq_in[me_t] = own
    sq_step = rcopy(
        sq_in.at[pl.ds(0, NTP - 1)], sq_in.at[pl.ds(0, NTP - 1)], sq_ssem, sq_rsem, partner
    )
    sq_step.wait_recv()
    total_sq = sq_in[0]
    for j in range(1, NTP):
        total_sq = total_sq + sq_in[j]
    final = lax.rsqrt(
        jnp.sum(jnp.where(token_diagonal, total_sq, 0.0), axis=1, keepdims=True) / WIDTH + EPS
    )
    out[...] = (combined * final * ogain[...]).astype(BF16)

    for copy in wparts + sends + passes + [tok_pass, dh_copy, h_copy] + qsends:
        copy.wait_send()
    tok_step.wait_send()
    dense_step.wait_send()
    sq_step.wait_send()
    for ref, ssem, rsem in ((a2a_out, a2a_ssem, a2a_rsem), (ret_out, ret_ssem, ret_rsem)):
        part = ref.at[pl.ds(0, NEP - 1)]
        rcopy(part, part, ssem, rsem, partner).wait_send()


def local(
    tokens,
    norm_gain,
    route_experts,
    route_logits,
    expert_gate,
    expert_up,
    expert_down,
    dense_gate,
    dense_up,
    dense_down,
    mix_weight,
    out_gain,
):
    vmem = pl.BlockSpec(memory_space=pltpu.VMEM)
    dma = pltpu.SemaphoreType.DMA
    return pl.pallas_call(
        kernel,
        out_shape=jax.ShapeDtypeStruct((8, PART), BF16),
        in_specs=[pl.BlockSpec(memory_space=pl.ANY)] * 12,
        out_specs=vmem,
        scratch_shapes=[
            pltpu.VMEM((8, PART), BF16),
            pltpu.VMEM((1, WIDTH), F32),
            pltpu.SMEM((2, 8), jnp.int32),
            pltpu.SMEM((2, 8), F32),
            pltpu.VMEM((1, WIDTH), F32),
            pltpu.VMEM((1, PART), F32),
            pltpu.VMEM((4, 64, WIDTH), BF16),
            pltpu.VMEM((NY, 2, 64, PART), BF16),
            pltpu.VMEM((NY, 2, 64, PART), BF16),
            pltpu.VMEM((128, WIDTH), BF16),
            pltpu.VMEM((NY, 64, PART), BF16),
            pltpu.VMEM((NY, 64, PART), BF16),
            pltpu.VMEM((NEP, 8, 128), BF16),
            pltpu.VMEM((NEP, 8, 128), BF16),
            pltpu.VMEM((2, NY, ROWS, PART), BF16),
            pltpu.VMEM((2, NY, 8, PART), BF16),
            pltpu.VMEM((NY, 8, PART), F32),
            pltpu.VMEM((NY, 8, PART), F32),
            pltpu.VMEM((8, 64), BF16),
            pltpu.VMEM((8, 64), BF16),
            pltpu.VMEM((16, 256), F32),
            pltpu.VMEM((ROWS, 128), BF16),
            pltpu.VMEM((ROWS, 128), BF16),
            pltpu.VMEM((7, ROWS, PART), jnp.int16),
            pltpu.VMEM((7, ROWS, PART), jnp.int16),
            pltpu.VMEM((7, 1, 128), F32),
            pltpu.VMEM((8, 1, 128), F32),
            pltpu.VMEM((3, ROWS, PART), F32),
            pltpu.VMEM((NEP, 8, 128), F32),
            pltpu.VMEM((NEP, 8, 128), F32),
            pltpu.VMEM((1, 128), F32),
            pltpu.VMEM((NTP, 1, 128), F32),
            pltpu.VMEM((ROWS, 128), F32),
            pltpu.VMEM((8, 128), F32),
            dma((6,)),
            dma((20,)),
            dma((2 * NY,)),
            dma((2 * NY,)),
            dma,
            dma,
            dma,
            dma,
            dma,
            dma,
            dma,
            dma,
            dma,
            dma,
            dma((14,)),
            dma((16,)),
            dma((8,)),
            dma((8,)),
            dma,
            dma,
            dma((8,)),
            dma((8,)),
            dma((8,)),
            dma((8,)),
            dma,
            dma,
            dma,
            dma,
        ],
        compiler_params=pltpu.CompilerParams(collective_id=0, has_side_effects=True),
    )(
        tokens,
        norm_gain.reshape(1, WIDTH),
        route_experts.T,
        route_logits.T,
        jnp.swapaxes(expert_gate, 1, 2),
        jnp.swapaxes(expert_up, 1, 2),
        expert_down,
        dense_gate.T,
        dense_up.T,
        dense_down,
        mix_weight.reshape(1, WIDTH),
        out_gain.reshape(1, PART),
    )


def solution(mesh):
    tp = "tp"
    in_specs = (
        P("ep", tp),
        P(),
        P("ep", None),
        P("ep", None),
        P("ep", None, tp),
        P("ep", None, tp),
        P("ep", tp, None),
        P(None, tp),
        P(None, tp),
        P(tp, None),
        P(),
        P(tp),
    )
    return jax.shard_map(
        local, mesh=mesh, in_specs=in_specs, out_specs=P("ep", tp), check_vma=False
    )
```

time: 66.1 us -> 60.5 us (0.915)
  Pallas kernels: 64.6 us -> 59.1 us
    pallas_call x1, Pallas kernels: 64.6 us -> 59.1 us  [local(): pl.pallas_call(kernel, out_shape=jax.ShapeDtypeStruct((8, PART), BF16), i...]
where the time goes in v2:
time: 60.5 us; the launch traced here: 60.4 us
  Pallas kernels  59.1 us (98%)
  local copies, waits for them, and re-layouts  1.28 us (2%)
    pallas_call x1, Pallas kernels, local(): pl.pallas_call(kernel, out_shape=jax.ShapeDtypeStruct((8, PART), BF16), i...  59.1 us
    unnamed x1, local copies, waits for them, and re-layouts  1.28 us

profile of v2, /device:TPU:1, one launch (start us, length us, event | category | flops | bytes accessed | tf_op | source)
XLA Modules:
  0.0 60.4 jit_solution(6715541730469387303)
XLA Ops:
  0.0 59.1 %shard_map.118 = bf16[8,256]{1,0:T(8,128)(2,1)} custom-call(bf16[8,256]{1,0:T(8,128)(2,1)} %tok_hbm.1, f32[1,4096]{1,0:T(1,128)} %bitcast.13, s32[2,8]{1,0:T(2,128)} %bitcast.15, f32[2,8]{1,0:T(2,128)} %bitcast.16, bf16[2,64,4096]{2,1,0:T(8,128)(2,1)} %bitcast.9, bf16[2,64,4096]{2,1,0:T(8,128)(2,1)} %bitcast.10, bf16[2,64,4096]{2,1,0:T(8,128)(2,1)} %wd.1, ...), custom_call_target="tpu_custom_call" | custom-call | tf_op jit(solution)/shard_map/pallas_call | solution.py:551
  59.1 1.3 %copy.14 = bf16[8,256]{1,0:T(8,128)(2,1)} copy(bf16[8,256]{1,0:T(8,128)(2,1)} %shard_map.118) | data formatting | bytes 8192

commit v3 on v2

--- a/solution.py
+++ b/solution.py
@@ -16,6 +16,7 @@
 NEP = NX * NZ
 NTP = 2 * NY
 ROWS = 128
+HALF = ROWS // 2
 PART = 256
 WIDTH = 4096
 
@@ -60,8 +61,7 @@
     mixw,
     ogain,
     w_gu,
-    wd_own,
-    wd_par,
+    wd_all,
     w_dense,
     dd_own,
     dd_par,
@@ -74,8 +74,11 @@
     dh_own,
     dh_par,
     comb,
-    h_own,
-    h_par,
+    slots,
+    r_out,
+    r_in,
+    acts,
+    hid,
     q_out,
     q_in,
     s_out,
@@ -85,7 +88,6 @@
     ret_in,
     sq_out,
     sq_in,
-    ssq,
     gate_ref,
     i_sem,
     w_sem,
@@ -105,8 +107,8 @@
     ag_rsem,
     pf_ssem,
     pf_rsem,
-    h_ssem,
-    h_rsem,
+    r_ssem,
+    r_rsem,
     q_ssem,
     q_rsem,
     sc_ssem,
@@ -152,8 +154,8 @@
     loads = [
         pltpu.make_async_copy(dg, w_dense.at[pl.ds(0, 64)], w_sem.at[0]),
         pltpu.make_async_copy(du, w_dense.at[pl.ds(64, 64)], w_sem.at[1]),
-        pltpu.make_async_copy(wg, w_gu.at[pl.ds(0, 2)], w_sem.at[2]),
-        pltpu.make_async_copy(wu, w_gu.at[pl.ds(2, 2)], w_sem.at[3]),
+        pltpu.make_async_copy(wg, w_gu.at[0, pl.ds(0, 2)], w_sem.at[2]),
+        pltpu.make_async_copy(wu, w_gu.at[0, pl.ds(2, 2)], w_sem.at[3]),
     ]
 
     def columns(k, c):
@@ -165,7 +167,7 @@
         )
     for k in range(NY):
         loads.append(
-            pltpu.make_async_copy(wd.at[:, :, columns(k, core)], wd_own.at[k], w_sem.at[12 + k])
+            pltpu.make_async_copy(wd.at[:, :, columns(k, core)], wd_all.at[k, 0], w_sem.at[12 + k])
         )
     for load in smalls + loads:
         load.start()
@@ -196,6 +198,7 @@
     weight = (jnp.where(is0, e0, 0.0) + jnp.where(is1, e1, 0.0)) / (e0 + e1) * placed
     comb[0:8, :] = jnp.where(half == 0, weight, 0.0)
     comb[8:16, :] = jnp.where(half == 1, weight, 0.0)
+    slots[...] = placed
     place = jnp.concatenate(
         [jnp.where(half == 0, placed, 0.0), jnp.where(half == 1, placed, 0.0)], axis=0
     ).astype(BF16)
@@ -229,9 +232,19 @@
     for k in range(NY):
         copy = rcopy(
             wd.at[:, :, columns(k, other)],
-            wd_par.at[k],
+            wd_all.at[k, 1],
             wp_ssem.at[NY + k],
             wp_rsem.at[NY + k],
+            partner,
+        )
+        copy.start()
+        wparts.append(copy)
+    for k, ref in enumerate((wg, wu)):
+        copy = rcopy(
+            ref,
+            w_gu.at[1, pl.ds(2 * k, 2)],
+            wp_ssem.at[2 * NY + k],
+            wp_rsem.at[2 * NY + k],
             partner,
         )
         copy.start()
@@ -277,11 +290,6 @@
         ref = gathered.at[other, ys[rel]]
         rcopy(ref, ref, pf_ssem.at[rel], pf_rsem.at[rel], partner).wait_recv()
 
-    def add_squares(c, rel):
-        v = gathered[c, ys[rel]].astype(F32)
-        v = v * v
-        ssq[...] += v[:, 0:128] + v[:, 128:256]
-
     ag_send(0, low, 12, 2)
     ag_send(0, low, 4, -2)
     ag_send(0, high, 13, 2)
@@ -289,7 +297,6 @@
     ag_send(0, whole, 14, 1)
     ag_send(0, whole, 2, -1)
     pass_on(0)
-    ssq[...] = left * left + right * right
 
     tok_step = rcopy(
         tok_all.at[0, pl.ds(0, NY - 1)], tok_all.at[0, pl.ds(0, NY - 1)], tok_ssem, tok_rsem, partner
@@ -306,6 +313,10 @@
         v = tok_all[j % 2, j // 2].astype(F32)
         squares = squares + v * v
     scale = lax.rsqrt(jnp.sum(squares, axis=1, keepdims=True) / WIDTH + EPS)
+    r_out[...] = jnp.sum(slots[...] * scale, axis=0, keepdims=True)
+    for peer in peers:
+        rcopy(r_out, r_in.at[me_e], r_ssem, r_rsem, (peer, me_t)).start()
+    r_in[me_e] = r_out[...]
     act = jnp.zeros((8, 128), F32)
     mix_acc = jnp.zeros((8, PART), F32)
     for j in range(NTP):
@@ -342,104 +353,125 @@
             dh_own[...], dd_own[k], preferred_element_type=F32
         ) + jnp.dot(dh_par[...], dd_par[k], preferred_element_type=F32)
     dense_in[y] = dense_out[y]
-    add_squares(core, 6)
-    add_squares(core, 2)
     for rel in (7, 1):
         ag_wait(rel, whole, 2 * rel)
         pass_on(rel)
-    for rel in (7, 1):
-        add_squares(core, rel)
     for step in y_order:
         rcopy(
             dense_out.at[ys[step]], dense_in.at[y], dense_ssem, dense_rsem, ydev(step)
         ).start()
+    loads[2].wait()
+    loads[3].wait()
+    for copy in wparts[2 * NY :]:
+        copy.wait_recv()
+    rcopy(
+        r_in.at[pl.ds(0, NEP - 1)], r_in.at[pl.ds(0, NEP - 1)], r_ssem, r_rsem, partner
+    ).wait_recv()
+    picked = (
+        lax.broadcasted_iota(jnp.int32, (ROWS, NEP), 0) // 4
+        == lax.broadcasted_iota(jnp.int32, (ROWS, NEP), 1)
+    )
+    spread = jnp.dot(
+        jnp.where(picked, 1.0, 0.0),
+        r_in[...].reshape(NEP, 256),
+        preferred_element_type=F32,
+        precision=lax.Precision.HIGHEST,
+    )
+    wanted = me_e * 8 + lax.broadcasted_iota(jnp.int32, (ROWS, 256), 0) % 4
+    here = lax.broadcasted_iota(jnp.int32, (ROWS, 256), 1) == wanted
+    row_scale = jnp.sum(jnp.where(here, spread, 0.0), axis=1, keepdims=True)
+
+    def project(c, rel, first=False):
+        cols = pl.ds(pl.multiple_of((2 * ys[rel] + c) * PART, PART), PART)
+        n = (gathered[c, ys[rel]].astype(F32) * row_scale * gain[:, cols]).astype(BF16)
+        for k in range(2):
+            v = nt_dot(n, w_gu[k, :, :, cols].reshape(256, PART))
+            acts[k] = v if first else acts[k] + v
+
+    project(core, 0, True)
+    for rel in (6, 2, 7, 1):
+        project(core, rel)
+    for rel in (0, 6, 2, 7, 1):
+        pass_wait(rel)
+        project(other, rel)
     for rel in (5, 3):
         ag_wait(rel, low, 2 * rel)
         ag_wait(rel, high, 2 * rel + 1)
         pass_on(rel)
-    for rel in (0, 6, 2, 7, 1):
-        pass_wait(rel)
-        add_squares(other, rel)
-    for rel in (5, 3):
-        add_squares(core, rel)
     ag_wait(4, low, 8)
     ag_wait(4, high, 9)
     pass_on(4)
-    add_squares(core, 4)
+    for rel in (5, 3, 4):
+        project(core, rel)
     for rel in (5, 3, 4):
         pass_wait(rel)
-        add_squares(other, rel)
-
-    row_scale = lax.rsqrt(jnp.sum(ssq[...], axis=1, keepdims=True) / WIDTH + EPS)
-    loads[2].wait()
-    loads[3].wait()
-    acts = jnp.zeros((ROWS, 256), F32)
-    for j in range(NTP):
-        cols = slice(j * PART, (j + 1) * PART)
-        n = (gathered[j % 2, j // 2].astype(F32) * row_scale * gain[:, cols]).astype(BF16)
-        acts = acts + nt_dot(n, w_gu[:, :, cols].reshape(256, PART))
-    hidden = silu(acts[:, 0:128]) * acts[:, 128:256]
+        project(other, rel)
+
     row = lax.broadcasted_iota(jnp.int32, (ROWS, 128), 0)
     col = lax.broadcasted_iota(jnp.int32, (ROWS, 128), 1)
-    hidden = jnp.where((row // 2) % 2 == col // 64, hidden, 0.0).astype(BF16)
-    h_own[...] = hidden
-    h_copy = rcopy(h_own, h_par, h_ssem, h_rsem, partner)
-    h_copy.start()
+    mine = (row // 2) % 2 == col // 64
+    for k in range(2):
+        v = acts[k]
+        hidden = silu(v[:, 0:128]) * v[:, 128:256]
+        hid[:, k * 128 : (k + 1) * 128] = jnp.where(mine, hidden, 0.0).astype(BF16)
     for load in loads[12:]:
         load.wait()
-    for copy in wparts[NY:]:
+    for copy in wparts[NY : 2 * NY]:
         copy.wait_recv()
-    h_copy.wait_recv()
-
-    diagonal = row == col
+
+    diagonal = (
+        lax.broadcasted_iota(jnp.int32, (HALF, 128), 0)
+        == lax.broadcasted_iota(jnp.int32, (HALF, 128), 1)
+    )
 
     def partial(rel):
-        k = ys[rel]
         return jnp.dot(
-            h_own[...], wd_own[k].reshape(128, PART), preferred_element_type=F32
-        ) + jnp.dot(h_par[...], wd_par[k].reshape(128, PART), preferred_element_type=F32)
-
-    def pack(value, slot):
+            hid[...], wd_all[ys[rel]].reshape(256, PART), preferred_element_type=F32
+        )
+
+    def pack(value, slot, h):
         most = jnp.maximum(jnp.max(jnp.abs(value), axis=1, keepdims=True), 1e-30)
-        q_out[slot] = jnp.round(value * (32767.0 / most)).astype(jnp.int16)
-        s_out[slot] = jnp.sum(
+        q_out[slot, h] = jnp.round(value * (32767.0 / most)).astype(jnp.int16)
+        s_out[slot, h] = jnp.sum(
             jnp.where(diagonal, most * (1.0 / 32767.0), 0.0), axis=0, keepdims=True
         )
 
-    def unpack(slot, sslot):
-        unit = jnp.sum(jnp.where(diagonal, s_in[sslot], 0.0), axis=1, keepdims=True)
-        return q_in[slot].astype(F32) * unit
+    def unpack(slot, h):
+        unit = jnp.sum(jnp.where(diagonal, s_in[slot, h], 0.0), axis=1, keepdims=True)
+        return q_in[slot, h].astype(F32) * unit
 
     qsends = []
 
-    def q_send(slot, rows, sem, step):
-        device = ydev(step)
-        copy = rcopy(
-            q_out.at[slot, rows], q_in.at[slot, rows], q_ssem.at[sem], q_rsem.at[sem], device
-        )
-        copy.start()
-        qsends.append(copy)
-        copy = rcopy(s_out.at[slot], s_in.at[sem], sc_ssem.at[sem], sc_rsem.at[sem], device)
-        copy.start()
-        qsends.append(copy)
-
-    def q_wait(slot, rows, sem):
-        rcopy(
-            q_out.at[slot, rows], q_in.at[slot, rows], q_ssem.at[sem], q_rsem.at[sem], partner
-        ).wait_recv()
-        rcopy(s_out.at[slot], s_in.at[sem], sc_ssem.at[sem], sc_rsem.at[sem], partner).wait_recv()
-
-    pack(partial(4), 2)
-    q_send(2, low, 2, 2)
-    q_send(2, high, 7, -2)
-    pack(partial(3), 0)
-    q_send(0, whole, 0, 1)
-    pack(partial(5), 1)
-    q_send(1, whole, 1, -1)
-    pack(partial(1), 3)
-    q_send(3, whole, 3, 1)
-    pack(partial(7), 4)
-    q_send(4, whole, 4, -1)
+    def q_copies(slot, h, device):
+        at = (slot, h)
+        return (
+            rcopy(q_out.at[at], q_in.at[at], q_ssem.at[at], q_rsem.at[at], device),
+            rcopy(s_out.at[at], s_in.at[at], sc_ssem.at[at], sc_rsem.at[at], device),
+        )
+
+    def q_send(value, slot, h, step):
+        pack(value, slot, h)
+        for copy in q_copies(slot, h, ydev(step)):
+            copy.start()
+            qsends.append(copy)
+
+    def q_get(slot, h):
+        for copy in q_copies(slot, h, partner):
+            copy.wait_recv()
+        return unpack(slot, h)
+
+    v = partial(4)
+    q_send(v[:HALF], 2, 0, 2)
+    q_send(v[HALF:], 2, 1, -2)
+    v, w = partial(3), partial(5)
+    q_send(v[:HALF], 0, 0, 1)
+    q_send(w[HALF:], 1, 1, -1)
+    q_send(v[HALF:], 0, 1, 1)
+    q_send(w[:HALF], 1, 0, -1)
+    v, w = partial(1), partial(7)
+    for h in range(2):
+        q_send(v[h * HALF : (h + 1) * HALF], 3, h, 1)
+        q_send(w[h * HALF : (h + 1) * HALF], 4, h, -1)
     kept[0] = partial(2)
     kept[1] = partial(6)
     kept[2] = partial(0)
@@ -456,23 +488,15 @@
         dense = dense + dense_in[k]
     gate = gate_ref[...]
     dense = jnp.concatenate([gate, gate], axis=1) * dense
-    q_wait(0, whole, 0)
-    q_wait(2, low, 2)
-    total = kept[0] + unpack(0, 0)
-    far = jnp.where(lax.broadcasted_iota(jnp.int32, (ROWS, PART), 0) < ROWS // 2, 1.0, 0.0)
-    q_wait(2, high, 7)
-    q_wait(1, whole, 1)
-    pack(total + unpack(2, 2) * far, 5)
-    q_send(5, whole, 5, 2)
-    pack(kept[1] + unpack(1, 1) + unpack(2, 7) * (1.0 - far), 6)
-    q_send(6, whole, 6, -2)
-    q_wait(3, whole, 3)
-    q_wait(4, whole, 4)
-    kept[2] += unpack(3, 3) + unpack(4, 4)
-    q_wait(5, whole, 5)
-    q_wait(6, whole, 6)
-    summed = kept[2] + unpack(5, 5) + unpack(6, 6)
-
+    q_send(kept[0, :HALF] + q_get(2, 0) + q_get(0, 0), 5, 0, 2)
+    q_send(kept[1, HALF:] + q_get(2, 1) + q_get(1, 1), 6, 1, -2)
+    q_send(kept[0, HALF:] + q_get(0, 1), 5, 1, 2)
+    q_send(kept[1, :HALF] + q_get(1, 0), 6, 0, -2)
+    for h in range(2):
+        kept[2, h * HALF : (h + 1) * HALF] += q_get(3, h) + q_get(4, h)
+    summed = kept[2] + jnp.concatenate(
+        [q_get(5, 0) + q_get(6, 0), q_get(6, 1) + q_get(5, 1)], axis=0
+    )
     left = summed[:, 0:128].reshape(16, 8, 128)
     right = summed[:, 128:256].reshape(16, 8, 128)
     even = jnp.where(sub3 < 4, left, pltpu.roll(right, 4, 1))
@@ -522,12 +546,16 @@
     )
     out[...] = (combined * final * ogain[...]).astype(BF16)
 
-    for copy in wparts + sends + passes + [tok_pass, dh_copy, h_copy] + qsends:
+    for copy in wparts + sends + passes + [tok_pass, dh_copy] + qsends:
         copy.wait_send()
     tok_step.wait_send()
     dense_step.wait_send()
     sq_step.wait_send()
-    for ref, ssem, rsem in ((a2a_out, a2a_ssem, a2a_rsem), (ret_out, ret_ssem, ret_rsem)):
+    for ref, ssem, rsem in (
+        (a2a_out, a2a_ssem, a2a_rsem),
+        (r_in, r_ssem, r_rsem),
+        (ret_out, ret_ssem, ret_rsem),
+    ):
         part = ref.at[pl.ds(0, NEP - 1)]
         rcopy(part, part, ssem, rsem, partner).wait_send()
 
@@ -550,7 +578,7 @@
     dma = pltpu.SemaphoreType.DMA
     return pl.pallas_call(
         kernel,
-        out_shape=jax.ShapeDtypeStruct((8, PART), BF16),
+        out_shape=pltpu.VMEM((8, PART), BF16),
         in_specs=[pl.BlockSpec(memory_space=pl.ANY)] * 12,
         out_specs=vmem,
         scratch_shapes=[
@@ -560,9 +588,8 @@
             pltpu.SMEM((2, 8), F32),
             pltpu.VMEM((1, WIDTH), F32),
             pltpu.VMEM((1, PART), F32),
-            pltpu.VMEM((4, 64, WIDTH), BF16),
-            pltpu.VMEM((NY, 2, 64, PART), BF16),
-            pltpu.VMEM((NY, 2, 64, PART), BF16),
+            pltpu.VMEM((2, 4, 64, WIDTH), BF16),
+            pltpu.VMEM((NY, 2, 2, 64, PART), BF16),
             pltpu.VMEM((128, WIDTH), BF16),
             pltpu.VMEM((NY, 64, PART), BF16),
             pltpu.VMEM((NY, 64, PART), BF16),
@@ -575,23 +602,25 @@
             pltpu.VMEM((8, 64), BF16),
             pltpu.VMEM((8, 64), BF16),
             pltpu.VMEM((16, 256), F32),
-            pltpu.VMEM((ROWS, 128), BF16),
-            pltpu.VMEM((ROWS, 128), BF16),
-            pltpu.VMEM((7, ROWS, PART), jnp.int16),
-            pltpu.VMEM((7, ROWS, PART), jnp.int16),
-            pltpu.VMEM((7, 1, 128), F32),
-            pltpu.VMEM((8, 1, 128), F32),
+            pltpu.VMEM((8, 256), F32),
+            pltpu.VMEM((1, 256), F32),
+            pltpu.VMEM((NEP, 1, 256), F32),
+            pltpu.VMEM((2, ROWS, 256), F32),
+            pltpu.VMEM((ROWS, 256), BF16),
+            pltpu.VMEM((7, 2, HALF, PART), jnp.int16),
+            pltpu.VMEM((7, 2, HALF, PART), jnp.int16),
+            pltpu.VMEM((7, 2, 1, 128), F32),
+            pltpu.VMEM((7, 2, 1, 128), F32),
             pltpu.VMEM((3, ROWS, PART), F32),
             pltpu.VMEM((NEP, 8, 128), F32),
             pltpu.VMEM((NEP, 8, 128), F32),
             pltpu.VMEM((1, 128), F32),
             pltpu.VMEM((NTP, 1, 128), F32),
-            pltpu.VMEM((ROWS, 128), F32),
             pltpu.VMEM((8, 128), F32),
             dma((6,)),
             dma((20,)),
-            dma((2 * NY,)),
-            dma((2 * NY,)),
+            dma((2 * NY + 2,)),
+            dma((2 * NY + 2,)),
             dma,
             dma,
             dma,
@@ -608,16 +637,18 @@
             dma((8,)),
             dma,
             dma,
-            dma((8,)),
-            dma((8,)),
-            dma((8,)),
-            dma((8,)),
+            dma((7, 2)),
+            dma((7, 2)),
+            dma((7, 2)),
+            dma((7, 2)),
             dma,
             dma,
             dma,
             dma,
         ],
-        compiler_params=pltpu.CompilerParams(collective_id=0, has_side_effects=True),
+        compiler_params=pltpu.CompilerParams(
+            collective_id=0, has_side_effects=True, vmem_limit_bytes=56650000
+        ),
     )(
         tokens,
         norm_gain.reshape(1, WIDTH),

time: 60.5 us -> 57.9 us (0.957)
  Pallas kernels: 59.1 us -> 57.2 us
  local copies, waits for them, and re-layouts: 1.28 us -> 0.6 us
    pallas_call x1, Pallas kernels: 59.1 us -> 57.2 us  [local(): pl.pallas_call(kernel, out_shape=pltpu.VMEM((8, PART), BF16), in_specs=[p...]
    unnamed x1, local copies, waits for them, and re-layouts: 1.28 us -> 0.6 us
where the time goes in v3:
time: 57.9 us; the launch traced here: 57.8 us
  Pallas kernels  57.2 us (99%)
  local copies, waits for them, and re-layouts  0.6 us (1%)
    pallas_call x1, Pallas kernels, local(): pl.pallas_call(kernel, out_shape=pltpu.VMEM((8, PART), BF16), in_specs=[p...  57.2 us

profile of v3, /device:TPU:1, one launch (start us, length us, event | category | flops | bytes accessed | tf_op | source)
XLA Modules:
  0.0 57.8 jit_solution(490513467325217564)
XLA Ops:
  0.0 57.2 %shard_map.118 = bf16[8,256]{1,0:T(8,128)(2,1)S(1)} custom-call(bf16[8,256]{1,0:T(8,128)(2,1)} %tok_hbm.1, f32[1,4096]{1,0:T(1,128)} %bitcast.13, s32[2,8]{1,0:T(2,128)} %bitcast.15, f32[2,8]{1,0:T(2,128)} %bitcast.16, bf16[2,64,4096]{2,1,0:T(8,128)(2,1)} %bitcast.9, bf16[2,64,4096]{2,1,0:T(8,128)(2,1)} %bitcast.10, bf16[2,64,4096]{2,1,0:T(8,128)(2,1)} %wd.1, ...), custom_call_target="tpu_custom_call" | custom-call | tf_op jit(solution)/shard_map/pallas_call | solution.py:579
  57.2 0.6 %copy.14 = bf16[8,256]{1,0:T(8,128)(2,1)} copy(bf16[8,256]{1,0:T(8,128)(2,1)S(1)} %shard_map.118) | data formatting | bytes 8192

commit v4 on v3

--- a/solution.py
+++ b/solution.py
@@ -16,7 +16,8 @@
 NEP = NX * NZ
 NTP = 2 * NY
 ROWS = 128
-HALF = ROWS // 2
+FAR = (3, 4, 5)
+NEAR = (2, 6, 1, 7)
 PART = 256
 WIDTH = 4096
 
@@ -67,6 +68,8 @@
     dd_par,
     a2a_out,
     a2a_in,
+    far_out,
+    far_in,
     gathered,
     tok_all,
     dense_out,
@@ -74,6 +77,7 @@
     dh_own,
     dh_par,
     comb,
+    place,
     slots,
     r_out,
     r_in,
@@ -83,6 +87,12 @@
     q_in,
     s_out,
     s_in,
+    fq_out,
+    fq_in,
+    fs_out,
+    fs_in,
+    fy_out,
+    fy_in,
     kept,
     ret_out,
     ret_in,
@@ -95,10 +105,10 @@
     wp_rsem,
     a2a_ssem,
     a2a_rsem,
+    far_ssem,
+    far_rsem,
     tok_ssem,
     tok_rsem,
-    tp_ssem,
-    tp_rsem,
     dh_ssem,
     dh_rsem,
     dense_ssem,
@@ -113,6 +123,12 @@
     q_rsem,
     sc_ssem,
     sc_rsem,
+    fq_ssem,
+    fq_rsem,
+    fs_ssem,
+    fs_rsem,
+    fy_ssem,
+    fy_rsem,
     ret_ssem,
     ret_rsem,
     sq_ssem,
@@ -199,28 +215,35 @@
     comb[0:8, :] = jnp.where(half == 0, weight, 0.0)
     comb[8:16, :] = jnp.where(half == 1, weight, 0.0)
     slots[...] = placed
-    place = jnp.concatenate(
+    place[...] = jnp.concatenate(
         [jnp.where(half == 0, placed, 0.0), jnp.where(half == 1, placed, 0.0)], axis=0
     ).astype(BF16)
+
+    def placed_rows(value):
+        halves = jnp.concatenate(
+            [value[:, 0:128].astype(F32), value[:, 128:256].astype(F32)], axis=0
+        ).astype(BF16)
+        rows = lax.dot_general(
+            place[...], halves, (((0,), (0,)), ((), ())), preferred_element_type=F32
+        )
+        return rows.astype(BF16).reshape(NEP, 8, 128)
+
     tok_value = tok[...]
-    halves = jnp.concatenate(
-        [tok_value[:, 0:128].astype(F32), tok_value[:, 128:256].astype(F32)], axis=0
-    ).astype(BF16)
-    a2a_out[...] = (
-        lax.dot_general(place, halves, (((0,), (0,)), ((), ())), preferred_element_type=F32)
-        .astype(BF16)
-        .reshape(NEP, 8, 128)
-    )
+    a2a_out[...] = placed_rows(tok_value)
     a2a_in[me_e] = a2a_out[me_e]
-    tok_all[core, y] = tok_value
+    tok_all[me_t] = tok_value
 
     pl.semaphore_wait(barrier, NEP - 1 + NTP - 1)
+
+    for step in y_order:
+        for c in range(2):
+            rcopy(
+                tok, tok_all.at[me_t], tok_ssem, tok_rsem, (me_e, ys[step] * 2 + c)
+            ).start()
+    rcopy(tok, tok_all.at[me_t], tok_ssem, tok_rsem, partner).start()
 
     for peer in peers:
         rcopy(a2a_out.at[peer], a2a_in.at[me_e], a2a_ssem, a2a_rsem, (peer, me_t)).start()
-
-    for step in y_order:
-        rcopy(tok, tok_all.at[core, y], tok_ssem, tok_rsem, ydev(step)).start()
 
     wparts = []
     for k in range(NY):
@@ -250,78 +273,71 @@
         copy.start()
         wparts.append(copy)
 
-    rcopy(
-        a2a_out.at[pl.ds(0, NEP - 1)],
-        a2a_in.at[pl.ds(0, NEP - 1)],
-        a2a_ssem,
-        a2a_rsem,
-        partner,
-    ).wait_recv()
-    pairs = a2a_in[...].astype(F32).reshape(16, 2, 8, 128)
-    even, odd = pairs[:, 0], pairs[:, 1]
-    sub3 = lax.broadcasted_iota(jnp.int32, (16, 8, 128), 1)
-    left = jnp.where(sub3 < 4, even, pltpu.roll(odd, 4, 1)).reshape(ROWS, 128)
-    right = jnp.where(sub3 < 4, pltpu.roll(even, 4, 1), odd).reshape(ROWS, 128)
-    gathered[core, y, :, 0:128] = left.astype(BF16)
-    gathered[core, y, :, 128:256] = right.astype(BF16)
-
-    sends = []
-    whole, low, high = pl.ds(0, ROWS), pl.ds(0, ROWS // 2), pl.ds(ROWS // 2, ROWS // 2)
-
-    def ag_send(rel, rows, sem, step):
-        ref = gathered.at[core, ys[rel], rows]
-        copy = rcopy(ref, ref, ag_ssem.at[len(sends)], ag_rsem.at[sem], ydev(step))
-        copy.start()
-        sends.append(copy)
-
-    def ag_wait(rel, rows, sem):
-        ref = gathered.at[core, ys[rel], rows]
-        rcopy(ref, ref, ag_ssem.at[0], ag_rsem.at[sem], partner).wait_recv()
-
-    passes = []
-
-    def pass_on(rel):
-        ref = gathered.at[core, ys[rel]]
-        copy = rcopy(ref, ref, pf_ssem.at[rel], pf_rsem.at[rel], partner)
-        copy.start()
-        passes.append(copy)
-
-    def pass_wait(rel):
-        ref = gathered.at[other, ys[rel]]
-        rcopy(ref, ref, pf_ssem.at[rel], pf_rsem.at[rel], partner).wait_recv()
-
-    ag_send(0, low, 12, 2)
-    ag_send(0, low, 4, -2)
-    ag_send(0, high, 13, 2)
-    ag_send(0, high, 5, -2)
-    ag_send(0, whole, 14, 1)
-    ag_send(0, whole, 2, -1)
-    pass_on(0)
-
-    tok_step = rcopy(
-        tok_all.at[0, pl.ds(0, NY - 1)], tok_all.at[0, pl.ds(0, NY - 1)], tok_ssem, tok_rsem, partner
-    )
-    tok_step.wait_recv()
-    tok_pass = rcopy(tok_all.at[core], tok_all.at[core], tp_ssem, tp_rsem, partner)
-    tok_pass.start()
-    for load in smalls[3:6] + loads[0:2]:
-        load.wait()
-    rcopy(tok_all.at[other], tok_all.at[other], tp_ssem, tp_rsem, partner).wait_recv()
-
+    def arrived(src, dst, ssem, rsem, n):
+        part = pl.ds(0, n)
+        copy = rcopy(src.at[part], dst.at[part], ssem, rsem, partner)
+        copy.wait_recv()
+        return copy
+
+    done = [arrived(tok_all, tok_all, tok_ssem, tok_rsem, NTP - 1)]
     squares = jnp.zeros((8, PART), F32)
     for j in range(NTP):
-        v = tok_all[j % 2, j // 2].astype(F32)
+        v = tok_all[j].astype(F32)
         squares = squares + v * v
     scale = lax.rsqrt(jnp.sum(squares, axis=1, keepdims=True) / WIDTH + EPS)
     r_out[...] = jnp.sum(slots[...] * scale, axis=0, keepdims=True)
     for peer in peers:
         rcopy(r_out, r_in.at[me_e], r_ssem, r_rsem, (peer, me_t)).start()
     r_in[me_e] = r_out[...]
+    for i, rel in enumerate(FAR):
+        far_out[:, i] = placed_rows(tok_all[ys[rel] * 2 + core])
+    for peer in peers:
+        rcopy(far_out.at[peer], far_in.at[me_e], far_ssem, far_rsem, (peer, me_t)).start()
+    far_in[me_e] = far_out[me_e]
+
+    done.append(arrived(a2a_out, a2a_in, a2a_ssem, a2a_rsem, NEP - 1))
+    sub3 = lax.broadcasted_iota(jnp.int32, (16, 8, 128), 1)
+
+    def keep_rows(value, rel):
+        pairs = value.astype(F32).reshape(16, 2, 8, 128)
+        even, odd = pairs[:, 0], pairs[:, 1]
+        left = jnp.where(sub3 < 4, even, pltpu.roll(odd, 4, 1)).reshape(ROWS, 128)
+        right = jnp.where(sub3 < 4, pltpu.roll(even, 4, 1), odd).reshape(ROWS, 128)
+        gathered[core, ys[rel], :, 0:128] = left.astype(BF16)
+        gathered[core, ys[rel], :, 128:256] = right.astype(BF16)
+
+    keep_rows(a2a_in[...], 0)
+
+    sends = []
+
+    def ag_copy(slot, k, rel, device):
+        ref = gathered.at[core, ys[slot]]
+        return rcopy(ref, ref, ag_ssem.at[k], ag_rsem.at[rel], device)
+
+    for k, (rel, step) in enumerate(((6, 2), (2, -2), (7, 1), (1, -1))):
+        copy = ag_copy(0, k, rel, ydev(step))
+        copy.start()
+        sends.append(copy)
+
+    def pass_on(rel):
+        ref = gathered.at[core, ys[rel]]
+        copy = rcopy(ref, ref, pf_ssem.at[rel], pf_rsem.at[rel], partner)
+        copy.start()
+        sends.append(copy)
+
+    def pass_wait(rel):
+        ref = gathered.at[other, ys[rel]]
+        rcopy(ref, ref, pf_ssem.at[rel], pf_rsem.at[rel], partner).wait_recv()
+
+    pass_on(0)
+
+    for load in smalls[3:6] + loads[0:2]:
+        load.wait()
     act = jnp.zeros((8, 128), F32)
     mix_acc = jnp.zeros((8, PART), F32)
     for j in range(NTP):
         cols = slice(j * PART, (j + 1) * PART)
-        n = (tok_all[j % 2, j // 2].astype(F32) * scale * gain[:, cols]).astype(BF16)
+        n = (tok_all[j].astype(F32) * scale * gain[:, cols]).astype(BF16)
         mix_acc = mix_acc + n.astype(F32) * mixw[:, cols]
         act = act + nt_dot(n, w_dense[:, cols])
     gate_ref[...] = jnp.broadcast_to(
@@ -331,18 +347,9 @@
     dh_copy = rcopy(dh_own, dh_par, dh_ssem, dh_rsem, partner)
     dh_copy.start()
 
-    ag_wait(6, low, 12)
-    ag_send(6, low, 8, 2)
-    ag_send(6, low, 10, 1)
-    ag_wait(2, low, 4)
-    ag_send(2, low, 6, -1)
-    ag_wait(6, high, 13)
-    ag_send(6, high, 11, 1)
-    ag_wait(2, high, 5)
-    ag_send(2, high, 9, -2)
-    ag_send(2, high, 7, -1)
-    pass_on(6)
-    pass_on(2)
+    for rel in (6, 2):
+        ag_copy(rel, 0, rel, partner).wait_recv()
+        pass_on(rel)
     for load in loads[4:12]:
         load.wait()
     for copy in wparts[0:NY]:
@@ -354,7 +361,7 @@
         ) + jnp.dot(dh_par[...], dd_par[k], preferred_element_type=F32)
     dense_in[y] = dense_out[y]
     for rel in (7, 1):
-        ag_wait(rel, whole, 2 * rel)
+        ag_copy(rel, 0, rel, partner).wait_recv()
         pass_on(rel)
     for step in y_order:
         rcopy(
@@ -364,9 +371,7 @@
     loads[3].wait()
     for copy in wparts[2 * NY :]:
         copy.wait_recv()
-    rcopy(
-        r_in.at[pl.ds(0, NEP - 1)], r_in.at[pl.ds(0, NEP - 1)], r_ssem, r_rsem, partner
-    ).wait_recv()
+    done.append(arrived(r_in, r_in, r_ssem, r_rsem, NEP - 1))
     picked = (
         lax.broadcasted_iota(jnp.int32, (ROWS, NEP), 0) // 4
         == lax.broadcasted_iota(jnp.int32, (ROWS, NEP), 1)
@@ -389,21 +394,18 @@
             acts[k] = v if first else acts[k] + v
 
     project(core, 0, True)
-    for rel in (6, 2, 7, 1):
+    for rel in NEAR:
         project(core, rel)
-    for rel in (0, 6, 2, 7, 1):
+    for rel in (0,) + NEAR:
         pass_wait(rel)
         project(other, rel)
-    for rel in (5, 3):
-        ag_wait(rel, low, 2 * rel)
-        ag_wait(rel, high, 2 * rel + 1)
+    done.append(arrived(far_out, far_in, far_ssem, far_rsem, NEP - 1))
+    for i, rel in enumerate(FAR):
+        keep_rows(far_in[:, i], rel)
         pass_on(rel)
-    ag_wait(4, low, 8)
-    ag_wait(4, high, 9)
-    pass_on(4)
-    for rel in (5, 3, 4):
+    for rel in FAR:
         project(core, rel)
-    for rel in (5, 3, 4):
+    for rel in FAR:
         pass_wait(rel)
         project(other, rel)
 
@@ -419,99 +421,100 @@
     for copy in wparts[NY : 2 * NY]:
         copy.wait_recv()
 
-    diagonal = (
-        lax.broadcasted_iota(jnp.int32, (HALF, 128), 0)
-        == lax.broadcasted_iota(jnp.int32, (HALF, 128), 1)
-    )
+    diagonal = row == col
 
     def partial(rel):
         return jnp.dot(
             hid[...], wd_all[ys[rel]].reshape(256, PART), preferred_element_type=F32
         )
 
-    def pack(value, slot, h):
+    def column(value):
+        return jnp.sum(jnp.where(diagonal, value, 0.0), axis=0, keepdims=True)
+
+    def messages(value):
+        left = value[:, 0:128].reshape(16, 8, 128)
+        right = value[:, 128:256].reshape(16, 8, 128)
+        even = jnp.where(sub3 < 4, left, pltpu.roll(right, 4, 1))
+        odd = jnp.where(sub3 < 4, pltpu.roll(left, 4, 1), right)
+        return jnp.stack([even, odd], axis=1).reshape(NEP, 8, 128)
+
+    def q_copies(k, device):
+        return (
+            rcopy(q_out.at[k], q_in.at[k], q_ssem.at[k], q_rsem.at[k], device),
+            rcopy(s_out.at[k], s_in.at[k], sc_ssem.at[k], sc_rsem.at[k], device),
+        )
+
+    def q_send(k):
+        value = partial(NEAR[k])
         most = jnp.maximum(jnp.max(jnp.abs(value), axis=1, keepdims=True), 1e-30)
-        q_out[slot, h] = jnp.round(value * (32767.0 / most)).astype(jnp.int16)
-        s_out[slot, h] = jnp.sum(
-            jnp.where(diagonal, most * (1.0 / 32767.0), 0.0), axis=0, keepdims=True
-        )
-
-    def unpack(slot, h):
-        unit = jnp.sum(jnp.where(diagonal, s_in[slot, h], 0.0), axis=1, keepdims=True)
-        return q_in[slot, h].astype(F32) * unit
-
-    qsends = []
-
-    def q_copies(slot, h, device):
-        at = (slot, h)
-        return (
-            rcopy(q_out.at[at], q_in.at[at], q_ssem.at[at], q_rsem.at[at], device),
-            rcopy(s_out.at[at], s_in.at[at], sc_ssem.at[at], sc_rsem.at[at], device),
-        )
-
-    def q_send(value, slot, h, step):
-        pack(value, slot, h)
-        for copy in q_copies(slot, h, ydev(step)):
+        q_out[k] = jnp.round(value * (32767.0 / most)).astype(jnp.int16)
+        s_out[k] = column(most * (1.0 / 32767.0))
+        for copy in q_copies(k, ydev(NEAR[k])):
             copy.start()
-            qsends.append(copy)
-
-    def q_get(slot, h):
-        for copy in q_copies(slot, h, partner):
+            sends.append(copy)
+
+    def q_get(k):
+        for copy in q_copies(k, partner):
             copy.wait_recv()
-        return unpack(slot, h)
-
-    v = partial(4)
-    q_send(v[:HALF], 2, 0, 2)
-    q_send(v[HALF:], 2, 1, -2)
-    v, w = partial(3), partial(5)
-    q_send(v[:HALF], 0, 0, 1)
-    q_send(w[HALF:], 1, 1, -1)
-    q_send(v[HALF:], 0, 1, 1)
-    q_send(w[:HALF], 1, 0, -1)
-    v, w = partial(1), partial(7)
-    for h in range(2):
-        q_send(v[h * HALF : (h + 1) * HALF], 3, h, 1)
-        q_send(w[h * HALF : (h + 1) * HALF], 4, h, -1)
-    kept[0] = partial(2)
-    kept[1] = partial(6)
-    kept[2] = partial(0)
-    dense_step = rcopy(
-        dense_out.at[pl.ds(0, NY - 1)],
-        dense_in.at[pl.ds(0, NY - 1)],
-        dense_ssem,
-        dense_rsem,
-        partner,
-    )
-    dense_step.wait_recv()
+        unit = jnp.sum(jnp.where(diagonal, s_in[k], 0.0), axis=1, keepdims=True)
+        return q_in[k].astype(F32) * unit
+
+    values = [partial(rel) for rel in FAR]
+    most = jnp.maximum(jnp.maximum(jnp.abs(values[0]), jnp.abs(values[1])), jnp.abs(values[2]))
+    most = jnp.maximum(jnp.max(most, axis=1, keepdims=True), 1e-30)
+    fs_out[...] = column(most * (1.0 / 32767.0))
+    for i in range(3):
+        fq_out[:, i] = messages(jnp.round(values[i] * (32767.0 / most))).astype(jnp.int16)
+    for peer in peers:
+        rcopy(fq_out.at[peer], fq_in.at[me_e], fq_ssem, fq_rsem, (peer, me_t)).start()
+        rcopy(fs_out, fs_in.at[me_e], fs_ssem, fs_rsem, (peer, me_t)).start()
+    for k in range(4):
+        q_send(k)
+    fq_in[me_e] = fq_out[me_e]
+    fs_in[me_e] = fs_out[...]
+    kept[...] = partial(0)
+    done.append(arrived(dense_out, dense_in, dense_ssem, dense_rsem, NY - 1))
     dense = dense_in[0]
     for k in range(1, NY):
         dense = dense + dense_in[k]
     gate = gate_ref[...]
     dense = jnp.concatenate([gate, gate], axis=1) * dense
-    q_send(kept[0, :HALF] + q_get(2, 0) + q_get(0, 0), 5, 0, 2)
-    q_send(kept[1, HALF:] + q_get(2, 1) + q_get(1, 1), 6, 1, -2)
-    q_send(kept[0, HALF:] + q_get(0, 1), 5, 1, 2)
-    q_send(kept[1, :HALF] + q_get(1, 0), 6, 0, -2)
-    for h in range(2):
-        kept[2, h * HALF : (h + 1) * HALF] += q_get(3, h) + q_get(4, h)
-    summed = kept[2] + jnp.concatenate(
-        [q_get(5, 0) + q_get(6, 0), q_get(6, 1) + q_get(5, 1)], axis=0
-    )
-    left = summed[:, 0:128].reshape(16, 8, 128)
-    right = summed[:, 128:256].reshape(16, 8, 128)
-    even = jnp.where(sub3 < 4, left, pltpu.roll(right, 4, 1))
-    odd = jnp.where(sub3 < 4, pltpu.roll(left, 4, 1), right)
-    ret_out[...] = jnp.stack([even, odd], axis=1).reshape(NEP, 8, 128)
+    summed = kept[...]
+    for k in (2, 3, 0, 1):
+        summed = summed + q_get(k)
+    ret_out[...] = messages(summed)
     for peer in peers:
         rcopy(ret_out.at[peer], ret_in.at[me_e], ret_ssem, ret_rsem, (peer, me_t)).start()
     ret_in[me_e] = ret_out[me_e]
-    rcopy(
-        ret_out.at[pl.ds(0, NEP - 1)],
-        ret_in.at[pl.ds(0, NEP - 1)],
-        ret_ssem,
-        ret_rsem,
-        partner,
-    ).wait_recv()
+    done.append(arrived(fq_out, fq_in, fq_ssem, fq_rsem, NEP - 1))
+    done.append(arrived(fs_in, fs_in, fs_ssem, fs_rsem, NEP - 1))
+    lane2 = lax.broadcasted_iota(jnp.int32, (128, 256), 1)
+    mine4 = lax.broadcasted_iota(jnp.int32, (128, 256), 0) == me_e * 4 + lane2 % 4
+    unit = jnp.dot(
+        fs_in[...].reshape(NEP, 128),
+        jnp.where(mine4, 1.0, 0.0),
+        preferred_element_type=F32,
+        precision=lax.Precision.HIGHEST,
+    )
+    source = lax.broadcasted_iota(jnp.int32, (NEP, 256), 0)
+    source = source == lax.broadcasted_iota(jnp.int32, (NEP, 256), 1) // 8
+    unit = jnp.sum(jnp.where(source, unit, 0.0), axis=0, keepdims=True)
+    far_sum = jnp.dot(
+        comb[...] * unit,
+        jnp.concatenate(
+            [fq_in[:, i].astype(F32).reshape(256, 128) for i in range(3)], axis=1
+        ),
+        preferred_element_type=F32,
+        precision=lax.Precision.HIGHEST,
+    )
+    for i, rel in enumerate(FAR):
+        cols = slice(i * 128, (i + 1) * 128)
+        fy_out[i, :, 0:128] = far_sum[0:8, cols]
+        fy_out[i, :, 128:256] = far_sum[8:16, cols]
+        copy = rcopy(fy_out.at[i], fy_in.at[i], fy_ssem.at[i], fy_rsem.at[i], ydev(rel))
+        copy.start()
+        sends.append(copy)
+    done.append(arrived(ret_out, ret_in, ret_ssem, ret_rsem, NEP - 1))
     mixed = jnp.dot(
         comb[...],
         ret_in[...].reshape(256, 128),
@@ -519,6 +522,9 @@
         precision=lax.Precision.HIGHEST,
     )
     combined = jnp.concatenate([mixed[0:8], mixed[8:16]], axis=1) + dense
+    for i in range(3):
+        rcopy(fy_out.at[i], fy_in.at[i], fy_ssem.at[i], fy_rsem.at[i], partner).wait_recv()
+        combined = combined + fy_in[i]
     token_diagonal = (
         lax.broadcasted_iota(jnp.int32, (8, 128), 0)
         == lax.broadcasted_iota(jnp.int32, (8, 128), 1)
@@ -534,10 +540,7 @@
             rcopy(sq_out, sq_in.at[me_t], sq_ssem, sq_rsem, (me_e, ys[step] * 2 + c)).start()
     rcopy(sq_out, sq_in.at[me_t], sq_ssem, sq_rsem, partner).start()
     sq_in[me_t] = own
-    sq_step = rcopy(
-        sq_in.at[pl.ds(0, NTP - 1)], sq_in.at[pl.ds(0, NTP - 1)], sq_ssem, sq_rsem, partner
-    )
-    sq_step.wait_recv()
+    done.append(arrived(sq_in, sq_in, sq_ssem, sq_rsem, NTP - 1))
     total_sq = sq_in[0]
     for j in range(1, NTP):
         total_sq = total_sq + sq_in[j]
@@ -546,18 +549,8 @@
     )
     out[...] = (combined * final * ogain[...]).astype(BF16)
 
-    for copy in wparts + sends + passes + [tok_pass, dh_copy] + qsends:
+    for copy in wparts + sends + [dh_copy] + done:
         copy.wait_send()
-    tok_step.wait_send()
-    dense_step.wait_send()
-    sq_step.wait_send()
-    for ref, ssem, rsem in (
-        (a2a_out, a2a_ssem, a2a_rsem),
-        (r_in, r_ssem, r_rsem),
-        (ret_out, ret_ssem, ret_rsem),
-    ):
-        part = ref.at[pl.ds(0, NEP - 1)]
-        rcopy(part, part, ssem, rsem, partner).wait_send()
 
 
 def local(
@@ -595,23 +588,32 @@
             pltpu.VMEM((NY, 64, PART), BF16),
             pltpu.VMEM((NEP, 8, 128), BF16),
             pltpu.VMEM((NEP, 8, 128), BF16),
+            pltpu.VMEM((NEP, 3, 8, 128), BF16),
+            pltpu.VMEM((NEP, 3, 8, 128), BF16),
             pltpu.VMEM((2, NY, ROWS, PART), BF16),
-            pltpu.VMEM((2, NY, 8, PART), BF16),
+            pltpu.VMEM((NTP, 8, PART), BF16),
             pltpu.VMEM((NY, 8, PART), F32),
             pltpu.VMEM((NY, 8, PART), F32),
             pltpu.VMEM((8, 64), BF16),
             pltpu.VMEM((8, 64), BF16),
             pltpu.VMEM((16, 256), F32),
+            pltpu.VMEM((16, 256), BF16),
             pltpu.VMEM((8, 256), F32),
             pltpu.VMEM((1, 256), F32),
             pltpu.VMEM((NEP, 1, 256), F32),
             pltpu.VMEM((2, ROWS, 256), F32),
             pltpu.VMEM((ROWS, 256), BF16),
-            pltpu.VMEM((7, 2, HALF, PART), jnp.int16),
-            pltpu.VMEM((7, 2, HALF, PART), jnp.int16),
-            pltpu.VMEM((7, 2, 1, 128), F32),
-            pltpu.VMEM((7, 2, 1, 128), F32),
-            pltpu.VMEM((3, ROWS, PART), F32),
+            pltpu.VMEM((4, ROWS, PART), jnp.int16),
+            pltpu.VMEM((4, ROWS, PART), jnp.int16),
+            pltpu.VMEM((4, 1, 128), F32),
+            pltpu.VMEM((4, 1, 128), F32),
+            pltpu.VMEM((NEP, 3, 8, 128), jnp.int16),
+            pltpu.VMEM((NEP, 3, 8, 128), jnp.int16),
+            pltpu.VMEM((1, 128), F32),
+            pltpu.VMEM((NEP, 1, 128), F32),
+            pltpu.VMEM((3, 8, PART), F32),
+            pltpu.VMEM((3, 8, PART), F32),
+            pltpu.VMEM((ROWS, PART), F32),
             pltpu.VMEM((NEP, 8, 128), F32),
             pltpu.VMEM((NEP, 8, 128), F32),
             pltpu.VMEM((1, 128), F32),
@@ -631,16 +633,22 @@
             dma,
             dma,
             dma,
-            dma((14,)),
-            dma((16,)),
+            dma((4,)),
             dma((8,)),
             dma((8,)),
-            dma,
-            dma,
-            dma((7, 2)),
-            dma((7, 2)),
-            dma((7, 2)),
-            dma((7, 2)),
+            dma((8,)),
+            dma,
+            dma,
+            dma((4,)),
+            dma((4,)),
+            dma((4,)),
+            dma((4,)),
+            dma,
+            dma,
+            dma,
+            dma,
+            dma((3,)),
+            dma((3,)),
             dma,
             dma,
             dma,

time: 57.9 us -> 54.2 us (0.936)
  Pallas kernels: 57.2 us -> 53.5 us
    pallas_call x1, Pallas kernels: 57.2 us -> 53.5 us  [local(): pl.pallas_call(kernel, out_shape=pltpu.VMEM((8, PART), BF16), in_specs=[p...]
where the time goes in v4:
time: 54.2 us; the launch traced here: 54.1 us
  Pallas kernels  53.5 us (99%)
  local copies, waits for them, and re-layouts  0.6 us (1%)
    pallas_call x1, Pallas kernels, local(): pl.pallas_call(kernel, out_shape=pltpu.VMEM((8, PART), BF16), in_specs=[p...  53.5 us

profile of v4, /device:TPU:1, one launch (start us, length us, event | category | flops | bytes accessed | tf_op | source)
XLA Modules:
  0.0 54.1 jit_solution(4261828409214847314)
XLA Ops:
  0.0 53.5 %shard_map.118 = bf16[8,256]{1,0:T(8,128)(2,1)S(1)} custom-call(bf16[8,256]{1,0:T(8,128)(2,1)} %tok_hbm.1, f32[1,4096]{1,0:T(1,128)} %bitcast.13, s32[2,8]{1,0:T(2,128)} %bitcast.15, f32[2,8]{1,0:T(2,128)} %bitcast.16, bf16[2,64,4096]{2,1,0:T(8,128)(2,1)} %bitcast.9, bf16[2,64,4096]{2,1,0:T(8,128)(2,1)} %bitcast.10, bf16[2,64,4096]{2,1,0:T(8,128)(2,1)} %wd.1, ...), custom_call_target="tpu_custom_call" | custom-call | tf_op jit(solution)/shard_map/pallas_call | solution.py:572
  53.5 0.6 %copy.14 = bf16[8,256]{1,0:T(8,128)(2,1)} copy(bf16[8,256]{1,0:T(8,128)(2,1)S(1)} %shard_map.118) | data formatting | bytes 8192

commit v5 on v4

--- a/solution.py
+++ b/solution.py
@@ -347,9 +347,6 @@
     dh_copy = rcopy(dh_own, dh_par, dh_ssem, dh_rsem, partner)
     dh_copy.start()
 
-    for rel in (6, 2):
-        ag_copy(rel, 0, rel, partner).wait_recv()
-        pass_on(rel)
     for load in loads[4:12]:
         load.wait()
     for copy in wparts[0:NY]:
@@ -360,6 +357,41 @@
             dh_own[...], dd_own[k], preferred_element_type=F32
         ) + jnp.dot(dh_par[...], dd_par[k], preferred_element_type=F32)
     dense_in[y] = dense_out[y]
+    loads[2].wait()
+    loads[3].wait()
+    for copy in wparts[2 * NY :]:
+        copy.wait_recv()
+    for rel in (6, 2):
+        ag_copy(rel, 0, rel, partner).wait_recv()
+        pass_on(rel)
+    done.append(arrived(r_in, r_in, r_ssem, r_rsem, NEP - 1))
+    picked = (
+        lax.broadcasted_iota(jnp.int32, (ROWS, NEP), 0) // 4
+        == lax.broadcasted_iota(jnp.int32, (ROWS, NEP), 1)
+    )
+    spread = jnp.dot(
+        jnp.where(picked, 1.0, 0.0),
+        r_in[...].reshape(NEP, 256),
+        preferred_element_type=F32,
+        precision=lax.Precision.HIGHEST,
+    )
+    wanted = me_e * 8 + lax.broadcasted_iota(jnp.int32, (ROWS, 256), 0) % 4
+    here = lax.broadcasted_iota(jnp.int32, (ROWS, 256), 1) == wanted
+    row_scale = jnp.sum(jnp.where(here, spread, 0.0), axis=1, keepdims=True)
+
+    def project(*slices, first=False):
+        sums = [None, None]
+        for c, rel in slices:
+            cols = pl.ds(pl.multiple_of((2 * ys[rel] + c) * PART, PART), PART)
+            n = (gathered[c, ys[rel]].astype(F32) * row_scale * gain[:, cols]).astype(BF16)
+            for k in range(2):
+                v = nt_dot(n, w_gu[k, :, :, cols].reshape(256, PART))
+                sums[k] = v if sums[k] is None else sums[k] + v
+        for k in range(2):
+            acts[k] = sums[k] if first else acts[k] + sums[k]
+
+    pass_wait(0)
+    project((core, 0), (other, 0), (core, 6), (core, 2), first=True)
     for rel in (7, 1):
         ag_copy(rel, 0, rel, partner).wait_recv()
         pass_on(rel)
@@ -367,47 +399,19 @@
         rcopy(
             dense_out.at[ys[step]], dense_in.at[y], dense_ssem, dense_rsem, ydev(step)
         ).start()
-    loads[2].wait()
-    loads[3].wait()
-    for copy in wparts[2 * NY :]:
-        copy.wait_recv()
-    done.append(arrived(r_in, r_in, r_ssem, r_rsem, NEP - 1))
-    picked = (
-        lax.broadcasted_iota(jnp.int32, (ROWS, NEP), 0) // 4
-        == lax.broadcasted_iota(jnp.int32, (ROWS, NEP), 1)
-    )
-    spread = jnp.dot(
-        jnp.where(picked, 1.0, 0.0),
-        r_in[...].reshape(NEP, 256),
-        preferred_element_type=F32,
-        precision=lax.Precision.HIGHEST,
-    )
-    wanted = me_e * 8 + lax.broadcasted_iota(jnp.int32, (ROWS, 256), 0) % 4
-    here = lax.broadcasted_iota(jnp.int32, (ROWS, 256), 1) == wanted
-    row_scale = jnp.sum(jnp.where(here, spread, 0.0), axis=1, keepdims=True)
-
-    def project(c, rel, first=False):
-        cols = pl.ds(pl.multiple_of((2 * ys[rel] + c) * PART, PART), PART)
-        n = (gathered[c, ys[rel]].astype(F32) * row_scale * gain[:, cols]).astype(BF16)
-        for k in range(2):
-            v = nt_dot(n, w_gu[k, :, :, cols].reshape(256, PART))
-            acts[k] = v if first else acts[k] + v
-
-    project(core, 0, True)
-    for rel in NEAR:
-        project(core, rel)
-    for rel in (0,) + NEAR:
-        pass_wait(rel)
-        project(other, rel)
+    pass_wait(6)
+    pass_wait(2)
+    project((core, 7), (core, 1), (other, 6), (other, 2))
     done.append(arrived(far_out, far_in, far_ssem, far_rsem, NEP - 1))
     for i, rel in enumerate(FAR):
         keep_rows(far_in[:, i], rel)
         pass_on(rel)
-    for rel in FAR:
-        project(core, rel)
+    pass_wait(7)
+    pass_wait(1)
+    project((other, 7), (other, 1), (core, 3), (core, 4), (core, 5))
     for rel in FAR:
         pass_wait(rel)
-        project(other, rel)
+    project((other, 3), (other, 4), (other, 5))
 
     row = lax.broadcasted_iota(jnp.int32, (ROWS, 128), 0)
     col = lax.broadcasted_iota(jnp.int32, (ROWS, 128), 1)

time: 54.2 us -> 54 us (level)
  no operation moved by 1% of the time
where the time goes in v5:
time: 54 us; the launch traced here: 53.8 us
  Pallas kernels  53.2 us (99%)
  local copies, waits for them, and re-layouts  0.6 us (1%)
    pallas_call x1, Pallas kernels, local(): pl.pallas_call(kernel, out_shape=pltpu.VMEM((8, PART), BF16), in_specs=[p...  53.2 us

profile of v5, /device:TPU:1, one launch (start us, length us, event | category | flops | bytes accessed | tf_op | source)
XLA Modules:
  0.0 53.8 jit_solution(10376114655388440455)
XLA Ops:
  0.0 53.2 %shard_map.118 = bf16[8,256]{1,0:T(8,128)(2,1)S(1)} custom-call(bf16[8,256]{1,0:T(8,128)(2,1)} %tok_hbm.1, f32[1,4096]{1,0:T(1,128)} %bitcast.13, s32[2,8]{1,0:T(2,128)} %bitcast.15, f32[2,8]{1,0:T(2,128)} %bitcast.16, bf16[2,64,4096]{2,1,0:T(8,128)(2,1)} %bitcast.9, bf16[2,64,4096]{2,1,0:T(8,128)(2,1)} %bitcast.10, bf16[2,64,4096]{2,1,0:T(8,128)(2,1)} %wd.1, ...), custom_call_target="tpu_custom_call" | custom-call | tf_op jit(solution)/shard_map/pallas_call | solution.py:576
  53.2 0.6 %copy.14 = bf16[8,256]{1,0:T(8,128)(2,1)} copy(bf16[8,256]{1,0:T(8,128)(2,1)S(1)} %shard_map.118) | data formatting | bytes 8192

commit v6 on v5

--- a/solution.py
+++ b/solution.py
@@ -17,7 +17,7 @@
 NTP = 2 * NY
 ROWS = 128
 FAR = (3, 4, 5)
-NEAR = (2, 6, 1, 7)
+NEAR = (6, 2, 7, 1)
 PART = 256
 WIDTH = 4096
 
@@ -62,7 +62,8 @@
     mixw,
     ogain,
     w_gu,
-    wd_all,
+    wd_own,
+    wd_par,
     w_dense,
     dd_own,
     dd_par,
@@ -70,6 +71,7 @@
     a2a_in,
     far_out,
     far_in,
+    far_par,
     gathered,
     tok_all,
     dense_out,
@@ -117,6 +119,8 @@
     ag_rsem,
     pf_ssem,
     pf_rsem,
+    fp_ssem,
+    fp_rsem,
     r_ssem,
     r_rsem,
     q_ssem,
@@ -167,29 +171,29 @@
         pltpu.make_async_copy(mixw_hbm, mixw, i_sem.at[4]),
         pltpu.make_async_copy(ogain_hbm, ogain, i_sem.at[5]),
     ]
-    loads = [
-        pltpu.make_async_copy(dg, w_dense.at[pl.ds(0, 64)], w_sem.at[0]),
-        pltpu.make_async_copy(du, w_dense.at[pl.ds(64, 64)], w_sem.at[1]),
-        pltpu.make_async_copy(wg, w_gu.at[0, pl.ds(0, 2)], w_sem.at[2]),
-        pltpu.make_async_copy(wu, w_gu.at[0, pl.ds(2, 2)], w_sem.at[3]),
-    ]
 
     def columns(k, c):
         return pl.ds(pl.multiple_of((2 * k + c) * PART, PART), PART)
 
+    def load(src, dst, k):
+        pltpu.make_async_copy(src, dst, w_sem.at[k]).start()
+
+    def loaded(dst, k):
+        pltpu.make_async_copy(dst, dst, w_sem.at[k]).wait()
+
+    for copy in smalls:
+        copy.start()
+    load(dg, w_dense.at[pl.ds(0, 64)], 0)
+    load(du, w_dense.at[pl.ds(64, 64)], 0)
     for k in range(NY):
-        loads.append(
-            pltpu.make_async_copy(dd.at[:, columns(k, core)], dd_own.at[k], w_sem.at[4 + k])
-        )
+        load(dd.at[:, columns(k, core)], dd_own.at[k], 1)
+    load(wg, w_gu.at[0, pl.ds(0, 2)], 2)
+    load(wu, w_gu.at[0, pl.ds(2, 2)], 2)
     for k in range(NY):
-        loads.append(
-            pltpu.make_async_copy(wd.at[:, :, columns(k, core)], wd_all.at[k, 0], w_sem.at[12 + k])
-        )
-    for load in smalls + loads:
-        load.start()
-
-    for load in smalls[0:3]:
-        load.wait()
+        load(wd.at[:, :, columns(k, core)], wd_own.at[k], 3)
+
+    for copy in smalls[0:3]:
+        copy.wait()
     lane = lax.broadcasted_iota(jnp.int32, (8, 256), 1)
     sub = lax.broadcasted_iota(jnp.int32, (8, 256), 0)
     expert = 2 * (lane // 8) + (lane // 2) % 2
@@ -245,33 +249,22 @@
     for peer in peers:
         rcopy(a2a_out.at[peer], a2a_in.at[me_e], a2a_ssem, a2a_rsem, (peer, me_t)).start()
 
-    wparts = []
     for k in range(NY):
-        copy = rcopy(
-            dd.at[:, columns(k, other)], dd_par.at[k], wp_ssem.at[k], wp_rsem.at[k], partner
-        )
-        copy.start()
-        wparts.append(copy)
+        rcopy(
+            dd.at[:, columns(k, other)], dd_par.at[k], wp_ssem.at[0], wp_rsem.at[0], partner
+        ).start()
+    for k, ref in enumerate((wg, wu)):
+        rcopy(
+            ref, w_gu.at[1, pl.ds(2 * k, 2)], wp_ssem.at[1], wp_rsem.at[1], partner
+        ).start()
     for k in range(NY):
-        copy = rcopy(
-            wd.at[:, :, columns(k, other)],
-            wd_all.at[k, 1],
-            wp_ssem.at[NY + k],
-            wp_rsem.at[NY + k],
-            partner,
-        )
-        copy.start()
-        wparts.append(copy)
-    for k, ref in enumerate((wg, wu)):
-        copy = rcopy(
-            ref,
-            w_gu.at[1, pl.ds(2 * k, 2)],
-            wp_ssem.at[2 * NY + k],
-            wp_rsem.at[2 * NY + k],
-            partner,
-        )
-        copy.start()
-        wparts.append(copy)
+        rcopy(
+            wd.at[:, :, columns(k, other)], wd_par.at[k], wp_ssem.at[2], wp_rsem.at[2], partner
+        ).start()
+    parts = [
+        rcopy(ref, ref, wp_ssem.at[k], wp_rsem.at[k], partner)
+        for k, ref in enumerate((dd_par, w_gu.at[1], wd_par))
+    ]
 
     def arrived(src, dst, ssem, rsem, n):
         part = pl.ds(0, n)
@@ -286,53 +279,51 @@
         squares = squares + v * v
     scale = lax.rsqrt(jnp.sum(squares, axis=1, keepdims=True) / WIDTH + EPS)
     r_out[...] = jnp.sum(slots[...] * scale, axis=0, keepdims=True)
-    for peer in peers:
-        rcopy(r_out, r_in.at[me_e], r_ssem, r_rsem, (peer, me_t)).start()
-    r_in[me_e] = r_out[...]
     for i, rel in enumerate(FAR):
         far_out[:, i] = placed_rows(tok_all[ys[rel] * 2 + core])
     for peer in peers:
+        rcopy(r_out, r_in.at[me_e], r_ssem, r_rsem, (peer, me_t)).start()
+    for peer in peers:
         rcopy(far_out.at[peer], far_in.at[me_e], far_ssem, far_rsem, (peer, me_t)).start()
+    r_in[me_e] = r_out[...]
     far_in[me_e] = far_out[me_e]
 
     done.append(arrived(a2a_out, a2a_in, a2a_ssem, a2a_rsem, NEP - 1))
     sub3 = lax.broadcasted_iota(jnp.int32, (16, 8, 128), 1)
 
-    def keep_rows(value, rel):
+    def keep_rows(value, c, rel):
         pairs = value.astype(F32).reshape(16, 2, 8, 128)
         even, odd = pairs[:, 0], pairs[:, 1]
         left = jnp.where(sub3 < 4, even, pltpu.roll(odd, 4, 1)).reshape(ROWS, 128)
         right = jnp.where(sub3 < 4, pltpu.roll(even, 4, 1), odd).reshape(ROWS, 128)
-        gathered[core, ys[rel], :, 0:128] = left.astype(BF16)
-        gathered[core, ys[rel], :, 128:256] = right.astype(BF16)
-
-    keep_rows(a2a_in[...], 0)
-
-    sends = []
-
-    def ag_copy(slot, k, rel, device):
+        gathered[c, ys[rel], :, 0:128] = left.astype(BF16)
+        gathered[c, ys[rel], :, 128:256] = right.astype(BF16)
+
+    keep_rows(a2a_in[...], core, 0)
+
+    def ag_copy(slot, k, device):
         ref = gathered.at[core, ys[slot]]
-        return rcopy(ref, ref, ag_ssem.at[k], ag_rsem.at[rel], device)
-
-    for k, (rel, step) in enumerate(((6, 2), (2, -2), (7, 1), (1, -1))):
-        copy = ag_copy(0, k, rel, ydev(step))
-        copy.start()
-        sends.append(copy)
+        return rcopy(ref, ref, ag_ssem, ag_rsem.at[k], device)
+
+    for k, step in enumerate((2, -2, 1, -1)):
+        ag_copy(0, k, ydev(step)).start()
+
+    def pass_copy(c, rel):
+        ref = gathered.at[c, ys[rel]]
+        k = ((0,) + NEAR).index(rel)
+        return rcopy(ref, ref, pf_ssem, pf_rsem.at[k], partner)
 
     def pass_on(rel):
-        ref = gathered.at[core, ys[rel]]
-        copy = rcopy(ref, ref, pf_ssem.at[rel], pf_rsem.at[rel], partner)
-        copy.start()
-        sends.append(copy)
+        pass_copy(core, rel).start()
 
     def pass_wait(rel):
-        ref = gathered.at[other, ys[rel]]
-        rcopy(ref, ref, pf_ssem.at[rel], pf_rsem.at[rel], partner).wait_recv()
+        pass_copy(other, rel).wait_recv()
 
     pass_on(0)
 
-    for load in smalls[3:6] + loads[0:2]:
-        load.wait()
+    for copy in smalls[3:6]:
+        copy.wait()
+    loaded(w_dense, 0)
     act = jnp.zeros((8, 128), F32)
     mix_acc = jnp.zeros((8, PART), F32)
     for j in range(NTP):
@@ -347,22 +338,18 @@
     dh_copy = rcopy(dh_own, dh_par, dh_ssem, dh_rsem, partner)
     dh_copy.start()
 
-    for load in loads[4:12]:
-        load.wait()
-    for copy in wparts[0:NY]:
-        copy.wait_recv()
+    loaded(dd_own, 1)
+    parts[0].wait_recv()
     dh_copy.wait_recv()
     for k in range(NY):
         dense_out[k] = jnp.dot(
             dh_own[...], dd_own[k], preferred_element_type=F32
         ) + jnp.dot(dh_par[...], dd_par[k], preferred_element_type=F32)
     dense_in[y] = dense_out[y]
-    loads[2].wait()
-    loads[3].wait()
-    for copy in wparts[2 * NY :]:
-        copy.wait_recv()
+    loaded(w_gu.at[0], 2)
+    parts[1].wait_recv()
     for rel in (6, 2):
-        ag_copy(rel, 0, rel, partner).wait_recv()
+        ag_copy(rel, NEAR.index(rel), partner).wait_recv()
         pass_on(rel)
     done.append(arrived(r_in, r_in, r_ssem, r_rsem, NEP - 1))
     picked = (
@@ -393,7 +380,7 @@
     pass_wait(0)
     project((core, 0), (other, 0), (core, 6), (core, 2), first=True)
     for rel in (7, 1):
-        ag_copy(rel, 0, rel, partner).wait_recv()
+        ag_copy(rel, NEAR.index(rel), partner).wait_recv()
         pass_on(rel)
     for step in y_order:
         rcopy(
@@ -403,14 +390,16 @@
     pass_wait(2)
     project((core, 7), (core, 1), (other, 6), (other, 2))
     done.append(arrived(far_out, far_in, far_ssem, far_rsem, NEP - 1))
+    raw = rcopy(far_in, far_par, fp_ssem, fp_rsem, partner)
+    raw.start()
     for i, rel in enumerate(FAR):
-        keep_rows(far_in[:, i], rel)
-        pass_on(rel)
+        keep_rows(far_in[:, i], core, rel)
     pass_wait(7)
     pass_wait(1)
     project((other, 7), (other, 1), (core, 3), (core, 4), (core, 5))
-    for rel in FAR:
-        pass_wait(rel)
+    raw.wait_recv()
+    for i, rel in enumerate(FAR):
+        keep_rows(far_par[:, i], other, rel)
     project((other, 3), (other, 4), (other, 5))
 
     row = lax.broadcasted_iota(jnp.int32, (ROWS, 128), 0)
@@ -420,17 +409,17 @@
         v = acts[k]
         hidden = silu(v[:, 0:128]) * v[:, 128:256]
         hid[:, k * 128 : (k + 1) * 128] = jnp.where(mine, hidden, 0.0).astype(BF16)
-    for load in loads[12:]:
-        load.wait()
-    for copy in wparts[NY : 2 * NY]:
-        copy.wait_recv()
+    loaded(wd_own, 3)
+    parts[2].wait_recv()
 
     diagonal = row == col
 
     def partial(rel):
-        return jnp.dot(
-            hid[...], wd_all[ys[rel]].reshape(256, PART), preferred_element_type=F32
+        k = ys[rel]
+        both = jnp.concatenate(
+            [wd_own[k].reshape(128, PART), wd_par[k].reshape(128, PART)], axis=0
         )
+        return jnp.dot(hid[...], both, preferred_element_type=F32)
 
     def column(value):
         return jnp.sum(jnp.where(diagonal, value, 0.0), axis=0, keepdims=True)
@@ -444,8 +433,8 @@
 
     def q_copies(k, device):
         return (
-            rcopy(q_out.at[k], q_in.at[k], q_ssem.at[k], q_rsem.at[k], device),
-            rcopy(s_out.at[k], s_in.at[k], sc_ssem.at[k], sc_rsem.at[k], device),
+            rcopy(q_out.at[k], q_in.at[k], q_ssem, q_rsem.at[k], device),
+            rcopy(s_out.at[k], s_in.at[k], sc_ssem, sc_rsem.at[k], device),
         )
 
     def q_send(k):
@@ -455,7 +444,6 @@
         s_out[k] = column(most * (1.0 / 32767.0))
         for copy in q_copies(k, ydev(NEAR[k])):
             copy.start()
-            sends.append(copy)
 
     def q_get(k):
         for copy in q_copies(k, partner):
@@ -471,9 +459,10 @@
         fq_out[:, i] = messages(jnp.round(values[i] * (32767.0 / most))).astype(jnp.int16)
     for peer in peers:
         rcopy(fq_out.at[peer], fq_in.at[me_e], fq_ssem, fq_rsem, (peer, me_t)).start()
-        rcopy(fs_out, fs_in.at[me_e], fs_ssem, fs_rsem, (peer, me_t)).start()
     for k in range(4):
         q_send(k)
+    for peer in peers:
+        rcopy(fs_out, fs_in.at[me_e], fs_ssem, fs_rsem, (peer, me_t)).start()
     fq_in[me_e] = fq_out[me_e]
     fs_in[me_e] = fs_out[...]
     kept[...] = partial(0)
@@ -484,7 +473,7 @@
     gate = gate_ref[...]
     dense = jnp.concatenate([gate, gate], axis=1) * dense
     summed = kept[...]
-    for k in (2, 3, 0, 1):
+    for k in range(4):
         summed = summed + q_get(k)
     ret_out[...] = messages(summed)
     for peer in peers:
@@ -515,9 +504,7 @@
         cols = slice(i * 128, (i + 1) * 128)
         fy_out[i, :, 0:128] = far_sum[0:8, cols]
         fy_out[i, :, 128:256] = far_sum[8:16, cols]
-        copy = rcopy(fy_out.at[i], fy_in.at[i], fy_ssem.at[i], fy_rsem.at[i], ydev(rel))
-        copy.start()
-        sends.append(copy)
+        rcopy(fy_out.at[i], fy_in.at[i], fy_ssem, fy_rsem, ydev(rel)).start()
     done.append(arrived(ret_out, ret_in, ret_ssem, ret_rsem, NEP - 1))
     mixed = jnp.dot(
         comb[...],
@@ -526,9 +513,9 @@
         precision=lax.Precision.HIGHEST,
     )
     combined = jnp.concatenate([mixed[0:8], mixed[8:16]], axis=1) + dense
-    for i in range(3):
-        rcopy(fy_out.at[i], fy_in.at[i], fy_ssem.at[i], fy_rsem.at[i], partner).wait_recv()
-        combined = combined + fy_in[i]
+    fy_copy = rcopy(fy_out, fy_in, fy_ssem, fy_rsem, partner)
+    fy_copy.wait_recv()
+    combined = combined + fy_in[0] + fy_in[1] + fy_in[2]
     token_diagonal = (
         lax.broadcasted_iota(jnp.int32, (8, 128), 0)
         == lax.broadcasted_iota(jnp.int32, (8, 128), 1)
@@ -553,7 +540,15 @@
     )
     out[...] = (combined * final * ogain[...]).astype(BF16)
 
-    for copy in wparts + sends + [dh_copy] + done:
+    near = gathered.at[core, pl.ds(0, 4)]
+    done += [
+        rcopy(near, near, ag_ssem, ag_rsem.at[0], partner),
+        rcopy(q_out, q_in, q_ssem, q_rsem.at[0], partner),
+        rcopy(s_out, s_in, sc_ssem, sc_rsem.at[0], partner),
+    ]
+    five = gathered.at[core, pl.ds(0, 5)]
+    done.append(rcopy(five, five, pf_ssem, pf_rsem.at[0], partner))
+    for copy in parts + [dh_copy, raw, fy_copy] + done:
         copy.wait_send()
 
 
@@ -586,12 +581,14 @@
             pltpu.VMEM((1, WIDTH), F32),
             pltpu.VMEM((1, PART), F32),
             pltpu.VMEM((2, 4, 64, WIDTH), BF16),
-            pltpu.VMEM((NY, 2, 2, 64, PART), BF16),
+            pltpu.VMEM((NY, 2, 64, PART), BF16),
+            pltpu.VMEM((NY, 2, 64, PART), BF16),
             pltpu.VMEM((128, WIDTH), BF16),
             pltpu.VMEM((NY, 64, PART), BF16),
             pltpu.VMEM((NY, 64, PART), BF16),
             pltpu.VMEM((NEP, 8, 128), BF16),
             pltpu.VMEM((NEP, 8, 128), BF16),
+            pltpu.VMEM((NEP, 3, 8, 128), BF16),
             pltpu.VMEM((NEP, 3, 8, 128), BF16),
             pltpu.VMEM((NEP, 3, 8, 128), BF16),
             pltpu.VMEM((2, NY, ROWS, PART), BF16),
@@ -624,35 +621,37 @@
             pltpu.VMEM((NTP, 1, 128), F32),
             pltpu.VMEM((8, 128), F32),
             dma((6,)),
-            dma((20,)),
-            dma((2 * NY + 2,)),
-            dma((2 * NY + 2,)),
-            dma,
-            dma,
-            dma,
-            dma,
-            dma,
-            dma,
-            dma,
-            dma,
-            dma,
-            dma,
             dma((4,)),
-            dma((8,)),
-            dma((8,)),
-            dma((8,)),
-            dma,
-            dma,
-            dma((4,)),
-            dma((4,)),
-            dma((4,)),
-            dma((4,)),
-            dma,
-            dma,
-            dma,
-            dma,
             dma((3,)),
             dma((3,)),
+            dma,
+            dma,
+            dma,
+            dma,
+            dma,
+            dma,
+            dma,
+            dma,
+            dma,
+            dma,
+            dma,
+            dma((4,)),
+            dma,
+            dma((5,)),
+            dma,
+            dma,
+            dma,
+            dma,
+            dma,
+            dma((4,)),
+            dma,
+            dma((4,)),
+            dma,
+            dma,
+            dma,
+            dma,
+            dma,
+            dma,
             dma,
             dma,
             dma,

time: 54 us -> 54 us (level)
  no operation moved by 1% of the time
where the time goes in v6:
time: 54 us; the launch traced here: 53.9 us
  Pallas kernels  53.3 us (99%)
  local copies, waits for them, and re-layouts  0.6 us (1%)
    pallas_call x1, Pallas kernels, local(): pl.pallas_call(kernel, out_shape=pltpu.VMEM((8, PART), BF16), in_specs=[p...  53.3 us

profile of v6, /device:TPU:1, one launch (start us, length us, event | category | flops | bytes accessed | tf_op | source)
XLA Modules:
  0.0 53.9 jit_solution(7239792722747381237)
XLA Ops:
  0.0 53.3 %shard_map.118 = bf16[8,256]{1,0:T(8,128)(2,1)S(1)} custom-call(bf16[8,256]{1,0:T(8,128)(2,1)} %tok_hbm.1, f32[1,4096]{1,0:T(1,128)} %bitcast.13, s32[2,8]{1,0:T(2,128)} %bitcast.15, f32[2,8]{1,0:T(2,128)} %bitcast.16, bf16[2,64,4096]{2,1,0:T(8,128)(2,1)} %bitcast.9, bf16[2,64,4096]{2,1,0:T(8,128)(2,1)} %bitcast.10, bf16[2,64,4096]{2,1,0:T(8,128)(2,1)} %wd.1, ...), custom_call_target="tpu_custom_call" | custom-call | tf_op jit(solution)/shard_map/pallas_call | solution.py:571
  53.3 0.6 %copy.14 = bf16[8,256]{1,0:T(8,128)(2,1)} copy(bf16[8,256]{1,0:T(8,128)(2,1)S(1)} %shard_map.118) | data formatting | bytes 8192

commit v7 on v6

--- a/solution.py
+++ b/solution.py
@@ -16,6 +16,7 @@
 NEP = NX * NZ
 NTP = 2 * NY
 ROWS = 128
+HALF = ROWS // 2
 FAR = (3, 4, 5)
 NEAR = (6, 2, 7, 1)
 PART = 256
@@ -150,6 +151,23 @@
     peers = [zs[dz] + xs[dx] for dz in (4, 3, 5, 2, 6, 1, 7, 0) for dx in (2, 1, 3, 0)][:-1]
     y_order = (4, 3, 5, 2, 6, 1, 7)
 
+    block = lax.div(z, 4)
+    opposite = zs[4] + xs[0]
+    z4 = [lax.rem(z + k, 4) * NX for k in range(4)]
+
+    def to_block(b, send):
+        for dz in (2, 1, 3, 0):
+            for dx in (2, 1, 3, 0):
+                if dz or dx:
+                    send(4 * NX * b + z4[dz] + xs[dx])
+
+        @pl.when(block != b)
+        def _():
+            send(opposite)
+
+    def part(b, n):
+        return pl.ds(b * n, n)
+
     def ydev(step):
         return (me_e, ys[step % NY] * 2 + core)
 
@@ -267,8 +285,8 @@
     ]
 
     def arrived(src, dst, ssem, rsem, n):
-        part = pl.ds(0, n)
-        copy = rcopy(src.at[part], dst.at[part], ssem, rsem, partner)
+        first = pl.ds(0, n)
+        copy = rcopy(src.at[first], dst.at[first], ssem, rsem, partner)
         copy.wait_recv()
         return copy
 
@@ -283,23 +301,34 @@
         far_out[:, i] = placed_rows(tok_all[ys[rel] * 2 + core])
     for peer in peers:
         rcopy(r_out, r_in.at[me_e], r_ssem, r_rsem, (peer, me_t)).start()
-    for peer in peers:
-        rcopy(far_out.at[peer], far_in.at[me_e], far_ssem, far_rsem, (peer, me_t)).start()
+    def send_far():
+        for peer in peers:
+            rcopy(
+                far_out.at[peer], far_in.at[me_e], far_ssem, far_rsem.at[block], (peer, me_t)
+            ).start()
+
+    pl.when(block == 0)(send_far)
+    far_self = pltpu.make_async_copy(
+        far_out.at[me_e], far_in.at[me_e], far_rsem.at[block]
+    )
+    far_self.start()
     r_in[me_e] = r_out[...]
-    far_in[me_e] = far_out[me_e]
 
     done.append(arrived(a2a_out, a2a_in, a2a_ssem, a2a_rsem, NEP - 1))
-    sub3 = lax.broadcasted_iota(jnp.int32, (16, 8, 128), 1)
-
-    def keep_rows(value, c, rel):
-        pairs = value.astype(F32).reshape(16, 2, 8, 128)
+    def low_half(n):
+        return lax.broadcasted_iota(jnp.int32, (n, 8, 128), 1) < 4
+
+    def keep_rows(value, c, rel, rows):
+        n = value.shape[0] // 2
+        low = low_half(n)
+        pairs = value.astype(F32).reshape(n, 2, 8, 128)
         even, odd = pairs[:, 0], pairs[:, 1]
-        left = jnp.where(sub3 < 4, even, pltpu.roll(odd, 4, 1)).reshape(ROWS, 128)
-        right = jnp.where(sub3 < 4, pltpu.roll(even, 4, 1), odd).reshape(ROWS, 128)
-        gathered[c, ys[rel], :, 0:128] = left.astype(BF16)
-        gathered[c, ys[rel], :, 128:256] = right.astype(BF16)
-
-    keep_rows(a2a_in[...], core, 0)
+        left = jnp.where(low, even, pltpu.roll(odd, 4, 1)).reshape(8 * n, 128)
+        right = jnp.where(low, pltpu.roll(even, 4, 1), odd).reshape(8 * n, 128)
+        gathered[c, ys[rel], rows, 0:128] = left.astype(BF16)
+        gathered[c, ys[rel], rows, 128:256] = right.astype(BF16)
+
+    keep_rows(a2a_in[...], core, 0, slice(0, ROWS))
 
     def ag_copy(slot, k, device):
         ref = gathered.at[core, ys[slot]]
@@ -337,6 +366,7 @@
     dh_own[...] = (silu(act[:, 0:64]) * act[:, 64:128]).astype(BF16)
     dh_copy = rcopy(dh_own, dh_par, dh_ssem, dh_rsem, partner)
     dh_copy.start()
+    pl.when(block == 1)(send_far)
 
     loaded(dd_own, 1)
     parts[0].wait_recv()
@@ -366,16 +396,17 @@
     here = lax.broadcasted_iota(jnp.int32, (ROWS, 256), 1) == wanted
     row_scale = jnp.sum(jnp.where(here, spread, 0.0), axis=1, keepdims=True)
 
-    def project(*slices, first=False):
+    def project(*slices, rows=slice(0, ROWS), first=False):
         sums = [None, None]
         for c, rel in slices:
             cols = pl.ds(pl.multiple_of((2 * ys[rel] + c) * PART, PART), PART)
-            n = (gathered[c, ys[rel]].astype(F32) * row_scale * gain[:, cols]).astype(BF16)
+            n = gathered[c, ys[rel], rows].astype(F32) * row_scale[rows] * gain[:, cols]
+            n = n.astype(BF16)
             for k in range(2):
                 v = nt_dot(n, w_gu[k, :, :, cols].reshape(256, PART))
                 sums[k] = v if sums[k] is None else sums[k] + v
         for k in range(2):
-            acts[k] = sums[k] if first else acts[k] + sums[k]
+            acts[k, rows] = sums[k] if first else acts[k, rows] + sums[k]
 
     pass_wait(0)
     project((core, 0), (other, 0), (core, 6), (core, 2), first=True)
@@ -389,100 +420,139 @@
     pass_wait(6)
     pass_wait(2)
     project((core, 7), (core, 1), (other, 6), (other, 2))
-    done.append(arrived(far_out, far_in, far_ssem, far_rsem, NEP - 1))
-    raw = rcopy(far_in, far_par, fp_ssem, fp_rsem, partner)
-    raw.start()
-    for i, rel in enumerate(FAR):
-        keep_rows(far_in[:, i], core, rel)
-    pass_wait(7)
-    pass_wait(1)
-    project((other, 7), (other, 1), (core, 3), (core, 4), (core, 5))
-    raw.wait_recv()
-    for i, rel in enumerate(FAR):
-        keep_rows(far_par[:, i], other, rel)
-    project((other, 3), (other, 4), (other, 5))
-
-    row = lax.broadcasted_iota(jnp.int32, (ROWS, 128), 0)
-    col = lax.broadcasted_iota(jnp.int32, (ROWS, 128), 1)
+    row = lax.broadcasted_iota(jnp.int32, (HALF, 128), 0)
+    col = lax.broadcasted_iota(jnp.int32, (HALF, 128), 1)
     mine = (row // 2) % 2 == col // 64
-    for k in range(2):
-        v = acts[k]
-        hidden = silu(v[:, 0:128]) * v[:, 128:256]
-        hid[:, k * 128 : (k + 1) * 128] = jnp.where(mine, hidden, 0.0).astype(BF16)
-    loaded(wd_own, 3)
-    parts[2].wait_recv()
-
     diagonal = row == col
 
-    def partial(rel):
+    def rows_of(b):
+        return slice(b * HALF, (b + 1) * HALF)
+
+    def far_wait(b):
+        ref = far_in.at[part(b, 16)]
+        rcopy(ref, ref, far_ssem, far_rsem.at[b], partner).wait_recv()
+        copy = rcopy(ref, far_par.at[part(b, 16)], fp_ssem, fp_rsem.at[b], partner)
+        copy.start()
+        for i, rel in enumerate(FAR):
+            keep_rows(far_in[b * 16 : (b + 1) * 16, i], core, rel, rows_of(b))
+        return copy
+
+    def far_other(b, copy):
+        copy.wait_recv()
+        for i, rel in enumerate(FAR):
+            keep_rows(far_par[b * 16 : (b + 1) * 16, i], other, rel, rows_of(b))
+        project((other, 3), (other, 4), (other, 5), rows=rows_of(b))
+
+    def hide(b):
+        for k in range(2):
+            v = acts[k, rows_of(b)]
+            hidden = silu(v[:, 0:128]) * v[:, 128:256]
+            hid[rows_of(b), k * 128 : (k + 1) * 128] = jnp.where(mine, hidden, 0.0).astype(
+                BF16
+            )
+
+    def partial(rel, b):
         k = ys[rel]
         both = jnp.concatenate(
             [wd_own[k].reshape(128, PART), wd_par[k].reshape(128, PART)], axis=0
         )
-        return jnp.dot(hid[...], both, preferred_element_type=F32)
+        return jnp.dot(hid[rows_of(b), :], both, preferred_element_type=F32)
 
     def column(value):
         return jnp.sum(jnp.where(diagonal, value, 0.0), axis=0, keepdims=True)
 
     def messages(value):
-        left = value[:, 0:128].reshape(16, 8, 128)
-        right = value[:, 128:256].reshape(16, 8, 128)
-        even = jnp.where(sub3 < 4, left, pltpu.roll(right, 4, 1))
-        odd = jnp.where(sub3 < 4, pltpu.roll(left, 4, 1), right)
-        return jnp.stack([even, odd], axis=1).reshape(NEP, 8, 128)
-
-    def q_copies(k, device):
+        n = value.shape[0] // 8
+        low = low_half(n)
+        left = value[:, 0:128].reshape(n, 8, 128)
+        right = value[:, 128:256].reshape(n, 8, 128)
+        even = jnp.where(low, left, pltpu.roll(right, 4, 1))
+        odd = jnp.where(low, pltpu.roll(left, 4, 1), right)
+        return jnp.stack([even, odd], axis=1).reshape(2 * n, 8, 128)
+
+    def q_copies(k, b, device):
+        at = (k, b)
         return (
-            rcopy(q_out.at[k], q_in.at[k], q_ssem, q_rsem.at[k], device),
-            rcopy(s_out.at[k], s_in.at[k], sc_ssem, sc_rsem.at[k], device),
+            rcopy(q_out.at[at], q_in.at[at], q_ssem, q_rsem.at[at], device),
+            rcopy(s_out.at[at], s_in.at[at], sc_ssem, sc_rsem.at[at], device),
         )
 
-    def q_send(k):
-        value = partial(NEAR[k])
+    def q_send(k, b):
+        value = partial(NEAR[k], b)
         most = jnp.maximum(jnp.max(jnp.abs(value), axis=1, keepdims=True), 1e-30)
-        q_out[k] = jnp.round(value * (32767.0 / most)).astype(jnp.int16)
-        s_out[k] = column(most * (1.0 / 32767.0))
-        for copy in q_copies(k, ydev(NEAR[k])):
+        q_out[k, b] = jnp.round(value * (32767.0 / most)).astype(jnp.int16)
+        s_out[k, b] = column(most * (1.0 / 32767.0))
+        for copy in q_copies(k, b, ydev(NEAR[k])):
             copy.start()
 
-    def q_get(k):
-        for copy in q_copies(k, partner):
+    def q_get(k, b):
+        for copy in q_copies(k, b, partner):
             copy.wait_recv()
-        unit = jnp.sum(jnp.where(diagonal, s_in[k], 0.0), axis=1, keepdims=True)
-        return q_in[k].astype(F32) * unit
-
-    values = [partial(rel) for rel in FAR]
-    most = jnp.maximum(jnp.maximum(jnp.abs(values[0]), jnp.abs(values[1])), jnp.abs(values[2]))
-    most = jnp.maximum(jnp.max(most, axis=1, keepdims=True), 1e-30)
-    fs_out[...] = column(most * (1.0 / 32767.0))
-    for i in range(3):
-        fq_out[:, i] = messages(jnp.round(values[i] * (32767.0 / most))).astype(jnp.int16)
-    for peer in peers:
+        unit = jnp.sum(jnp.where(diagonal, s_in[k, b], 0.0), axis=1, keepdims=True)
+        return q_in[k, b].astype(F32) * unit
+
+    def send_fq(peer):
         rcopy(fq_out.at[peer], fq_in.at[me_e], fq_ssem, fq_rsem, (peer, me_t)).start()
-    for k in range(4):
-        q_send(k)
-    for peer in peers:
-        rcopy(fs_out, fs_in.at[me_e], fs_ssem, fs_rsem, (peer, me_t)).start()
+
+    def down(b):
+        values = [partial(rel, b) for rel in FAR]
+        most = jnp.maximum(
+            jnp.maximum(jnp.abs(values[0]), jnp.abs(values[1])), jnp.abs(values[2])
+        )
+        most = jnp.maximum(jnp.max(most, axis=1, keepdims=True), 1e-30)
+        fs_out[b] = column(most * (1.0 / 32767.0))
+        for i in range(3):
+            fq_out[b * 16 : (b + 1) * 16, i] = messages(
+                jnp.round(values[i] * (32767.0 / most))
+            ).astype(jnp.int16)
+        to_block(b, send_fq)
+        for k in range(4):
+            q_send(k, b)
+
+        def send_fs(peer):
+            rcopy(fs_out.at[b], fs_in.at[me_e], fs_ssem, fs_rsem, (peer, me_t)).start()
+
+        to_block(b, send_fs)
+        kept[b] = partial(0, b)
+
+    def send_ret(peer):
+        rcopy(ret_out.at[peer], ret_in.at[me_e], ret_ssem, ret_rsem, (peer, me_t)).start()
+
+    def give_back(b):
+        summed = kept[b]
+        for k in range(4):
+            summed = summed + q_get(k, b)
+        ret_out[b * 16 : (b + 1) * 16] = messages(summed)
+        to_block(b, send_ret)
+
+    raw0 = far_wait(0)
+    pass_wait(7)
+    pass_wait(1)
+    project((other, 7), (other, 1))
+    project((core, 3), (core, 4), (core, 5), rows=rows_of(0))
+    far_other(0, raw0)
+    hide(0)
+    loaded(wd_own, 3)
+    parts[2].wait_recv()
+    down(0)
+    raw1 = far_wait(1)
+    project((core, 3), (core, 4), (core, 5), rows=rows_of(1))
+    far_other(1, raw1)
+    hide(1)
+    down(1)
     fq_in[me_e] = fq_out[me_e]
-    fs_in[me_e] = fs_out[...]
-    kept[...] = partial(0)
+    fs_in[me_e] = fs_out[block]
     done.append(arrived(dense_out, dense_in, dense_ssem, dense_rsem, NY - 1))
     dense = dense_in[0]
     for k in range(1, NY):
         dense = dense + dense_in[k]
     gate = gate_ref[...]
     dense = jnp.concatenate([gate, gate], axis=1) * dense
-    summed = kept[...]
-    for k in range(4):
-        summed = summed + q_get(k)
-    ret_out[...] = messages(summed)
-    for peer in peers:
-        rcopy(ret_out.at[peer], ret_in.at[me_e], ret_ssem, ret_rsem, (peer, me_t)).start()
-    ret_in[me_e] = ret_out[me_e]
+    give_back(0)
     done.append(arrived(fq_out, fq_in, fq_ssem, fq_rsem, NEP - 1))
     done.append(arrived(fs_in, fs_in, fs_ssem, fs_rsem, NEP - 1))
     lane2 = lax.broadcasted_iota(jnp.int32, (128, 256), 1)
-    mine4 = lax.broadcasted_iota(jnp.int32, (128, 256), 0) == me_e * 4 + lane2 % 4
+    mine4 = lax.broadcasted_iota(jnp.int32, (128, 256), 0) == lax.rem(me_e, 16) * 4 + lane2 % 4
     unit = jnp.dot(
         fs_in[...].reshape(NEP, 128),
         jnp.where(mine4, 1.0, 0.0),
@@ -505,6 +575,8 @@
         fy_out[i, :, 0:128] = far_sum[0:8, cols]
         fy_out[i, :, 128:256] = far_sum[8:16, cols]
         rcopy(fy_out.at[i], fy_in.at[i], fy_ssem, fy_rsem, ydev(rel)).start()
+    give_back(1)
+    ret_in[me_e] = ret_out[me_e]
     done.append(arrived(ret_out, ret_in, ret_ssem, ret_rsem, NEP - 1))
     mixed = jnp.dot(
         comb[...],
@@ -541,14 +613,16 @@
     out[...] = (combined * final * ogain[...]).astype(BF16)
 
     near = gathered.at[core, pl.ds(0, 4)]
+    most_far = far_in.at[pl.ds(0, NEP - 1)]
     done += [
         rcopy(near, near, ag_ssem, ag_rsem.at[0], partner),
-        rcopy(q_out, q_in, q_ssem, q_rsem.at[0], partner),
-        rcopy(s_out, s_in, sc_ssem, sc_rsem.at[0], partner),
+        rcopy(q_out, q_in, q_ssem, q_rsem.at[0, 0], partner),
+        rcopy(s_out, s_in, sc_ssem, sc_rsem.at[0, 0], partner),
+        rcopy(most_far, most_far, far_ssem, far_rsem.at[0], partner),
     ]
     five = gathered.at[core, pl.ds(0, 5)]
     done.append(rcopy(five, five, pf_ssem, pf_rsem.at[0], partner))
-    for copy in parts + [dh_copy, raw, fy_copy] + done:
+    for copy in parts + [dh_copy, raw0, raw1, fy_copy] + done:
         copy.wait_send()
 
 
@@ -604,17 +678,17 @@
             pltpu.VMEM((NEP, 1, 256), F32),
             pltpu.VMEM((2, ROWS, 256), F32),
             pltpu.VMEM((ROWS, 256), BF16),
-            pltpu.VMEM((4, ROWS, PART), jnp.int16),
-            pltpu.VMEM((4, ROWS, PART), jnp.int16),
-            pltpu.VMEM((4, 1, 128), F32),
-            pltpu.VMEM((4, 1, 128), F32),
+            pltpu.VMEM((4, 2, HALF, PART), jnp.int16),
+            pltpu.VMEM((4, 2, HALF, PART), jnp.int16),
+            pltpu.VMEM((4, 2, 1, 128), F32),
+            pltpu.VMEM((4, 2, 1, 128), F32),
             pltpu.VMEM((NEP, 3, 8, 128), jnp.int16),
             pltpu.VMEM((NEP, 3, 8, 128), jnp.int16),
-            pltpu.VMEM((1, 128), F32),
+            pltpu.VMEM((2, 1, 128), F32),
             pltpu.VMEM((NEP, 1, 128), F32),
             pltpu.VMEM((3, 8, PART), F32),
             pltpu.VMEM((3, 8, PART), F32),
-            pltpu.VMEM((ROWS, PART), F32),
+            pltpu.VMEM((2, HALF, PART), F32),
             pltpu.VMEM((NEP, 8, 128), F32),
             pltpu.VMEM((NEP, 8, 128), F32),
             pltpu.VMEM((1, 128), F32),
@@ -627,7 +701,7 @@
             dma,
             dma,
             dma,
-            dma,
+            dma((2,)),
             dma,
             dma,
             dma,
@@ -639,13 +713,13 @@
             dma,
             dma((5,)),
             dma,
-            dma,
-            dma,
-            dma,
-            dma,
-            dma((4,)),
-            dma,
-            dma((4,)),
+            dma((2,)),
+            dma,
+            dma,
+            dma,
+            dma((4, 2)),
+            dma,
+            dma((4, 2)),
             dma,
             dma,
             dma,

time: 54 us -> 54.2 us (level)
  the two profiles are of different devices: /device:TPU:1 before, /device:TPU:64 now
where the time goes in v7:
time: 54.2 us; the launch traced here: 54.1 us
  Pallas kernels  53.5 us (99%)
  local copies, waits for them, and re-layouts  0.6 us (1%)
    pallas_call x1, Pallas kernels, local(): pl.pallas_call(kernel, out_shape=pltpu.VMEM((8, PART), BF16), in_specs=[p...  53.5 us

profile of v7, /device:TPU:64, one launch (start us, length us, event | category | flops | bytes accessed | tf_op | source)
XLA Modules:
  0.0 54.1 jit_solution(10568043331518074148)
XLA Ops:
  0.0 53.5 %shard_map.118 = bf16[8,256]{1,0:T(8,128)(2,1)S(1)} custom-call(bf16[8,256]{1,0:T(8,128)(2,1)} %tok_hbm.1, f32[1,4096]{1,0:T(1,128)} %bitcast.13, s32[2,8]{1,0:T(2,128)} %bitcast.15, f32[2,8]{1,0:T(2,128)} %bitcast.16, bf16[2,64,4096]{2,1,0:T(8,128)(2,1)} %bitcast.9, bf16[2,64,4096]{2,1,0:T(8,128)(2,1)} %bitcast.10, bf16[2,64,4096]{2,1,0:T(8,128)(2,1)} %wd.1, ...), custom_call_target="tpu_custom_call" | custom-call | tf_op jit(solution)/shard_map/pallas_call | solution.py:645
  53.5 0.6 %copy.14 = bf16[8,256]{1,0:T(8,128)(2,1)} copy(bf16[8,256]{1,0:T(8,128)(2,1)S(1)} %shard_map.118) | data formatting | bytes 8192

commit v8 on v6

--- a/solution.py
+++ b/solution.py
@@ -149,6 +149,7 @@
     ys = [lax.rem(y + k, NY) for k in range(NY)]
     peers = [zs[dz] + xs[dx] for dz in (4, 3, 5, 2, 6, 1, 7, 0) for dx in (2, 1, 3, 0)][:-1]
     y_order = (4, 3, 5, 2, 6, 1, 7)
+    owners = [k + lax.div(k - me_e + NEP, NEP) for k in range(NEP - 1)]
 
     def ydev(step):
         return (me_e, ys[step % NY] * 2 + core)
@@ -457,11 +458,11 @@
     fs_out[...] = column(most * (1.0 / 32767.0))
     for i in range(3):
         fq_out[:, i] = messages(jnp.round(values[i] * (32767.0 / most))).astype(jnp.int16)
-    for peer in peers:
+    for peer in owners:
         rcopy(fq_out.at[peer], fq_in.at[me_e], fq_ssem, fq_rsem, (peer, me_t)).start()
     for k in range(4):
         q_send(k)
-    for peer in peers:
+    for peer in owners:
         rcopy(fs_out, fs_in.at[me_e], fs_ssem, fs_rsem, (peer, me_t)).start()
     fq_in[me_e] = fq_out[me_e]
     fs_in[me_e] = fs_out[...]
@@ -476,7 +477,7 @@
     for k in range(4):
         summed = summed + q_get(k)
     ret_out[...] = messages(summed)
-    for peer in peers:
+    for peer in owners:
         rcopy(ret_out.at[peer], ret_in.at[me_e], ret_ssem, ret_rsem, (peer, me_t)).start()
     ret_in[me_e] = ret_out[me_e]
     done.append(arrived(fq_out, fq_in, fq_ssem, fq_rsem, NEP - 1))

time: 54 us -> 54.1 us (level)
  no operation moved by 1% of the time
where the time goes in v8:
time: 54.1 us; the launch traced here: 54 us
  Pallas kernels  53.3 us (99%)
  local copies, waits for them, and re-layouts  0.6 us (1%)
    pallas_call x1, Pallas kernels, local(): pl.pallas_call(kernel, out_shape=pltpu.VMEM((8, PART), BF16), in_specs=[p...  53.3 us

profile of v8, /device:TPU:1, one launch (start us, length us, event | category | flops | bytes accessed | tf_op | source)
XLA Modules:
  0.0 54.0 jit_solution(17578708572057137498)
XLA Ops:
  0.0 53.3 %shard_map.118 = bf16[8,256]{1,0:T(8,128)(2,1)S(1)} custom-call(bf16[8,256]{1,0:T(8,128)(2,1)} %tok_hbm.1, f32[1,4096]{1,0:T(1,128)} %bitcast.13, s32[2,8]{1,0:T(2,128)} %bitcast.15, f32[2,8]{1,0:T(2,128)} %bitcast.16, bf16[2,64,4096]{2,1,0:T(8,128)(2,1)} %bitcast.9, bf16[2,64,4096]{2,1,0:T(8,128)(2,1)} %bitcast.10, bf16[2,64,4096]{2,1,0:T(8,128)(2,1)} %wd.1, ...), custom_call_target="tpu_custom_call" | custom-call | tf_op jit(solution)/shard_map/pallas_call | solution.py:572
  53.4 0.6 %copy.14 = bf16[8,256]{1,0:T(8,128)(2,1)} copy(bf16[8,256]{1,0:T(8,128)(2,1)S(1)} %shard_map.118) | data formatting | bytes 8192

commit v9 on v6

--- a/solution.py
+++ b/solution.py
@@ -35,6 +35,14 @@
 
 def nt_dot(a, b):
     return lax.dot_general(a, b, (((1,), (1,)), ((), ())), preferred_element_type=F32)
+
+
+def pieces(value, axis):
+    high = value.astype(BF16)
+    rest = value - high.astype(F32)
+    middle = rest.astype(BF16)
+    low = (rest - middle.astype(F32)).astype(BF16)
+    return jnp.concatenate([high, middle, low], axis=axis)
 
 
 def silu(v):
@@ -357,25 +365,23 @@
         == lax.broadcasted_iota(jnp.int32, (ROWS, NEP), 1)
     )
     spread = jnp.dot(
-        jnp.where(picked, 1.0, 0.0),
-        r_in[...].reshape(NEP, 256),
+        jnp.where(picked, 1.0, 0.0).astype(BF16),
+        pieces(r_in[...].reshape(NEP, 256), 1),
         preferred_element_type=F32,
-        precision=lax.Precision.HIGHEST,
-    )
+    )
+    spread = spread[:, 0:256] + spread[:, 256:512] + spread[:, 512:768]
     wanted = me_e * 8 + lax.broadcasted_iota(jnp.int32, (ROWS, 256), 0) % 4
     here = lax.broadcasted_iota(jnp.int32, (ROWS, 256), 1) == wanted
     row_scale = jnp.sum(jnp.where(here, spread, 0.0), axis=1, keepdims=True)
 
     def project(*slices, first=False):
-        sums = [None, None]
+        total = None
         for c, rel in slices:
             cols = pl.ds(pl.multiple_of((2 * ys[rel] + c) * PART, PART), PART)
             n = (gathered[c, ys[rel]].astype(F32) * row_scale * gain[:, cols]).astype(BF16)
-            for k in range(2):
-                v = nt_dot(n, w_gu[k, :, :, cols].reshape(256, PART))
-                sums[k] = v if sums[k] is None else sums[k] + v
-        for k in range(2):
-            acts[k] = sums[k] if first else acts[k] + sums[k]
+            v = nt_dot(n, w_gu[:, :, :, cols].reshape(512, PART))
+            total = v if total is None else total + v
+        acts[...] = total if first else acts[...] + total
 
     pass_wait(0)
     project((core, 0), (other, 0), (core, 6), (core, 2), first=True)
@@ -389,14 +395,15 @@
     pass_wait(6)
     pass_wait(2)
     project((core, 7), (core, 1), (other, 6), (other, 2))
+    pass_wait(7)
+    pass_wait(1)
+    project((other, 7), (other, 1))
     done.append(arrived(far_out, far_in, far_ssem, far_rsem, NEP - 1))
     raw = rcopy(far_in, far_par, fp_ssem, fp_rsem, partner)
     raw.start()
     for i, rel in enumerate(FAR):
         keep_rows(far_in[:, i], core, rel)
-    pass_wait(7)
-    pass_wait(1)
-    project((other, 7), (other, 1), (core, 3), (core, 4), (core, 5))
+    project((core, 3), (core, 4), (core, 5))
     raw.wait_recv()
     for i, rel in enumerate(FAR):
         keep_rows(far_par[:, i], other, rel)
@@ -406,7 +413,7 @@
     col = lax.broadcasted_iota(jnp.int32, (ROWS, 128), 1)
     mine = (row // 2) % 2 == col // 64
     for k in range(2):
-        v = acts[k]
+        v = acts[:, k * 256 : (k + 1) * 256]
         hidden = silu(v[:, 0:128]) * v[:, 128:256]
         hid[:, k * 128 : (k + 1) * 128] = jnp.where(mine, hidden, 0.0).astype(BF16)
     loaded(wd_own, 3)
@@ -414,12 +421,16 @@
 
     diagonal = row == col
 
-    def partial(rel):
-        k = ys[rel]
+    def partials(*rels):
         both = jnp.concatenate(
-            [wd_own[k].reshape(128, PART), wd_par[k].reshape(128, PART)], axis=0
+            [
+                jnp.concatenate([w[ys[rel]].reshape(128, PART) for rel in rels], axis=1)
+                for w in (wd_own, wd_par)
+            ],
+            axis=0,
         )
-        return jnp.dot(hid[...], both, preferred_element_type=F32)
+        v = jnp.dot(hid[...], both, preferred_element_type=F32)
+        return [v[:, i * PART : (i + 1) * PART] for i in range(len(rels))]
 
     def column(value):
         return jnp.sum(jnp.where(diagonal, value, 0.0), axis=0, keepdims=True)
@@ -437,8 +448,7 @@
             rcopy(s_out.at[k], s_in.at[k], sc_ssem, sc_rsem.at[k], device),
         )
 
-    def q_send(k):
-        value = partial(NEAR[k])
+    def q_send(k, value):
         most = jnp.maximum(jnp.max(jnp.abs(value), axis=1, keepdims=True), 1e-30)
         q_out[k] = jnp.round(value * (32767.0 / most)).astype(jnp.int16)
         s_out[k] = column(most * (1.0 / 32767.0))
@@ -451,21 +461,21 @@
         unit = jnp.sum(jnp.where(diagonal, s_in[k], 0.0), axis=1, keepdims=True)
         return q_in[k].astype(F32) * unit
 
-    values = [partial(rel) for rel in FAR]
+    values = partials(*FAR, 0)
+    kept[...] = values[3]
     most = jnp.maximum(jnp.maximum(jnp.abs(values[0]), jnp.abs(values[1])), jnp.abs(values[2]))
     most = jnp.maximum(jnp.max(most, axis=1, keepdims=True), 1e-30)
     fs_out[...] = column(most * (1.0 / 32767.0))
     for i in range(3):
         fq_out[:, i] = messages(jnp.round(values[i] * (32767.0 / most))).astype(jnp.int16)
     for peer in peers:
+        rcopy(fs_out, fs_in.at[me_e], fs_ssem, fs_rsem, (peer, me_t)).start()
+    for peer in peers:
         rcopy(fq_out.at[peer], fq_in.at[me_e], fq_ssem, fq_rsem, (peer, me_t)).start()
-    for k in range(4):
-        q_send(k)
-    for peer in peers:
-        rcopy(fs_out, fs_in.at[me_e], fs_ssem, fs_rsem, (peer, me_t)).start()
+    for k, value in enumerate(partials(*NEAR)):
+        q_send(k, value)
     fq_in[me_e] = fq_out[me_e]
     fs_in[me_e] = fs_out[...]
-    kept[...] = partial(0)
     done.append(arrived(dense_out, dense_in, dense_ssem, dense_rsem, NY - 1))
     dense = dense_in[0]
     for k in range(1, NY):
@@ -479,27 +489,30 @@
     for peer in peers:
         rcopy(ret_out.at[peer], ret_in.at[me_e], ret_ssem, ret_rsem, (peer, me_t)).start()
     ret_in[me_e] = ret_out[me_e]
-    done.append(arrived(fq_out, fq_in, fq_ssem, fq_rsem, NEP - 1))
     done.append(arrived(fs_in, fs_in, fs_ssem, fs_rsem, NEP - 1))
     lane2 = lax.broadcasted_iota(jnp.int32, (128, 256), 1)
     mine4 = lax.broadcasted_iota(jnp.int32, (128, 256), 0) == me_e * 4 + lane2 % 4
     unit = jnp.dot(
-        fs_in[...].reshape(NEP, 128),
-        jnp.where(mine4, 1.0, 0.0),
+        pieces(fs_in[...].reshape(NEP, 128), 0),
+        jnp.where(mine4, 1.0, 0.0).astype(BF16),
         preferred_element_type=F32,
-        precision=lax.Precision.HIGHEST,
-    )
+    )
+    unit = unit[0:NEP] + unit[NEP : 2 * NEP] + unit[2 * NEP : 3 * NEP]
     source = lax.broadcasted_iota(jnp.int32, (NEP, 256), 0)
     source = source == lax.broadcasted_iota(jnp.int32, (NEP, 256), 1) // 8
     unit = jnp.sum(jnp.where(source, unit, 0.0), axis=0, keepdims=True)
-    far_sum = jnp.dot(
-        comb[...] * unit,
-        jnp.concatenate(
-            [fq_in[:, i].astype(F32).reshape(256, 128) for i in range(3)], axis=1
-        ),
-        preferred_element_type=F32,
-        precision=lax.Precision.HIGHEST,
-    )
+    far_comb = pieces(comb[...] * unit, 0)
+    near_comb = pieces(comb[...], 0)
+    done.append(arrived(fq_out, fq_in, fq_ssem, fq_rsem, NEP - 1))
+    far_rows = jnp.concatenate(
+        [fq_in[:, i].astype(F32).reshape(256, 128) for i in range(3)], axis=1
+    )
+    far_high = far_rows.astype(BF16)
+    far_low = (far_rows - far_high.astype(F32)).astype(BF16)
+    far_sum = jnp.dot(far_comb, far_high, preferred_element_type=F32) + jnp.dot(
+        far_comb, far_low, preferred_element_type=F32
+    )
+    far_sum = far_sum[0:16] + far_sum[16:32] + far_sum[32:48]
     for i, rel in enumerate(FAR):
         cols = slice(i * 128, (i + 1) * 128)
         fy_out[i, :, 0:128] = far_sum[0:8, cols]
@@ -507,11 +520,10 @@
         rcopy(fy_out.at[i], fy_in.at[i], fy_ssem, fy_rsem, ydev(rel)).start()
     done.append(arrived(ret_out, ret_in, ret_ssem, ret_rsem, NEP - 1))
     mixed = jnp.dot(
-        comb[...],
-        ret_in[...].reshape(256, 128),
-        preferred_element_type=F32,
-        precision=lax.Precision.HIGHEST,
-    )
+        near_comb, pieces(ret_in[...].reshape(256, 128), 1), preferred_element_type=F32
+    )
+    mixed = mixed[:, 0:128] + mixed[:, 128:256] + mixed[:, 256:384]
+    mixed = mixed[0:16] + mixed[16:32] + mixed[32:48]
     combined = jnp.concatenate([mixed[0:8], mixed[8:16]], axis=1) + dense
     fy_copy = rcopy(fy_out, fy_in, fy_ssem, fy_rsem, partner)
     fy_copy.wait_recv()
@@ -602,7 +614,7 @@
             pltpu.VMEM((8, 256), F32),
             pltpu.VMEM((1, 256), F32),
             pltpu.VMEM((NEP, 1, 256), F32),
-            pltpu.VMEM((2, ROWS, 256), F32),
+            pltpu.VMEM((ROWS, 512), F32),
             pltpu.VMEM((ROWS, 256), BF16),
             pltpu.VMEM((4, ROWS, PART), jnp.int16),
             pltpu.VMEM((4, ROWS, PART), jnp.int16),

time: 54 us -> 52.5 us (0.972)
  Pallas kernels: 53.3 us -> 51.8 us
    pallas_call x1, Pallas kernels: 53.3 us -> 51.8 us  [local(): pl.pallas_call(kernel, out_shape=pltpu.VMEM((8, PART), BF16), in_specs=[p...]
where the time goes in v9:
time: 52.5 us; the launch traced here: 52.4 us
  Pallas kernels  51.8 us (99%)
  local copies, waits for them, and re-layouts  0.6 us (1%)
    pallas_call x1, Pallas kernels, local(): pl.pallas_call(kernel, out_shape=pltpu.VMEM((8, PART), BF16), in_specs=[p...  51.8 us

profile of v9, /device:TPU:1, one launch (start us, length us, event | category | flops | bytes accessed | tf_op | source)
XLA Modules:
  0.0 52.4 jit_solution(2311776891135834155)
XLA Ops:
  0.0 51.8 %shard_map.118 = bf16[8,256]{1,0:T(8,128)(2,1)S(1)} custom-call(bf16[8,256]{1,0:T(8,128)(2,1)} %tok_hbm.1, f32[1,4096]{1,0:T(1,128)} %bitcast.13, s32[2,8]{1,0:T(2,128)} %bitcast.15, f32[2,8]{1,0:T(2,128)} %bitcast.16, bf16[2,64,4096]{2,1,0:T(8,128)(2,1)} %bitcast.9, bf16[2,64,4096]{2,1,0:T(8,128)(2,1)} %bitcast.10, bf16[2,64,4096]{2,1,0:T(8,128)(2,1)} %wd.1, ...), custom_call_target="tpu_custom_call" | custom-call | tf_op jit(solution)/shard_map/pallas_call | solution.py:583
  51.8 0.6 %copy.14 = bf16[8,256]{1,0:T(8,128)(2,1)} copy(bf16[8,256]{1,0:T(8,128)(2,1)S(1)} %shard_map.118) | data formatting | bytes 8192

commit v10 on v9

--- a/solution.py
+++ b/solution.py
@@ -226,7 +226,14 @@
     weight = (jnp.where(is0, e0, 0.0) + jnp.where(is1, e1, 0.0)) / (e0 + e1) * placed
     comb[0:8, :] = jnp.where(half == 0, weight, 0.0)
     comb[8:16, :] = jnp.where(half == 1, weight, 0.0)
-    slots[...] = placed
+    left_half = lax.broadcasted_iota(jnp.int32, (256, 128), 0)
+    slot = lax.broadcasted_iota(jnp.int32, (256, 128), 1)
+    left_half = (left_half // 8 == slot // 4) & (left_half % 8 == slot % 4)
+    slots[...] = jnp.dot(
+        placed.astype(BF16),
+        jnp.where(left_half, 1.0, 0.0).astype(BF16),
+        preferred_element_type=F32,
+    )
     place[...] = jnp.concatenate(
         [jnp.where(half == 0, placed, 0.0), jnp.where(half == 1, placed, 0.0)], axis=0
     ).astype(BF16)
@@ -366,12 +373,12 @@
     )
     spread = jnp.dot(
         jnp.where(picked, 1.0, 0.0).astype(BF16),
-        pieces(r_in[...].reshape(NEP, 256), 1),
+        pieces(r_in[...].reshape(NEP, 128), 1),
         preferred_element_type=F32,
     )
-    spread = spread[:, 0:256] + spread[:, 256:512] + spread[:, 512:768]
-    wanted = me_e * 8 + lax.broadcasted_iota(jnp.int32, (ROWS, 256), 0) % 4
-    here = lax.broadcasted_iota(jnp.int32, (ROWS, 256), 1) == wanted
+    spread = spread[:, 0:128] + spread[:, 128:256] + spread[:, 256:384]
+    wanted = me_e * 4 + lax.broadcasted_iota(jnp.int32, (ROWS, 128), 0) % 4
+    here = lax.broadcasted_iota(jnp.int32, (ROWS, 128), 1) == wanted
     row_scale = jnp.sum(jnp.where(here, spread, 0.0), axis=1, keepdims=True)
 
     def project(*slices, first=False):
@@ -395,19 +402,26 @@
     pass_wait(6)
     pass_wait(2)
     project((core, 7), (core, 1), (other, 6), (other, 2))
+    done.append(arrived(far_out, far_in, far_ssem, far_rsem, NEP - 1))
+    raws = [
+        rcopy(far_in.at[:, i], far_par.at[:, i], fp_ssem, fp_rsem.at[i], partner)
+        for i in range(3)
+    ]
+    for copy in raws:
+        copy.start()
+    for i, rel in enumerate(FAR):
+        keep_rows(far_in[:, i], core, rel)
+    project((core, 3), (core, 4), (core, 5))
     pass_wait(7)
     pass_wait(1)
     project((other, 7), (other, 1))
-    done.append(arrived(far_out, far_in, far_ssem, far_rsem, NEP - 1))
-    raw = rcopy(far_in, far_par, fp_ssem, fp_rsem, partner)
-    raw.start()
-    for i, rel in enumerate(FAR):
-        keep_rows(far_in[:, i], core, rel)
-    project((core, 3), (core, 4), (core, 5))
-    raw.wait_recv()
-    for i, rel in enumerate(FAR):
-        keep_rows(far_par[:, i], other, rel)
-    project((other, 3), (other, 4), (other, 5))
+    for i in range(2):
+        raws[i].wait_recv()
+        keep_rows(far_par[:, i], other, FAR[i])
+    project((other, 3), (other, 4))
+    raws[2].wait_recv()
+    keep_rows(far_par[:, 2], other, FAR[2])
+    project((other, 5))
 
     row = lax.broadcasted_iota(jnp.int32, (ROWS, 128), 0)
     col = lax.broadcasted_iota(jnp.int32, (ROWS, 128), 1)
@@ -460,6 +474,9 @@
             copy.wait_recv()
         unit = jnp.sum(jnp.where(diagonal, s_in[k], 0.0), axis=1, keepdims=True)
         return q_in[k].astype(F32) * unit
+
+    for k, value in enumerate(partials(NEAR[0], NEAR[1])):
+        q_send(k, value)
 
     values = partials(*FAR, 0)
     kept[...] = values[3]
@@ -472,8 +489,8 @@
         rcopy(fs_out, fs_in.at[me_e], fs_ssem, fs_rsem, (peer, me_t)).start()
     for peer in peers:
         rcopy(fq_out.at[peer], fq_in.at[me_e], fq_ssem, fq_rsem, (peer, me_t)).start()
-    for k, value in enumerate(partials(*NEAR)):
-        q_send(k, value)
+    for k, value in enumerate(partials(NEAR[2], NEAR[3])):
+        q_send(2 + k, value)
     fq_in[me_e] = fq_out[me_e]
     fs_in[me_e] = fs_out[...]
     done.append(arrived(dense_out, dense_in, dense_ssem, dense_rsem, NY - 1))
@@ -560,7 +577,7 @@
     ]
     five = gathered.at[core, pl.ds(0, 5)]
     done.append(rcopy(five, five, pf_ssem, pf_rsem.at[0], partner))
-    for copy in parts + [dh_copy, raw, fy_copy] + done:
+    for copy in parts + [dh_copy, fy_copy] + raws + done:
         copy.wait_send()
 
 
@@ -611,9 +628,9 @@
             pltpu.VMEM((8, 64), BF16),
             pltpu.VMEM((16, 256), F32),
             pltpu.VMEM((16, 256), BF16),
-            pltpu.VMEM((8, 256), F32),
-            pltpu.VMEM((1, 256), F32),
-            pltpu.VMEM((NEP, 1, 256), F32),
+            pltpu.VMEM((8, 128), F32),
+            pltpu.VMEM((1, 128), F32),
+            pltpu.VMEM((NEP, 1, 128), F32),
             pltpu.VMEM((ROWS, 512), F32),
             pltpu.VMEM((ROWS, 256), BF16),
             pltpu.VMEM((4, ROWS, PART), jnp.int16),
@@ -651,7 +668,7 @@
             dma,
             dma((5,)),
             dma,
-            dma,
+            dma((3,)),
             dma,
             dma,
             dma,

time: 52.5 us -> 52.1 us (level)
  no operation moved by 1% of the time
where the time goes in v10:
time: 52.1 us; the launch traced here: 52 us
  Pallas kernels  51.4 us (99%)
  local copies, waits for them, and re-layouts  0.6 us (1%)
    pallas_call x1, Pallas kernels, local(): pl.pallas_call(kernel, out_shape=pltpu.VMEM((8, PART), BF16), in_specs=[p...  51.4 us

profile of v10, /device:TPU:1, one launch (start us, length us, event | category | flops | bytes accessed | tf_op | source)
XLA Modules:
  0.0 52.0 jit_solution(14424754245320633593)
XLA Ops:
  0.0 51.4 %shard_map.118 = bf16[8,256]{1,0:T(8,128)(2,1)S(1)} custom-call(bf16[8,256]{1,0:T(8,128)(2,1)} %tok_hbm.1, f32[1,4096]{1,0:T(1,128)} %bitcast.13, s32[2,8]{1,0:T(2,128)} %bitcast.15, f32[2,8]{1,0:T(2,128)} %bitcast.16, bf16[2,64,4096]{2,1,0:T(8,128)(2,1)} %bitcast.9, bf16[2,64,4096]{2,1,0:T(8,128)(2,1)} %bitcast.10, bf16[2,64,4096]{2,1,0:T(8,128)(2,1)} %wd.1, ...), custom_call_target="tpu_custom_call" | custom-call | tf_op jit(solution)/shard_map/pallas_call | solution.py:600
  51.4 0.6 %copy.14 = bf16[8,256]{1,0:T(8,128)(2,1)} copy(bf16[8,256]{1,0:T(8,128)(2,1)S(1)} %shard_map.118) | data formatting | bytes 8192

commit v11 on v10

--- a/solution.py
+++ b/solution.py
@@ -462,10 +462,12 @@
             rcopy(s_out.at[k], s_in.at[k], sc_ssem, sc_rsem.at[k], device),
         )
 
-    def q_send(k, value):
+    def q_pack(k, value):
         most = jnp.maximum(jnp.max(jnp.abs(value), axis=1, keepdims=True), 1e-30)
         q_out[k] = jnp.round(value * (32767.0 / most)).astype(jnp.int16)
         s_out[k] = column(most * (1.0 / 32767.0))
+
+    def q_send(k):
         for copy in q_copies(k, ydev(NEAR[k])):
             copy.start()
 
@@ -475,22 +477,27 @@
         unit = jnp.sum(jnp.where(diagonal, s_in[k], 0.0), axis=1, keepdims=True)
         return q_in[k].astype(F32) * unit
 
-    for k, value in enumerate(partials(NEAR[0], NEAR[1])):
-        q_send(k, value)
-
+    near2 = partials(NEAR[0], NEAR[1])
     values = partials(*FAR, 0)
+    q_pack(0, near2[0])
+    q_pack(1, near2[1])
     kept[...] = values[3]
     most = jnp.maximum(jnp.maximum(jnp.abs(values[0]), jnp.abs(values[1])), jnp.abs(values[2]))
     most = jnp.maximum(jnp.max(most, axis=1, keepdims=True), 1e-30)
     fs_out[...] = column(most * (1.0 / 32767.0))
     for i in range(3):
         fq_out[:, i] = messages(jnp.round(values[i] * (32767.0 / most))).astype(jnp.int16)
+    q_send(0)
+    q_send(1)
     for peer in peers:
         rcopy(fs_out, fs_in.at[me_e], fs_ssem, fs_rsem, (peer, me_t)).start()
     for peer in peers:
         rcopy(fq_out.at[peer], fq_in.at[me_e], fq_ssem, fq_rsem, (peer, me_t)).start()
-    for k, value in enumerate(partials(NEAR[2], NEAR[3])):
-        q_send(2 + k, value)
+    near1 = partials(NEAR[2], NEAR[3])
+    q_pack(2, near1[0])
+    q_pack(3, near1[1])
+    q_send(2)
+    q_send(3)
     fq_in[me_e] = fq_out[me_e]
     fs_in[me_e] = fs_out[...]
     done.append(arrived(dense_out, dense_in, dense_ssem, dense_rsem, NY - 1))

time: 52.1 us -> 51.9 us (level)
  no operation moved by 1% of the time
where the time goes in v11:
time: 51.9 us; the launch traced here: 51.8 us
  Pallas kernels  51.2 us (99%)
  local copies, waits for them, and re-layouts  0.6 us (1%)
    pallas_call x1, Pallas kernels, local(): pl.pallas_call(kernel, out_shape=pltpu.VMEM((8, PART), BF16), in_specs=[p...  51.2 us

profile of v11, /device:TPU:1, one launch (start us, length us, event | category | flops | bytes accessed | tf_op | source)
XLA Modules:
  0.0 51.8 jit_solution(8874236811001228535)
XLA Ops:
  0.0 51.2 %shard_map.118 = bf16[8,256]{1,0:T(8,128)(2,1)S(1)} custom-call(bf16[8,256]{1,0:T(8,128)(2,1)} %tok_hbm.1, f32[1,4096]{1,0:T(1,128)} %bitcast.13, s32[2,8]{1,0:T(2,128)} %bitcast.15, f32[2,8]{1,0:T(2,128)} %bitcast.16, bf16[2,64,4096]{2,1,0:T(8,128)(2,1)} %bitcast.9, bf16[2,64,4096]{2,1,0:T(8,128)(2,1)} %bitcast.10, bf16[2,64,4096]{2,1,0:T(8,128)(2,1)} %wd.1, ...), custom_call_target="tpu_custom_call" | custom-call | tf_op jit(solution)/shard_map/pallas_call | solution.py:607
  51.2 0.6 %copy.14 = bf16[8,256]{1,0:T(8,128)(2,1)} copy(bf16[8,256]{1,0:T(8,128)(2,1)S(1)} %shard_map.118) | data formatting | bytes 8192

commit v12 on v11

--- a/solution.py
+++ b/solution.py
@@ -82,6 +82,8 @@
     far_par,
     gathered,
     tok_all,
+    ss_out,
+    ss_in,
     dense_out,
     dense_in,
     dh_own,
@@ -119,6 +121,10 @@
     far_rsem,
     tok_ssem,
     tok_rsem,
+    tp_ssem,
+    tp_rsem,
+    ss_ssem,
+    ss_rsem,
     dh_ssem,
     dh_rsem,
     dense_ssem,
@@ -250,16 +256,31 @@
     tok_value = tok[...]
     a2a_out[...] = placed_rows(tok_value)
     a2a_in[me_e] = a2a_out[me_e]
-    tok_all[me_t] = tok_value
+    tok_all[core, y] = tok_value
+    token_diagonal = (
+        lax.broadcasted_iota(jnp.int32, (8, 128), 0)
+        == lax.broadcasted_iota(jnp.int32, (8, 128), 1)
+    )
+
+    def to_row(value):
+        return jnp.sum(jnp.where(token_diagonal, value, 0.0), axis=0, keepdims=True)
+
+    def to_column(value):
+        return jnp.sum(jnp.where(token_diagonal, value, 0.0), axis=1, keepdims=True)
+
+    wide = tok_value.astype(F32)
+    ss_out[...] = to_row(jnp.sum(wide * wide, axis=1, keepdims=True))
+    ss_in[me_t] = ss_out[...]
 
     pl.semaphore_wait(barrier, NEP - 1 + NTP - 1)
 
     for step in y_order:
+        rcopy(tok, tok_all.at[core, y], tok_ssem, tok_rsem, ydev(step)).start()
         for c in range(2):
             rcopy(
-                tok, tok_all.at[me_t], tok_ssem, tok_rsem, (me_e, ys[step] * 2 + c)
+                ss_out, ss_in.at[me_t], ss_ssem, ss_rsem, (me_e, ys[step] * 2 + c)
             ).start()
-    rcopy(tok, tok_all.at[me_t], tok_ssem, tok_rsem, partner).start()
+    rcopy(ss_out, ss_in.at[me_t], ss_ssem, ss_rsem, partner).start()
 
     for peer in peers:
         rcopy(a2a_out.at[peer], a2a_in.at[me_e], a2a_ssem, a2a_rsem, (peer, me_t)).start()
@@ -287,19 +308,23 @@
         copy.wait_recv()
         return copy
 
-    done = [arrived(tok_all, tok_all, tok_ssem, tok_rsem, NTP - 1)]
-    squares = jnp.zeros((8, PART), F32)
-    for j in range(NTP):
-        v = tok_all[j].astype(F32)
-        squares = squares + v * v
-    scale = lax.rsqrt(jnp.sum(squares, axis=1, keepdims=True) / WIDTH + EPS)
+    done = [arrived(ss_in, ss_in, ss_ssem, ss_rsem, NTP - 1)]
+    some = tok_all.at[0, pl.ds(0, NY - 1)]
+    tok_copy = rcopy(some, some, tok_ssem, tok_rsem, partner)
+    tok_copy.wait_recv()
+    squares = ss_in[0]
+    for j in range(1, NTP):
+        squares = squares + ss_in[j]
+    scale = lax.rsqrt(to_column(squares) / WIDTH + EPS)
     r_out[...] = jnp.sum(slots[...] * scale, axis=0, keepdims=True)
     for i, rel in enumerate(FAR):
-        far_out[:, i] = placed_rows(tok_all[ys[rel] * 2 + core])
+        far_out[:, i] = placed_rows(tok_all[core, ys[rel]])
     for peer in peers:
         rcopy(r_out, r_in.at[me_e], r_ssem, r_rsem, (peer, me_t)).start()
     for peer in peers:
         rcopy(far_out.at[peer], far_in.at[me_e], far_ssem, far_rsem, (peer, me_t)).start()
+    tok_pass = rcopy(tok_all.at[core], tok_all.at[core], tp_ssem, tp_rsem, partner)
+    tok_pass.start()
     r_in[me_e] = r_out[...]
     far_in[me_e] = far_out[me_e]
 
@@ -339,11 +364,12 @@
     for copy in smalls[3:6]:
         copy.wait()
     loaded(w_dense, 0)
+    rcopy(tok_all.at[other], tok_all.at[other], tp_ssem, tp_rsem, partner).wait_recv()
     act = jnp.zeros((8, 128), F32)
     mix_acc = jnp.zeros((8, PART), F32)
     for j in range(NTP):
         cols = slice(j * PART, (j + 1) * PART)
-        n = (tok_all[j].astype(F32) * scale * gain[:, cols]).astype(BF16)
+        n = (tok_all[j % 2, j // 2].astype(F32) * scale * gain[:, cols]).astype(BF16)
         mix_acc = mix_acc + n.astype(F32) * mixw[:, cols]
         act = act + nt_dot(n, w_dense[:, cols])
     gate_ref[...] = jnp.broadcast_to(
@@ -552,15 +578,7 @@
     fy_copy = rcopy(fy_out, fy_in, fy_ssem, fy_rsem, partner)
     fy_copy.wait_recv()
     combined = combined + fy_in[0] + fy_in[1] + fy_in[2]
-    token_diagonal = (
-        lax.broadcasted_iota(jnp.int32, (8, 128), 0)
-        == lax.broadcasted_iota(jnp.int32, (8, 128), 1)
-    )
-    own = jnp.sum(
-        jnp.where(token_diagonal, jnp.sum(combined * combined, axis=1, keepdims=True), 0.0),
-        axis=0,
-        keepdims=True,
-    )
+    own = to_row(jnp.sum(combined * combined, axis=1, keepdims=True))
     sq_out[...] = own
     for step in y_order:
         for c in range(2):
@@ -571,9 +589,7 @@
     total_sq = sq_in[0]
     for j in range(1, NTP):
         total_sq = total_sq + sq_in[j]
-    final = lax.rsqrt(
-        jnp.sum(jnp.where(token_diagonal, total_sq, 0.0), axis=1, keepdims=True) / WIDTH + EPS
-    )
+    final = lax.rsqrt(to_column(total_sq) / WIDTH + EPS)
     out[...] = (combined * final * ogain[...]).astype(BF16)
 
     near = gathered.at[core, pl.ds(0, 4)]
@@ -584,7 +600,7 @@
     ]
     five = gathered.at[core, pl.ds(0, 5)]
     done.append(rcopy(five, five, pf_ssem, pf_rsem.at[0], partner))
-    for copy in parts + [dh_copy, fy_copy] + raws + done:
+    for copy in parts + [tok_copy, tok_pass, dh_copy, fy_copy] + raws + done:
         copy.wait_send()
 
 
@@ -628,7 +644,9 @@
             pltpu.VMEM((NEP, 3, 8, 128), BF16),
             pltpu.VMEM((NEP, 3, 8, 128), BF16),
             pltpu.VMEM((2, NY, ROWS, PART), BF16),
-            pltpu.VMEM((NTP, 8, PART), BF16),
+            pltpu.VMEM((2, NY, 8, PART), BF16),
+            pltpu.VMEM((1, 128), F32),
+            pltpu.VMEM((NTP, 1, 128), F32),
             pltpu.VMEM((NY, 8, PART), F32),
             pltpu.VMEM((NY, 8, PART), F32),
             pltpu.VMEM((8, 64), BF16),
@@ -671,6 +689,10 @@
             dma,
             dma,
             dma,
+            dma,
+            dma,
+            dma,
+            dma,
             dma((4,)),
             dma,
             dma((5,)),

time: 51.9 us -> 52.1 us (level)
  no operation moved by 1% of the time
where the time goes in v12:
time: 52.1 us; the launch traced here: 52 us
  Pallas kernels  51.4 us (99%)
  local copies, waits for them, and re-layouts  0.6 us (1%)
    pallas_call x1, Pallas kernels, local(): pl.pallas_call(kernel, out_shape=pltpu.VMEM((8, PART), BF16), in_specs=[p...  51.4 us

profile of v12, /device:TPU:1, one launch (start us, length us, event | category | flops | bytes accessed | tf_op | source)
XLA Modules:
  0.0 52.0 jit_solution(1257011639460251047)
XLA Ops:
  0.0 51.4 %shard_map.118 = bf16[8,256]{1,0:T(8,128)(2,1)S(1)} custom-call(bf16[8,256]{1,0:T(8,128)(2,1)} %tok_hbm.1, f32[1,4096]{1,0:T(1,128)} %bitcast.13, s32[2,8]{1,0:T(2,128)} %bitcast.15, f32[2,8]{1,0:T(2,128)} %bitcast.16, bf16[2,64,4096]{2,1,0:T(8,128)(2,1)} %bitcast.9, bf16[2,64,4096]{2,1,0:T(8,128)(2,1)} %bitcast.10, bf16[2,64,4096]{2,1,0:T(8,128)(2,1)} %wd.1, ...), custom_call_target="tpu_custom_call" | custom-call | tf_op jit(solution)/shard_map/pallas_call | solution.py:623
  51.4 0.6 %copy.14 = bf16[8,256]{1,0:T(8,128)(2,1)} copy(bf16[8,256]{1,0:T(8,128)(2,1)S(1)} %shard_map.118) | data formatting | bytes 8192

commit v13 on v11

--- a/solution.py
+++ b/solution.py
@@ -16,7 +16,7 @@
 NEP = NX * NZ
 NTP = 2 * NY
 ROWS = 128
-FAR = (3, 4, 5)
+FAR = (4, 3, 5)
 NEAR = (6, 2, 7, 1)
 PART = 256
 WIDTH = 4096

time: 51.9 us -> 51.8 us (level)
  no operation moved by 1% of the time
where the time goes in v13:
time: 51.8 us; the launch traced here: 51.7 us
  Pallas kernels  51.1 us (99%)
  local copies, waits for them, and re-layouts  0.6 us (1%)
    pallas_call x1, Pallas kernels, local(): pl.pallas_call(kernel, out_shape=pltpu.VMEM((8, PART), BF16), in_specs=[p...  51.1 us

profile of v13, /device:TPU:1, one launch (start us, length us, event | category | flops | bytes accessed | tf_op | source)
XLA Modules:
  0.0 51.7 jit_solution(15278233240762028609)
XLA Ops:
  0.0 51.1 %shard_map.118 = bf16[8,256]{1,0:T(8,128)(2,1)S(1)} custom-call(bf16[8,256]{1,0:T(8,128)(2,1)} %tok_hbm.1, f32[1,4096]{1,0:T(1,128)} %bitcast.13, s32[2,8]{1,0:T(2,128)} %bitcast.15, f32[2,8]{1,0:T(2,128)} %bitcast.16, bf16[2,64,4096]{2,1,0:T(8,128)(2,1)} %bitcast.9, bf16[2,64,4096]{2,1,0:T(8,128)(2,1)} %bitcast.10, bf16[2,64,4096]{2,1,0:T(8,128)(2,1)} %wd.1, ...), custom_call_target="tpu_custom_call" | custom-call | tf_op jit(solution)/shard_map/pallas_call | solution.py:607
  51.1 0.6 %copy.14 = bf16[8,256]{1,0:T(8,128)(2,1)} copy(bf16[8,256]{1,0:T(8,128)(2,1)S(1)} %shard_map.118) | data formatting | bytes 8192

commit v14 on v10

--- a/solution.py
+++ b/solution.py
@@ -462,10 +462,12 @@
             rcopy(s_out.at[k], s_in.at[k], sc_ssem, sc_rsem.at[k], device),
         )
 
-    def q_send(k, value):
+    def q_pack(k, value):
         most = jnp.maximum(jnp.max(jnp.abs(value), axis=1, keepdims=True), 1e-30)
         q_out[k] = jnp.round(value * (32767.0 / most)).astype(jnp.int16)
         s_out[k] = column(most * (1.0 / 32767.0))
+
+    def q_send(k):
         for copy in q_copies(k, ydev(NEAR[k])):
             copy.start()
 
@@ -474,9 +476,6 @@
             copy.wait_recv()
         unit = jnp.sum(jnp.where(diagonal, s_in[k], 0.0), axis=1, keepdims=True)
         return q_in[k].astype(F32) * unit
-
-    for k, value in enumerate(partials(NEAR[0], NEAR[1])):
-        q_send(k, value)
 
     values = partials(*FAR, 0)
     kept[...] = values[3]
@@ -489,8 +488,10 @@
         rcopy(fs_out, fs_in.at[me_e], fs_ssem, fs_rsem, (peer, me_t)).start()
     for peer in peers:
         rcopy(fq_out.at[peer], fq_in.at[me_e], fq_ssem, fq_rsem, (peer, me_t)).start()
-    for k, value in enumerate(partials(NEAR[2], NEAR[3])):
-        q_send(2 + k, value)
+    for k, value in enumerate(partials(*NEAR)):
+        q_pack(k, value)
+    for k in range(4):
+        q_send(k)
     fq_in[me_e] = fq_out[me_e]
     fs_in[me_e] = fs_out[...]
     done.append(arrived(dense_out, dense_in, dense_ssem, dense_rsem, NY - 1))

time: 52.1 us -> 52.3 us (level)
  no operation moved by 1% of the time
where the time goes in v14:
time: 52.3 us; the launch traced here: 52.2 us
  Pallas kernels  51.6 us (99%)
  local copies, waits for them, and re-layouts  0.6 us (1%)
    pallas_call x1, Pallas kernels, local(): pl.pallas_call(kernel, out_shape=pltpu.VMEM((8, PART), BF16), in_specs=[p...  51.6 us

profile of v14, /device:TPU:1, one launch (start us, length us, event | category | flops | bytes accessed | tf_op | source)
XLA Modules:
  0.0 52.2 jit_solution(8486706502511132994)
XLA Ops:
  0.0 51.6 %shard_map.118 = bf16[8,256]{1,0:T(8,128)(2,1)S(1)} custom-call(bf16[8,256]{1,0:T(8,128)(2,1)} %tok_hbm.1, f32[1,4096]{1,0:T(1,128)} %bitcast.13, s32[2,8]{1,0:T(2,128)} %bitcast.15, f32[2,8]{1,0:T(2,128)} %bitcast.16, bf16[2,64,4096]{2,1,0:T(8,128)(2,1)} %bitcast.9, bf16[2,64,4096]{2,1,0:T(8,128)(2,1)} %bitcast.10, bf16[2,64,4096]{2,1,0:T(8,128)(2,1)} %wd.1, ...), custom_call_target="tpu_custom_call" | custom-call | tf_op jit(solution)/shard_map/pallas_call | solution.py:601
  51.6 0.6 %copy.14 = bf16[8,256]{1,0:T(8,128)(2,1)} copy(bf16[8,256]{1,0:T(8,128)(2,1)S(1)} %shard_map.118) | data formatting | bytes 8192

commit v15 on v11

--- a/solution.py
+++ b/solution.py
@@ -395,10 +395,6 @@
     for rel in (7, 1):
         ag_copy(rel, NEAR.index(rel), partner).wait_recv()
         pass_on(rel)
-    for step in y_order:
-        rcopy(
-            dense_out.at[ys[step]], dense_in.at[y], dense_ssem, dense_rsem, ydev(step)
-        ).start()
     pass_wait(6)
     pass_wait(2)
     project((core, 7), (core, 1), (other, 6), (other, 2))
@@ -409,6 +405,10 @@
     ]
     for copy in raws:
         copy.start()
+    for step in y_order:
+        rcopy(
+            dense_out.at[ys[step]], dense_in.at[y], dense_ssem, dense_rsem, ydev(step)
+        ).start()
     for i, rel in enumerate(FAR):
         keep_rows(far_in[:, i], core, rel)
     project((core, 3), (core, 4), (core, 5))

time: 51.9 us -> 51.9 us (level)
  no operation moved by 1% of the time
where the time goes in v15:
time: 51.9 us; the launch traced here: 51.8 us
  Pallas kernels  51.2 us (99%)
  local copies, waits for them, and re-layouts  0.6 us (1%)
    pallas_call x1, Pallas kernels, local(): pl.pallas_call(kernel, out_shape=pltpu.VMEM((8, PART), BF16), in_specs=[p...  51.2 us

profile of v15, /device:TPU:1, one launch (start us, length us, event | category | flops | bytes accessed | tf_op | source)
XLA Modules:
  0.0 51.8 jit_solution(300031792225319021)
XLA Ops:
  0.0 51.2 %shard_map.118 = bf16[8,256]{1,0:T(8,128)(2,1)S(1)} custom-call(bf16[8,256]{1,0:T(8,128)(2,1)} %tok_hbm.1, f32[1,4096]{1,0:T(1,128)} %bitcast.13, s32[2,8]{1,0:T(2,128)} %bitcast.15, f32[2,8]{1,0:T(2,128)} %bitcast.16, bf16[2,64,4096]{2,1,0:T(8,128)(2,1)} %bitcast.9, bf16[2,64,4096]{2,1,0:T(8,128)(2,1)} %bitcast.10, bf16[2,64,4096]{2,1,0:T(8,128)(2,1)} %wd.1, ...), custom_call_target="tpu_custom_call" | custom-call | tf_op jit(solution)/shard_map/pallas_call | solution.py:607
  51.2 0.6 %copy.14 = bf16[8,256]{1,0:T(8,128)(2,1)} copy(bf16[8,256]{1,0:T(8,128)(2,1)S(1)} %shard_map.118) | data formatting | bytes 8192
